TPU v7x, 256 devices: a 4x2x16 block of a 4x16x16 slice. The times are simulated.
256 devices in a mesh: grp: 2 (over y), ep: 64 (over z, x), tp: 2 (over core).
Axes of the slice: x: 4, y: 2, z: 16, core: 2. Of those that a mesh axis runs over, the one named last changes fastest.
The devices are a block of a 4x16x16 slice.
Arguments:
- tokens: bfloat16 [32768, 2048], P(('grp', 'ep'), 'tp'), parts along dimension 0, may hold values from -6 to 6
- norm_gain: bfloat16 [2048], P('tp'), may hold values from 0.099609375 to 1.8984375
- w_gate: bfloat16 [64, 2048, 1024], P('ep', None, 'tp'), may hold values from -0.125 to 0.125
- w_up: bfloat16 [64, 2048, 1024], P('ep', None, 'tp'), may hold values from -0.125 to 0.125
- w_down: bfloat16 [64, 1024, 2048], P('ep', 'tp'), may hold values from -0.1875 to 0.1875
- expert_ids: int32 [32768, 2], P(('grp', 'ep')), parts along dimension 0, may hold values from 0 to 63, as said below
- combine: float32 [32768, 2], P(('grp', 'ep')), parts along dimension 0, may hold values from 0.1 to 1
- final_gain: bfloat16 [2048], P('tp'), may hold values from 0.099609375 to 1.8984375
Outputs:
- result: bfloat16 [32768, 2048], P(('grp', 'ep'), 'tp'), parts along dimension 0
There are 2 independent parts, one for each index of `grp`. A program takes and returns all parts, laid end to end along the dimension named above; an argument that names none is the same for every part. Nothing has to cross between parts.
Inputs may be any that keep to these rules, and one draw needn't show every extreme that they name: `expert_ids`: the experts form 4 groups of consecutive ids of equal size; the 2 experts of a row are different and lie in one group. Among the rows of one index of ep no expert is named more than 20 times, and in each such block some expert is named exactly 20 times.
All inputs are finite; a program needn't handle non-finite values.
Results may differ from a plain program's by a relative error of at most 0.0077.
Values may be sent and summed in bfloat16 or wider, within the bound.
No kernel may reach another device: no remote copies, remote signals or barrier semaphores. Data moves between devices by JAX's collectives and lax.ppermute only.
A program may use at most 64 MiB of HBM per device.

v0:
```python
import jax
import jax.numpy as jnp
from jax import lax
from jax.sharding import PartitionSpec as P

GROUPS = 4


def total_of_pieces(x, axis):
    parts = lax.all_gather(x, axis)
    return parts.sum(axis=0)


def split_up(x, dim, count):
    lengths = x.shape
    parts = x.reshape(*lengths[:dim], count, lengths[dim] // count, *lengths[dim + 1 :])
    return jnp.moveaxis(parts, dim, 0)


def sent_and_summed(x, axis, dim):
    parts = split_up(x, dim, lax.axis_size(axis))
    arrived = lax.all_to_all(parts, axis, split_axis=0, concat_axis=0, tiled=True)
    return arrived.astype(jnp.float32).sum(axis=0)


def body(tokens, norm_gain, w_gate, w_up, w_down, expert_ids, combine, final_gain):
    eps = 1e-06
    tok_dev, half = tokens.shape
    n_ep = lax.axis_size("ep")
    n_tp = lax.axis_size("tp")
    width = half * n_tp
    exp_dev = w_gate.shape[0]
    experts = exp_dev * n_ep
    per_group = experts // GROUPS
    capacity = tok_dev // 8 * 5 * 2 // per_group
    top = expert_ids.shape[1]
    narrow = tokens.astype(jnp.float32)
    squares = total_of_pieces(jnp.sum(narrow * narrow, axis=1), "tp")
    scale = lax.rsqrt(squares[:, None] / width + eps)
    normed = (narrow * scale * norm_gain.astype(jnp.float32)).astype(jnp.bfloat16)
    columns = normed.shape[1]
    flat = expert_ids.reshape(-1)
    onehot = (flat[:, None] == jnp.arange(experts, dtype=jnp.int32)[None, :]).astype(jnp.int32)
    ranking = jnp.sum(jnp.cumsum(onehot, axis=0) * onehot, axis=1) - 1
    target = flat * capacity + ranking
    sources = jnp.arange(tok_dev * top, dtype=jnp.int32) // top
    owner = jnp.full((experts * capacity,), tok_dev, jnp.int32).at[target].set(sources)
    padded = jnp.concatenate([normed, jnp.zeros((1, columns), jnp.bfloat16)], axis=0)
    outgoing = padded[owner].reshape(n_ep, exp_dev * capacity, columns)
    arrived = lax.all_to_all(outgoing, "ep", split_axis=0, concat_axis=0, tiled=True)
    rows = (
        arrived.reshape(n_ep, exp_dev, capacity, columns)
        .transpose(1, 0, 2, 3)
        .reshape(exp_dev, n_ep * capacity, columns)
    )
    piece = lax.all_gather(rows, "tp", axis=2, tiled=True)
    gate = jnp.einsum("erd,edf->erf", piece, w_gate, preferred_element_type=jnp.float32)
    upper = jnp.einsum("erd,edf->erf", piece, w_up, preferred_element_type=jnp.float32)
    hidden = (jax.nn.silu(gate) * upper).astype(jnp.bfloat16)
    partial_out = jnp.einsum(
        "erf,efd->erd", hidden, w_down, preferred_element_type=jnp.float32
    ).astype(jnp.bfloat16)
    shares = sent_and_summed(partial_out, "tp", 2).astype(jnp.bfloat16)
    homeward = (
        shares.reshape(exp_dev, n_ep, capacity, half)
        .transpose(1, 0, 2, 3)
        .reshape(n_ep, exp_dev * capacity, half)
    )
    returned = lax.all_to_all(homeward, "ep", split_axis=0, concat_axis=0, tiled=True).reshape(
        experts * capacity, half
    )
    picked = returned[target].astype(jnp.float32).reshape(tok_dev, top, half)
    mixed = jnp.sum(picked * combine[:, :, None], axis=1)
    totals = total_of_pieces(jnp.sum(mixed * mixed, axis=1), "tp")
    norm = lax.rsqrt(totals[:, None] / width + eps)
    return (mixed * norm * final_gain.astype(jnp.float32)).astype(jnp.bfloat16)


def solution(mesh):
    placed = (
        P(("grp", "ep"), "tp"),
        P("tp"),
        P("ep", None, "tp"),
        P("ep", None, "tp"),
        P("ep", "tp", None),
        P(("grp", "ep"), None),
        P(("grp", "ep"), None),
        P("tp"),
    )
    return jax.shard_map(
        body, mesh=mesh, in_specs=placed, out_specs=P(("grp", "ep"), "tp"), check_vma=False
    )
```

profile of v0, /device:TPU:33, one launch (start us, length us, event | category | flops | bytes accessed | tf_op | source)
XLA Modules:
  0.0 464.1 jit_solution(18118570353789319803)
XLA Ops:
  6.5 0.0 copy-start
  6.6 0.0 all-gather.6.cloned.1.call-start
  6.6 1.0 copy.16
  7.5 0.1 eq.29
  7.7 0.1 eq.25
  7.8 0.7 broadcast_multiply_fusion
  8.5 1.2 reduce-window.6
  9.7 0.2 slice_reduce_fusion
  10.0 0.1 fusion.21
  10.1 0.1 copy.15
  10.3 0.1 mul.81
  10.4 2.5 scatter_custom_fusion
  12.9 1.2 fusion.17
  14.1 21.9 %all-gather.2 = f32[2,1,256]{2,1,0:T(1,128)S(1)} all-gather(f32[1,1,256]{2,1,0:T(1,128)S(1)} %bitcast.48), channel_id=2, replica_groups=mesh['grp'=2,'ep'=64,'tp'=2] {'tp'}, dimensions={0}, use_global_device_ids=true | all-gather | bytes 3072 | tf_op jit(solution)/shard_map/all_gather | solution.py:10
  36.1 0.7 convert_element_type.38
  36.8 1.2 fusion.19
  38.1 5.1 %gather_fusion = bf16[1280,1024]{1,0:T(8,128)(2,1)} fusion(bf16[257,1024]{1,0:T(8,128)(2,1)S(1)} %concatenate.3, s32[2048]{0:T(1024)S(1)} %pad_clamp_fusion), kind=kCustom, calls=%fused_computation | custom fusion | bytes 5248000 | tf_op jit(solution)/shard_map/gather | solution.py:49
  43.1 5.2 %reshape.113 = bf16[64,20,1024]{2,1,0:T(8,128)(2,1)} reshape(bf16[1280,1024]{1,0:T(8,128)(2,1)} %gather_fusion) | data formatting | bytes 5242880 | tf_op jit(solution)/shard_map/reshape | solution.py:49
  48.3 149.8 %all_to_all.15 = bf16[64,20,1024]{2,1,0:T(8,128)(2,1)} all-to-all(bf16[64,20,1024]{2,1,0:T(8,128)(2,1)} %reshape.113), channel_id=1, replica_groups=mesh['grp'=2,'ep'=64,'tp'=2] {'ep'}, dimensions={0} | all-to-all | bytes 5242880 | tf_op jit(solution)/shard_map/all_to_all | solution.py:50
  198.1 5.2 %reshape_transpose_reshape.6 = bf16[1,1280,1024]{2,1,0:T(8,128)(2,1)} reshape(bf16[64,20,1024]{2,1,0:T(8,128)(2,1)} %all_to_all.15) | data formatting | bytes 5242880 | tf_op jit(solution)/shard_map/reshape;transpose;reshape | solution.py:54
  203.3 0.1 all-gather.6.cloned.1.call-update
  203.3 21.7 %all-gather.6.cloned.1.call-done = bf16[1,1280,2048]{2,1,0:T(8,128)(2,1)} async-done(((bf16[1,1280,1024]{2,1,0:T(8,128)(2,1)}), bf16[1,1280,2048]{2,1,0:T(8,128)(2,1)}) %all-gather.6.cloned.1.call-update) | async-done | bytes 5242896 | tf_op jit(solution)/shard_map/all_gather | solution.py:56
  225.0 7.6 %fusion.2 = f32[1280,512]{1,0:T(8,128)} fusion(bf16[1,1280,2048]{2,1,0:T(8,128)(2,1)} %all-gather.6.cloned.1.call-done, bf16[1,2048,512]{2,1,0:T(8,128)(2,1)} %param.10), kind=kOutput, calls=%fused_computation.6 | convolution fusion | flops 2684354560 | bytes 9961472 | tf_op jit(solution)/shard_map/erd,edf->erf/dot_general | solution.py:57
  232.6 0.0 copy-done
  232.6 10.3 %convolution_convert_fusion = bf16[1280,2048]{1,0:T(8,128)(2,1)} fusion(bf16[1,512,2048]{2,1,0:T(8,128)(2,1)S(1)} %copy-done, bf16[1,1280,2048]{2,1,0:T(8,128)(2,1)} %all-gather.6.cloned.1.call-done, f32[1280,512]{1,0:T(8,128)} %fusion.2, bf16[1,2048,512]{2,1,0:T(8,128)(2,1)} %param.11), kind=kOutput, calls=%fused_computation.3 | convolution fusion | flops 5375262720 | bytes 17301504 | tf_op jit(solution)/shard_map/erf,efd->erd/dot_general | solution.py:60
  242.9 9.5 %reshape.118 = bf16[1,1280,2,1024]{3,2,1,0:T(2,128)(2,1)} reshape(bf16[1280,2048]{1,0:T(8,128)(2,1)} %convolution_convert_fusion) | data formatting | bytes 10485760 | tf_op jit(solution)/shard_map/reshape | solution.py:16
  252.4 4.1 copy.24
  256.5 9.0 %all_to_all.16 = bf16[2,1,1280,1024]{3,2,1,0:T(8,128)(2,1)} all-to-all(bf16[2,1,1280,1024]{3,2,1,0:T(8,128)(2,1)S(1)} %bitcast.44), channel_id=1, replica_groups=mesh['grp'=2,'ep'=64,'tp'=2] {'tp'}, dimensions={0} | all-to-all | bytes 10485760 | tf_op jit(solution)/shard_map/all_to_all | solution.py:22
  265.5 6.2 %reduce_sum.69 = bf16[1280,1024]{1,0:T(8,128)(2,1)} reduce(bf16[2,1,1280,1024]{3,2,1,0:T(8,128)(2,1)} %all_to_all.16, bf16[]{:T(256)} %constant.38.clone.1), dimensions={0,1}, to_apply=%region_6.7 | reduce | flops 1310720 | bytes 7864322 | tf_op jit(solution)/shard_map/reduce_sum | solution.py:23
  271.7 5.1 %reshape_transpose_reshape.7 = bf16[64,20,1024]{2,1,0:T(8,128)(2,1)} reshape(bf16[1280,1024]{1,0:T(8,128)(2,1)} %reduce_sum.69) | data formatting | bytes 5242880 | tf_op jit(solution)/shard_map/reshape;transpose;reshape | solution.py:67
  276.9 0.0 copy-start.1
  276.9 0.0 copy-start.2
  276.9 16.3 %all-to-all-start.2 = ((bf16[64,20,1024]{2,1,0:T(8,128)(2,1)}), bf16[64,20,1024]{2,1,0:T(8,128)(2,1)}, u32[]{:S(2)}, u32[]{:S(2)}) async-start(bf16[64,20,1024]{2,1,0:T(8,128)(2,1)} %reshape_transpose_reshape.7), calls=%async_computation.2 | async-start | bytes 6291456 | tf_op jit(solution)/shard_map/all_to_all | solution.py:69
  293.2 0.0 copy-done.1
  293.2 0.1 copy.20
  293.3 0.0 copy-done.2
  293.4 138.9 %all-to-all-done.2 = bf16[64,20,1024]{2,1,0:T(8,128)(2,1)} async-done(((bf16[64,20,1024]{2,1,0:T(8,128)(2,1)}), bf16[64,20,1024]{2,1,0:T(8,128)(2,1)}, u32[]{:S(2)}, u32[]{:S(2)}) %all-to-all-start.2) | async-done | bytes 2621472 | tf_op jit(solution)/shard_map/all_to_all | solution.py:69
  432.3 5.2 %reshape.119 = bf16[1280,1024]{1,0:T(8,128)(2,1)} reshape(bf16[64,20,1024]{2,1,0:T(8,128)(2,1)} %all-to-all-done.2) | data formatting | bytes 5242880 | tf_op jit(solution)/shard_map/reshape | solution.py:69
  437.4 4.8 %gather_fusion.1 = bf16[512,1024]{1,0:T(8,128)(2,1)S(1)} fusion(bf16[1280,1024]{1,0:T(8,128)(2,1)} %reshape.119, s32[1024]{0:T(1024)S(1)} %pad_clamp_fusion.1), kind=kCustom, calls=%fused_computation.1 | custom fusion | bytes 2099200 | tf_op jit(solution)/shard_map/gather | solution.py:72
  442.2 2.4 reshape.120
  444.6 4.3 multiply_reduce_fusion
  448.9 0.1 multiply_reduce_fusion.1
  449.1 7.2 %all-gather.3 = f32[2,1,256]{2,1,0:T(1,128)S(1)} all-gather(f32[1,1,256]{2,1,0:T(1,128)S(1)} %bitcast.49), channel_id=3, replica_groups=mesh['grp'=2,'ep'=64,'tp'=2] {'tp'}, dimensions={0}, use_global_device_ids=true | all-gather | bytes 3072 | tf_op jit(solution)/shard_map/all_gather | solution.py:10
  456.2 1.0 multiply_convert_fusion
  (15 shorter events, 0.2 us)
Async XLA Ops:
  6.5 226.0 %copy-start = (bf16[1,512,2048]{2,1,0:T(8,128)(2,1)S(1)}, bf16[1,512,2048]{2,1,0:T(8,128)(2,1)}, u32[]{:S(2)}) copy-start(bf16[1,512,2048]{2,1,0:T(8,128)(2,1)} %param.12) | copy-start | bytes 6291460
  6.6 218.5 %all-gather.6.cloned.1.call-start = ((), (), s32[]{:S(2)}) async-start(), calls=%async_computation.3 | async-start | bytes 7864320 | tf_op jit(solution)/shard_map/all_gather | solution.py:56
  276.9 16.3 %copy-start.1 = (f32[256,2]{0,1:T(2,128)S(1)}, f32[256,2]{0,1:T(2,128)}, u32[]{:S(2)}) copy-start(f32[256,2]{0,1:T(2,128)} %param.14) | copy-start | bytes 6148
  276.9 16.5 %copy-start.2 = (bf16[1024]{0:T(1024)(128)(2,1)S(1)}, bf16[1024]{0:T(1024)(128)(2,1)}, u32[]{:S(2)}) copy-start(bf16[1024]{0:T(1024)(128)(2,1)} %param.15) | copy-start | bytes 6148
  276.9 155.4 %all-to-all-start.2 = ((bf16[64,20,1024]{2,1,0:T(8,128)(2,1)}), bf16[64,20,1024]{2,1,0:T(8,128)(2,1)}, u32[]{:S(2)}, u32[]{:S(2)}) async-start(bf16[64,20,1024]{2,1,0:T(8,128)(2,1)} %reshape_transpose_reshape.7), calls=%async_computation.2 | async-start | bytes 6291456 | tf_op jit(solution)/shard_map/all_to_all | solution.py:69
Sparse Core Ops, SparseCore 0:
  203.4 21.5 all-gather.5
where the time goes:
time: 465 us; the launch traced here: 464 us
  blocking collectives  188 us (40%)
  waiting for transfers between devices  161 us (35%)
  local copies, waits for them, and re-layouts  50.9 us (11%)
  matrix products  17.9 us (4%)
  other arithmetic  16.9 us (4%)
  starting transfers between devices  16.3 us (4%)
  between operations  13.6 us (3%)
    all_to_all x1, blocking collectives, body(): lax.all_to_all(outgoing, 'ep', split_axis=0, concat_axis=0, tiled=True)  150 us
    all_to_all x1, waiting for transfers between devices, body(): lax.all_to_all(homeward, 'ep', split_axis=0, concat_axis=0, tiled=True)  139 us
    all_gather x2, blocking collectives, total_of_pieces(): parts = lax.all_gather(x, axis)  29.1 us
    all_gather x1, waiting for transfers between devices, body(): piece = lax.all_gather(rows, 'tp', axis=2, tiled=True)  21.7 us
    all_to_all x1, starting transfers between devices, body(): lax.all_to_all(homeward, 'ep', split_axis=0, concat_axis=0, tiled=True)  16.3 us
    reshape x2, local copies, waits for them, and re-layouts, split_up(): x.reshape(*lengths[:dim], count, lengths[dim] // count, *lengths[dim + 1:])  13.6 us
    dot_general x1, matrix products, body(): jnp.einsum('erf,efd->erd', hidden, w_down, preferred_element_type=jnp.flo...  10.3 us
  transfers between devices with their start and end apart: 2, of which 2 were waited for; matrix products, arithmetic and copies ran while one was open for 0% of the time, Pallas kernels for 0%

commit v1 on v0

v1 whole, which is shorter than its diff:
```python
import functools

import jax
import jax.numpy as jnp
from jax import lax
from jax.experimental import pallas as pl
from jax.experimental.pallas import tpu as pltpu
from jax.sharding import PartitionSpec as P

GROUPS = 4
EPS = 1e-06
LANES = 128
VMEM_LIMIT = 60 * 1024 * 1024


def dispatch_kernel(ids_ref, tok_ref, out_ref, pos_ref, tiles_ref, count_ref, *, capacity):
    tok_dev, half = tok_ref.shape
    sub = half // LANES
    top = ids_ref.shape[0]
    for j in range(sub):
        block = tok_ref[:, j * LANES : (j + 1) * LANES].astype(jnp.float32)
        tiles_ref[pl.ds(j, tok_dev, stride=sub), :] = block

    def clear(e, carry):
        count_ref[e] = 0
        return carry

    lax.fori_loop(0, count_ref.shape[0], clear, 0)

    def place(t, carry):
        row = tiles_ref[pl.ds(pl.multiple_of(t * sub, sub), sub), :].astype(jnp.bfloat16)
        for k in range(top):
            e = ids_ref[k, t]
            rank = count_ref[e]
            count_ref[e] = rank + 1
            slot = e * capacity + rank
            pos_ref[k, t] = slot
            out_ref[slot] = row
        return carry

    lax.fori_loop(0, tok_dev, place, 0, unroll=8)


def dispatch(ids, tokens, experts, capacity):
    tok_dev, half = tokens.shape
    sub = half // LANES
    return pl.pallas_call(
        functools.partial(dispatch_kernel, capacity=capacity),
        out_shape=(
            jax.ShapeDtypeStruct((experts * capacity, sub, LANES), jnp.bfloat16),
            jax.ShapeDtypeStruct(ids.shape, jnp.int32),
        ),
        in_specs=[
            pl.BlockSpec(memory_space=pltpu.SMEM),
            pl.BlockSpec(memory_space=pltpu.VMEM),
        ],
        out_specs=(
            pl.BlockSpec(memory_space=pltpu.VMEM),
            pl.BlockSpec(memory_space=pltpu.SMEM),
        ),
        scratch_shapes=[
            pltpu.VMEM((tok_dev * sub, LANES), jnp.float32),
            pltpu.SMEM((experts,), jnp.int32),
        ],
        compiler_params=pltpu.CompilerParams(vmem_limit_bytes=VMEM_LIMIT),
        name="dispatch",
    )(ids, tokens)


def expert_kernel(
    arr_ref, gain_ref, wg0, wg1, wu0, wu1, wd0, wd1, out_ref,
    tiles_ref, x_ref, hid_ref, wg_ref, wu_ref, wd_ref, sems, *, n_tp, per_part, width,
):
    rows = x_ref.shape[0]
    sub = arr_ref.shape[1]
    half = sub * LANES
    sources = rows // per_part
    copies = []
    for i, (src, dst) in enumerate(
        ((wg0, wg_ref.at[0]), (wg1, wg_ref.at[1]), (wu0, wu_ref.at[0]), (wu1, wu_ref.at[1]),
         (wd0, wd_ref.at[0]), (wd1, wd_ref.at[1]))
    ):
        copy = pltpu.make_async_copy(src.at[0], dst, sems.at[i])
        copy.start()
        copies.append(copy)

    def spread(s, carry):
        for c in range(n_tp):
            part = arr_ref[pl.ds((s * n_tp + c) * per_part, per_part)].astype(jnp.float32)
            at = pl.multiple_of(s * (per_part * sub), per_part * sub)
            tiles_ref[c, pl.ds(at, per_part * sub), :] = part.reshape(per_part * sub, LANES)
        return carry

    lax.fori_loop(0, sources, spread, 0, unroll=4)

    block = 80

    def normalize(b, carry):
        def piece(c, j):
            return tiles_ref[c, pl.ds(b * (block * sub) + j, block, stride=sub), :]

        squares = jnp.zeros((block, LANES), jnp.float32)
        for c in range(n_tp):
            for j in range(sub):
                v = piece(c, j)
                squares += v * v
        scale = lax.rsqrt(jnp.sum(squares, axis=1, keepdims=True) / width + EPS)
        at = pl.ds(pl.multiple_of(b * block, block), block)
        for c in range(n_tp):
            for j in range(sub):
                lo = c * half + j * LANES
                v = piece(c, j) * scale * gain_ref[:, lo : lo + LANES]
                x_ref[at, lo : lo + LANES] = v.astype(jnp.bfloat16)
        return carry

    lax.fori_loop(0, rows // block, normalize, 0)

    ff = wg_ref.shape[2]
    step = 256
    for h in range(n_tp):
        copies[h].wait()
        copies[n_tp + h].wait()
        for n in range(ff // step):
            cols = slice(n * step, (n + 1) * step)
            gate = jnp.dot(x_ref[...], wg_ref[h, :, cols], preferred_element_type=jnp.float32)
            upper = jnp.dot(x_ref[...], wu_ref[h, :, cols], preferred_element_type=jnp.float32)
            hidden = (gate / (1.0 + jnp.exp(-gate))) * upper
            hid_ref[:, h * ff + n * step : h * ff + (n + 1) * step] = hidden.astype(jnp.bfloat16)
    for h in range(n_tp):
        copies[2 * n_tp + h].wait()
    for c in range(n_tp):
        for n in range(half // step):
            lo = c * half + n * step
            total = jnp.dot(
                hid_ref[...],
                jnp.concatenate([wd_ref[h, :, lo : lo + step] for h in range(n_tp)], axis=0),
                preferred_element_type=jnp.float32,
            )
            for i in range(step // LANES):
                j = n * (step // LANES) + i
                tiles_ref[c, pl.ds(j, rows, stride=sub), :] = total[:, i * LANES : (i + 1) * LANES]

    def gather(s, carry):
        for c in range(n_tp):
            at = pl.multiple_of(s * (per_part * sub), per_part * sub)
            part = tiles_ref[c, pl.ds(at, per_part * sub), :].reshape(per_part, sub, LANES)
            out_ref[pl.ds((s * n_tp + c) * per_part, per_part)] = part.astype(jnp.bfloat16)
        return carry

    lax.fori_loop(0, sources, gather, 0, unroll=4)


def expert(arrived, gain, gates, uppers, downs, per_part, n_tp):
    total, sub, lanes = arrived.shape
    rows = total // n_tp
    _, width, ff = gates[0].shape
    anywhere = pl.BlockSpec(memory_space=pl.ANY)
    return pl.pallas_call(
        functools.partial(expert_kernel, n_tp=n_tp, per_part=per_part, width=width),
        out_shape=jax.ShapeDtypeStruct(arrived.shape, jnp.bfloat16),
        in_specs=[pl.BlockSpec(memory_space=pltpu.VMEM), pl.BlockSpec(memory_space=pltpu.VMEM)]
        + [anywhere] * (3 * n_tp),
        out_specs=pl.BlockSpec(memory_space=pltpu.VMEM),
        scratch_shapes=[
            pltpu.VMEM((n_tp, rows * sub, lanes), jnp.float32),
            pltpu.VMEM((rows, width), jnp.bfloat16),
            pltpu.VMEM((rows, ff * n_tp), jnp.bfloat16),
            pltpu.VMEM((n_tp, width, ff), jnp.bfloat16),
            pltpu.VMEM((n_tp, width, ff), jnp.bfloat16),
            pltpu.VMEM((n_tp, ff, width), jnp.bfloat16),
            pltpu.SemaphoreType.DMA((3 * n_tp,)),
        ],
        compiler_params=pltpu.CompilerParams(vmem_limit_bytes=VMEM_LIMIT),
        cost_estimate=pl.CostEstimate(
            flops=6 * rows * width * ff * n_tp, transcendentals=rows * ff * n_tp,
            bytes_accessed=12 * width * ff + 4 * total * sub * lanes,
        ),
        name="expert",
    )(arrived, gain, *gates, *uppers, *downs)


def combine_kernel(pos_ref, mix_ref, ret_ref, out_ref, sq_ref, tiles_ref):
    top, tok_dev = pos_ref.shape
    sub = ret_ref.shape[1]

    def pick(t, carry):
        total = mix_ref[0, t] * ret_ref[pos_ref[0, t]].astype(jnp.float32)
        for k in range(1, top):
            total += mix_ref[k, t] * ret_ref[pos_ref[k, t]].astype(jnp.float32)
        tiles_ref[pl.ds(pl.multiple_of(t * sub, sub), sub), :] = total
        return carry

    lax.fori_loop(0, tok_dev, pick, 0, unroll=8)
    squares = jnp.zeros((tok_dev, LANES), jnp.float32)
    for j in range(sub):
        v = tiles_ref[pl.ds(j, tok_dev, stride=sub), :]
        out_ref[:, j * LANES : (j + 1) * LANES] = v
        squares += v * v
    sq_ref[...] = jnp.sum(squares, axis=1, keepdims=True)


def combined(pos, mix, returned):
    _, tok_dev = pos.shape
    _, sub, lanes = returned.shape
    return pl.pallas_call(
        combine_kernel,
        out_shape=(
            jax.ShapeDtypeStruct((tok_dev, sub * lanes), jnp.float32),
            jax.ShapeDtypeStruct((tok_dev, 1), jnp.float32),
        ),
        in_specs=[
            pl.BlockSpec(memory_space=pltpu.SMEM),
            pl.BlockSpec(memory_space=pltpu.SMEM),
            pl.BlockSpec(memory_space=pltpu.VMEM),
        ],
        out_specs=(
            pl.BlockSpec(memory_space=pltpu.VMEM),
            pl.BlockSpec(memory_space=pltpu.VMEM),
        ),
        scratch_shapes=[pltpu.VMEM((tok_dev * sub, lanes), jnp.float32)],
        compiler_params=pltpu.CompilerParams(vmem_limit_bytes=VMEM_LIMIT),
        name="combine",
    )(pos, mix, returned)


def body(tokens, norm_gain, w_gate, w_up, w_down, expert_ids, combine, final_gain):
    tok_dev, half = tokens.shape
    n_ep = lax.axis_size("ep")
    n_tp = lax.axis_size("tp")
    width = half * n_tp
    experts = w_gate.shape[0] * n_ep
    capacity = tok_dev // 8 * 5 * 2 // (experts // GROUPS)
    per_part = capacity // n_tp
    sub = half // LANES

    swap = [(i, (i + 1) % n_tp) for i in range(n_tp)]
    others = [lax.ppermute(w, "tp", swap) for w in (w_gate, w_up, w_down)]
    gain = lax.all_gather(norm_gain.astype(jnp.float32), "tp", tiled=True)[None, :]

    outgoing, pos = dispatch(expert_ids.T, tokens, experts, capacity)
    shape = (n_ep * n_tp, per_part, sub, LANES)
    arrived = lax.all_to_all(
        outgoing.reshape(shape), ("ep", "tp"), split_axis=0, concat_axis=0, tiled=True
    )
    results = expert(
        arrived.reshape(-1, sub, LANES), gain, (w_gate, others[0]), (w_up, others[1]),
        (w_down, others[2]), per_part, n_tp,
    )
    returned = lax.all_to_all(
        results.reshape(shape), ("ep", "tp"), split_axis=0, concat_axis=0, tiled=True
    )
    mixed, squares = combined(pos, combine.T, returned.reshape(-1, sub, LANES))
    totals = lax.all_gather(squares[:, 0], "tp").sum(axis=0)
    norm = lax.rsqrt(totals[:, None] / width + EPS)
    return (mixed * norm * final_gain.astype(jnp.float32)).astype(jnp.bfloat16)


def solution(mesh):
    placed = (
        P(("grp", "ep"), "tp"),
        P("tp"),
        P("ep", None, "tp"),
        P("ep", None, "tp"),
        P("ep", "tp", None),
        P(("grp", "ep"), None),
        P(("grp", "ep"), None),
        P("tp"),
    )
    return jax.shard_map(
        body, mesh=mesh, in_specs=placed, out_specs=P(("grp", "ep"), "tp"), check_vma=False
    )
```

time: 465 us -> 315 us (0.68)
  blocking collectives: 188 us -> 13.6 us
  waiting for transfers between devices: 161 us -> 221 us
  local copies, waits for them, and re-layouts: 50.9 us -> 5.78 us
  starting transfers between devices: 16.3 us -> 46.5 us
  Pallas kernels: 0 us -> 25.4 us
  matrix products: 17.9 us -> 0 us
  other arithmetic: 16.9 us -> 2.36 us
  between operations: 13.6 us -> 0.08 us
    all_to_all x2 -> x0, blocking collectives: 159 us -> none  [the longest x1 150 us: body(): lax.all_to_all(outgoing, 'ep', split_axis=0, concat_axis=0, tiled=True)]
    all_to_all x1 -> x2, waiting for transfers between devices: 139 us -> 221 us  [the longest x1 118 us: body(): lax.all_to_all(results.reshape(shape), ('ep', 'tp'), split_axis=0, concat...]
    all_to_all x1 -> x2, starting transfers between devices: 16.3 us -> 43.3 us  [the longest x1 31 us: body(): lax.all_to_all(outgoing.reshape(shape), ('ep', 'tp'), split_axis=0, conca...]
    pallas_call x0 -> x3, Pallas kernels: none -> 25.4 us  [the longest x1 15.3 us: expert(): pl.pallas_call(functools.partial(expert_kernel, n_tp=n_tp, per_part=per_p...]
    reshape x4 -> x0, local copies, waits for them, and re-layouts: 23.9 us -> none  [the longest x2 13.6 us: split_up(): x.reshape(*lengths[:dim], count, lengths[dim] // count, *lengths[dim + 1:])]
    all_gather x1 -> x0, waiting for transfers between devices: 21.7 us -> none  [body(): piece = lax.all_gather(rows, 'tp', axis=2, tiled=True)]
    dot_general x2 -> x0, matrix products: 17.9 us -> none  [the longest x1 10.3 us: body(): jnp.einsum('erf,efd->erd', hidden, w_down, preferred_element_type=jnp.flo...]
    all_gather x2, blocking collectives: 29.1 us -> 13.6 us  [the longest x1 9.62 us: body(): lax.all_gather(norm_gain.astype(jnp.float32), 'tp', tiled=True)[None, :]]
  transfers between devices with their start and end apart: 2 -> 5, of which waited for: 2 -> 2; matrix products, arithmetic and copies ran while one was open for 0% -> 0% of each run, Pallas kernels for 0% -> 0%
where the time goes in v1:
time: 315 us; the launch traced here: 314 us
  waiting for transfers between devices  221 us (70%)
  starting transfers between devices  46.5 us (15%)
  Pallas kernels  25.4 us (8%)
  blocking collectives  13.6 us (4%)
  local copies, waits for them, and re-layouts  5.78 us (2%)
    all_to_all x1, waiting for transfers between devices, body(): lax.all_to_all(results.reshape(shape), ('ep', 'tp'), split_axis=0, concat...  118 us
    all_to_all x1, waiting for transfers between devices, body(): lax.all_to_all(outgoing.reshape(shape), ('ep', 'tp'), split_axis=0, conca...  103 us
    all_to_all x1, starting transfers between devices, body(): lax.all_to_all(outgoing.reshape(shape), ('ep', 'tp'), split_axis=0, conca...  31 us
    pallas_call x1, Pallas kernels, expert(): pl.pallas_call(functools.partial(expert_kernel, n_tp=n_tp, per_part=per_p...  15.3 us
    all_to_all x1, starting transfers between devices, body(): lax.all_to_all(results.reshape(shape), ('ep', 'tp'), split_axis=0, concat...  12.3 us
    all_gather x1, blocking collectives, body(): lax.all_gather(norm_gain.astype(jnp.float32), 'tp', tiled=True)[None, :]  9.62 us
  transfers between devices with their start and end apart: 5, of which 2 were waited for; matrix products, arithmetic and copies ran while one was open for 0% of the time, Pallas kernels for 0%

profile of v1, /device:TPU:33, one launch (start us, length us, event | category | flops | bytes accessed | tf_op | source)
XLA Modules:
  0.0 314.4 jit_solution(11452407933117789197)
XLA Ops:
  0.0 5.8 %dispatch.1 = (bf16[1280,8,128]{2,1,0:T(8,128)(2,1)}, s32[2,256]{1,0:T(2,128)}) custom-call(s32[2,256]{1,0:T(2,128)} %bitcast.12, bf16[256,1024]{1,0:T(8,128)(2,1)} %tok_ref.1), custom_call_target="tpu_custom_call" | custom-call | tf_op jit(solution)/shard_map/dispatch/pallas_call | solution.py:47
  5.8 0.0 copy-start.2
  5.8 31.0 %all-to-all-start = ((bf16[128,10,8,128]{3,2,1,0:T(8,128)(2,1)}), bf16[128,10,8,128]{3,2,1,0:T(8,128)(2,1)S(1)}, u32[]{:S(2)}, u32[]{:S(2)}) async-start(bf16[128,10,8,128]{3,2,1,0:T(8,128)(2,1)} %bitcast.9), calls=%async_computation | async-start | bytes 5242880 | tf_op jit(solution)/shard_map/all_to_all | solution.py:242
  36.8 2.7 collective-permute-start
  39.5 0.2 collective-permute-start.1
  39.7 0.4 collective-permute-start.2
  40.1 0.0 copy-done.2
  40.1 9.6 %all_gather.6 = f32[2048]{0:T(1024)} all-gather(f32[1024]{0:T(1024)S(1)} %convert_element_type.9), channel_id=1, replica_groups=mesh['grp'=2,'ep'=64,'tp'=2] {'tp'}, dimensions={0}, use_global_device_ids=true | all-gather | bytes 12288 | tf_op jit(solution)/shard_map/all_gather | solution.py:238
  49.7 0.0 collective-permute-done.wg1
  49.7 0.0 copy-start.4
  49.7 0.0 collective-permute-done.1.wu1
  49.7 1.3 copy-done.4
  51.0 0.0 copy-start.5
  51.0 1.4 copy-done.5
  52.4 0.0 collective-permute-done.2.wd1
  52.4 102.6 %all-to-all-done = bf16[128,10,8,128]{3,2,1,0:T(8,128)(2,1)S(1)} async-done(((bf16[128,10,8,128]{3,2,1,0:T(8,128)(2,1)}), bf16[128,10,8,128]{3,2,1,0:T(8,128)(2,1)S(1)}, u32[]{:S(2)}, u32[]{:S(2)}) %all-to-all-start) | async-done | bytes 2621472 | tf_op jit(solution)/shard_map/all_to_all | solution.py:242
  155.0 0.0 copy-start.1
  155.0 1.5 copy-done.1
  156.5 15.3 %expert.1 = bf16[1280,8,128]{2,1,0:T(8,128)(2,1)} custom-call(bf16[1280,8,128]{2,1,0:T(8,128)(2,1)} %bitcast.8, f32[1,2048]{1,0:T(1,128)} %bitcast.11, bf16[1,2048,512]{2,1,0:T(8,128)(2,1)} %wg0.1, bf16[1,2048,512]{2,1,0:T(8,128)(2,1)} %copy-done.4, bf16[1,2048,512]{2,1,0:T(8,128)(2,1)} %wu0.1, bf16[1,2048,512]{2,1,0:T(8,128)(2,1)} %copy-done.5, ...), custom_call_target="tpu_custom_call" | custom-call | flops 8053063680 | bytes 17825792 | tf_op jit(solution)/shard_map/expert/pallas_call | solution.py:158
  171.9 0.0 copy-start.3
  171.9 12.3 %all-to-all-start.1 = ((bf16[128,10,8,128]{3,2,1,0:T(8,128)(2,1)}), bf16[128,10,8,128]{3,2,1,0:T(8,128)(2,1)S(1)}, u32[]{:S(2)}, u32[]{:S(2)}) async-start(bf16[128,10,8,128]{3,2,1,0:T(8,128)(2,1)} %bitcast.10), calls=%async_computation.1 | async-start | bytes 5242880 | tf_op jit(solution)/shard_map/all_to_all | solution.py:249
  184.1 0.0 copy-done.3
  184.2 118.1 %all-to-all-done.1 = bf16[128,10,8,128]{3,2,1,0:T(8,128)(2,1)S(1)} async-done(((bf16[128,10,8,128]{3,2,1,0:T(8,128)(2,1)}), bf16[128,10,8,128]{3,2,1,0:T(8,128)(2,1)S(1)}, u32[]{:S(2)}, u32[]{:S(2)}) %all-to-all-start.1) | async-done | bytes 2621472 | tf_op jit(solution)/shard_map/all_to_all | solution.py:249
  302.3 0.0 copy-start
  302.3 1.5 copy-done
  303.8 4.2 %combine.1 = (f32[256,1024]{1,0:T(8,128)}, f32[256,1]{1,0:T(8,128)}) custom-call(s32[2,256]{1,0:T(2,128)} %get-tuple-element.9.pos_ref, f32[2,256]{1,0:T(2,128)} %bitcast.13, bf16[1280,8,128]{2,1,0:T(8,128)(2,1)} %bitcast.7), custom_call_target="tpu_custom_call" | custom-call | tf_op jit(solution)/shard_map/combine/pallas_call | solution.py:205
  308.0 3.9 %all-gather = f32[512,1]{1,0:T(8,128)S(1)} all-gather(f32[256,1]{1,0:T(8,128)} %get-tuple-element.12), channel_id=2, replica_groups=mesh['grp'=2,'ep'=64,'tp'=2] {'tp'}, dimensions={0}, use_global_device_ids=true | all-gather | bytes 3072 | tf_op jit(solution)/shard_map/all_gather | solution.py:253
  312.0 0.1 reduce
  312.2 2.2 multiply_convert_fusion
  (5 shorter events, 0.1 us)
Async XLA Ops:
  5.8 34.2 %copy-start.2 = (bf16[1024]{0:T(1024)(128)(2,1)S(1)}, bf16[1024]{0:T(1024)(128)(2,1)}, u32[]{:S(2)}) copy-start(bf16[1024]{0:T(1024)(128)(2,1)} %param.9) | copy-start | bytes 6148
  5.8 149.2 %all-to-all-start = ((bf16[128,10,8,128]{3,2,1,0:T(8,128)(2,1)}), bf16[128,10,8,128]{3,2,1,0:T(8,128)(2,1)S(1)}, u32[]{:S(2)}, u32[]{:S(2)}) async-start(bf16[128,10,8,128]{3,2,1,0:T(8,128)(2,1)} %bitcast.9), calls=%async_computation | async-start | bytes 5242880 | tf_op jit(solution)/shard_map/all_to_all | solution.py:242
  36.8 12.8 %collective-permute-start = (bf16[1,2048,512]{2,1,0:T(8,128)(2,1)}, bf16[1,2048,512]{2,1,0:T(8,128)(2,1)S(1)}, u32[]{:S(2)}, u32[]{:S(2)}) collective-permute-start(bf16[1,2048,512]{2,1,0:T(8,128)(2,1)} %wg0.1), channel_id=1, source_target_pairs={{0,1},{1,0},{2,3},{3,2},{4,5},{5,4},{6,7},{7,6},{8,9},{9,8},{10,11... | collective-permute-start | bytes 6291464 | tf_op jit(solution)/shard_map/ppermute | solution.py:237
  39.5 10.1 %collective-permute-start.1 = (bf16[1,2048,512]{2,1,0:T(8,128)(2,1)}, bf16[1,2048,512]{2,1,0:T(8,128)(2,1)S(1)}, u32[]{:S(2)}, u32[]{:S(2)}) collective-permute-start(bf16[1,2048,512]{2,1,0:T(8,128)(2,1)} %wu0.1), channel_id=1, source_target_pairs={{0,1},{1,0},{2,3},{3,2},{4,5},{5,4},{6,7},{7,6},{8,9},{9,8},{10,11... | collective-permute-start | bytes 6291464 | tf_op jit(solution)/shard_map/ppermute | solution.py:237
  39.7 12.7 %collective-permute-start.2 = (bf16[1,512,2048]{2,1,0:T(8,128)(2,1)}, bf16[1,512,2048]{2,1,0:T(8,128)(2,1)}, u32[]{:S(2)}, u32[]{:S(2)}) collective-permute-start(bf16[1,512,2048]{2,1,0:T(8,128)(2,1)} %wd0.1), channel_id=1, source_target_pairs={{0,1},{1,0},{2,3},{3,2},{4,5},{5,4},{6,7},{7,6},{8,9},{9,8},{10,11... | collective-permute-start | bytes 6291464 | tf_op jit(solution)/shard_map/ppermute | solution.py:237
  49.7 1.3 copy-start.4
  51.0 1.4 copy-start.5
  155.0 1.5 copy-start.1
  171.9 12.3 %copy-start.3 = (bf16[1024]{0:T(1024)(128)(2,1)S(1)}, bf16[1024]{0:T(1024)(128)(2,1)}, u32[]{:S(2)}) copy-start(bf16[1024]{0:T(1024)(128)(2,1)} %param.15) | copy-start | bytes 6148
  171.9 130.4 %all-to-all-start.1 = ((bf16[128,10,8,128]{3,2,1,0:T(8,128)(2,1)}), bf16[128,10,8,128]{3,2,1,0:T(8,128)(2,1)S(1)}, u32[]{:S(2)}, u32[]{:S(2)}) async-start(bf16[128,10,8,128]{3,2,1,0:T(8,128)(2,1)} %bitcast.10), calls=%async_computation.1 | async-start | bytes 5242880 | tf_op jit(solution)/shard_map/all_to_all | solution.py:249
  302.3 1.5 copy-start

commit v2 on v1

--- a/solution.py
+++ b/solution.py
@@ -10,10 +10,12 @@
 GROUPS = 4
 EPS = 1e-06
 LANES = 128
-VMEM_LIMIT = 60 * 1024 * 1024
-
-
-def dispatch_kernel(ids_ref, tok_ref, out_ref, pos_ref, tiles_ref, count_ref, *, capacity):
+DISPATCH_VMEM = 60 * 1024 * 1024
+EXPERT_VMEM = 40 * 1024 * 1024
+COMBINE_VMEM = 8 * 1024 * 1024
+
+
+def dispatch_kernel(ids_ref, tok_ref, out_ref, pos_ref, tiles_ref, next_ref, *, capacity):
     tok_dev, half = tok_ref.shape
     sub = half // LANES
     top = ids_ref.shape[0]
@@ -21,19 +23,15 @@
         block = tok_ref[:, j * LANES : (j + 1) * LANES].astype(jnp.float32)
         tiles_ref[pl.ds(j, tok_dev, stride=sub), :] = block
 
-    def clear(e, carry):
-        count_ref[e] = 0
-        return carry
-
-    lax.fori_loop(0, count_ref.shape[0], clear, 0)
+    for e in range(next_ref.shape[0]):
+        next_ref[e] = e * capacity
 
     def place(t, carry):
         row = tiles_ref[pl.ds(pl.multiple_of(t * sub, sub), sub), :].astype(jnp.bfloat16)
         for k in range(top):
             e = ids_ref[k, t]
-            rank = count_ref[e]
-            count_ref[e] = rank + 1
-            slot = e * capacity + rank
+            slot = next_ref[e]
+            next_ref[e] = slot + 1
             pos_ref[k, t] = slot
             out_ref[slot] = row
         return carry
@@ -62,14 +60,15 @@
             pltpu.VMEM((tok_dev * sub, LANES), jnp.float32),
             pltpu.SMEM((experts,), jnp.int32),
         ],
-        compiler_params=pltpu.CompilerParams(vmem_limit_bytes=VMEM_LIMIT),
+        compiler_params=pltpu.CompilerParams(vmem_limit_bytes=DISPATCH_VMEM),
         name="dispatch",
     )(ids, tokens)
 
 
 def expert_kernel(
     arr_ref, gain_ref, wg0, wg1, wu0, wu1, wd0, wd1, out_ref,
-    tiles_ref, x_ref, hid_ref, wg_ref, wu_ref, wd_ref, sems, *, n_tp, per_part, width,
+    tiles_ref, x_ref, hid_ref, wg_ref, wu_ref, wd_ref, rows_ref, sems, out_sems,
+    *, n_tp, per_part, width,
 ):
     rows = x_ref.shape[0]
     sub = arr_ref.shape[1]
@@ -77,7 +76,7 @@
     sources = rows // per_part
     copies = []
     for i, (src, dst) in enumerate(
-        ((wg0, wg_ref.at[0]), (wg1, wg_ref.at[1]), (wu0, wu_ref.at[0]), (wu1, wu_ref.at[1]),
+        ((wg0, wg_ref.at[0]), (wu0, wu_ref.at[0]), (wg1, wg_ref.at[1]), (wu1, wu_ref.at[1]),
          (wd0, wd_ref.at[0]), (wd1, wd_ref.at[1]))
     ):
         copy = pltpu.make_async_copy(src.at[0], dst, sems.at[i])
@@ -91,7 +90,7 @@
             tiles_ref[c, pl.ds(at, per_part * sub), :] = part.reshape(per_part * sub, LANES)
         return carry
 
-    lax.fori_loop(0, sources, spread, 0, unroll=4)
+    lax.fori_loop(0, sources, spread, 0, unroll=8)
 
     block = 80
 
@@ -118,8 +117,8 @@
     ff = wg_ref.shape[2]
     step = 256
     for h in range(n_tp):
-        copies[h].wait()
-        copies[n_tp + h].wait()
+        copies[2 * h].wait()
+        copies[2 * h + 1].wait()
         for n in range(ff // step):
             cols = slice(n * step, (n + 1) * step)
             gate = jnp.dot(x_ref[...], wg_ref[h, :, cols], preferred_element_type=jnp.float32)
@@ -128,6 +127,7 @@
             hid_ref[:, h * ff + n * step : h * ff + (n + 1) * step] = hidden.astype(jnp.bfloat16)
     for h in range(n_tp):
         copies[2 * n_tp + h].wait()
+    sends = []
     for c in range(n_tp):
         for n in range(half // step):
             lo = c * half + n * step
@@ -140,27 +140,38 @@
                 j = n * (step // LANES) + i
                 tiles_ref[c, pl.ds(j, rows, stride=sub), :] = total[:, i * LANES : (i + 1) * LANES]
 
-    def gather(s, carry):
-        for c in range(n_tp):
+        def gather(s, carry):
             at = pl.multiple_of(s * (per_part * sub), per_part * sub)
             part = tiles_ref[c, pl.ds(at, per_part * sub), :].reshape(per_part, sub, LANES)
-            out_ref[pl.ds((s * n_tp + c) * per_part, per_part)] = part.astype(jnp.bfloat16)
-        return carry
-
-    lax.fori_loop(0, sources, gather, 0, unroll=4)
+            rows_ref[c, s] = part.astype(jnp.bfloat16)
+            return carry
+
+        lax.fori_loop(0, sources, gather, 0, unroll=8)
+        sends.append(pltpu.make_async_copy(rows_ref.at[c], out_ref.at[:, c], out_sems.at[c]))
+        sends[c].start()
+    for send in sends:
+        send.wait()
+
+
+def in_vmem(x):
+    return pltpu.with_memory_space_constraint(x, pltpu.VMEM)
+
+
+def in_hbm(x):
+    return pltpu.with_memory_space_constraint(x, pltpu.HBM)
 
 
 def expert(arrived, gain, gates, uppers, downs, per_part, n_tp):
     total, sub, lanes = arrived.shape
     rows = total // n_tp
     _, width, ff = gates[0].shape
-    anywhere = pl.BlockSpec(memory_space=pl.ANY)
+    anywhere = pl.BlockSpec(memory_space=pltpu.HBM)
     return pl.pallas_call(
         functools.partial(expert_kernel, n_tp=n_tp, per_part=per_part, width=width),
-        out_shape=jax.ShapeDtypeStruct(arrived.shape, jnp.bfloat16),
+        out_shape=pltpu.HBM((rows // per_part, n_tp, per_part, sub, lanes), jnp.bfloat16),
         in_specs=[pl.BlockSpec(memory_space=pltpu.VMEM), pl.BlockSpec(memory_space=pltpu.VMEM)]
         + [anywhere] * (3 * n_tp),
-        out_specs=pl.BlockSpec(memory_space=pltpu.VMEM),
+        out_specs=pl.BlockSpec(memory_space=pltpu.HBM),
         scratch_shapes=[
             pltpu.VMEM((n_tp, rows * sub, lanes), jnp.float32),
             pltpu.VMEM((rows, width), jnp.bfloat16),
@@ -168,15 +179,17 @@
             pltpu.VMEM((n_tp, width, ff), jnp.bfloat16),
             pltpu.VMEM((n_tp, width, ff), jnp.bfloat16),
             pltpu.VMEM((n_tp, ff, width), jnp.bfloat16),
+            pltpu.VMEM((n_tp, rows // per_part, per_part, sub, lanes), jnp.bfloat16),
             pltpu.SemaphoreType.DMA((3 * n_tp,)),
+            pltpu.SemaphoreType.DMA((n_tp,)),
         ],
-        compiler_params=pltpu.CompilerParams(vmem_limit_bytes=VMEM_LIMIT),
+        compiler_params=pltpu.CompilerParams(vmem_limit_bytes=EXPERT_VMEM),
         cost_estimate=pl.CostEstimate(
             flops=6 * rows * width * ff * n_tp, transcendentals=rows * ff * n_tp,
             bytes_accessed=12 * width * ff + 4 * total * sub * lanes,
         ),
         name="expert",
-    )(arrived, gain, *gates, *uppers, *downs)
+    )(in_vmem(arrived), gain, *[in_hbm(w) for w in (*gates, *uppers, *downs)])
 
 
 def combine_kernel(pos_ref, mix_ref, ret_ref, out_ref, sq_ref, tiles_ref):
@@ -205,7 +218,7 @@
     return pl.pallas_call(
         combine_kernel,
         out_shape=(
-            jax.ShapeDtypeStruct((tok_dev, sub * lanes), jnp.float32),
+            pltpu.VMEM((tok_dev, sub * lanes), jnp.float32),
             jax.ShapeDtypeStruct((tok_dev, 1), jnp.float32),
         ),
         in_specs=[
@@ -218,9 +231,26 @@
             pl.BlockSpec(memory_space=pltpu.VMEM),
         ),
         scratch_shapes=[pltpu.VMEM((tok_dev * sub, lanes), jnp.float32)],
-        compiler_params=pltpu.CompilerParams(vmem_limit_bytes=VMEM_LIMIT),
+        compiler_params=pltpu.CompilerParams(vmem_limit_bytes=COMBINE_VMEM),
         name="combine",
-    )(pos, mix, returned)
+    )(pos, mix, in_vmem(returned))
+
+
+def finish_kernel(mix_ref, tot_ref, gain_ref, out_ref, *, width):
+    totals = jnp.sum(tot_ref[...], axis=0)
+    norm = lax.rsqrt(totals / width + EPS)
+    out_ref[...] = (mix_ref[...] * norm * gain_ref[...].astype(jnp.float32)).astype(jnp.bfloat16)
+
+
+def finished(mixed, totals, gain, width):
+    return pl.pallas_call(
+        functools.partial(finish_kernel, width=width),
+        out_shape=jax.ShapeDtypeStruct(mixed.shape, jnp.bfloat16),
+        in_specs=[pl.BlockSpec(memory_space=pltpu.VMEM)] * 3,
+        out_specs=pl.BlockSpec(memory_space=pltpu.VMEM),
+        compiler_params=pltpu.CompilerParams(vmem_limit_bytes=COMBINE_VMEM),
+        name="finish",
+    )(in_vmem(mixed), totals, gain[None, :])
 
 
 def body(tokens, norm_gain, w_gate, w_up, w_down, expert_ids, combine, final_gain):
@@ -250,9 +280,8 @@
         results.reshape(shape), ("ep", "tp"), split_axis=0, concat_axis=0, tiled=True
     )
     mixed, squares = combined(pos, combine.T, returned.reshape(-1, sub, LANES))
-    totals = lax.all_gather(squares[:, 0], "tp").sum(axis=0)
-    norm = lax.rsqrt(totals[:, None] / width + EPS)
-    return (mixed * norm * final_gain.astype(jnp.float32)).astype(jnp.bfloat16)
+    totals = lax.all_gather(squares, "tp")
+    return finished(mixed, totals, final_gain, width)
 
 
 def solution(mesh):

time: 315 us -> 305 us (0.968)
  Pallas kernels: 25.4 us -> 21.1 us
where the time goes in v2:
time: 305 us; the launch traced here: 304 us
  waiting for transfers between devices  221 us (72%)
  starting transfers between devices  46.4 us (15%)
  Pallas kernels  21.1 us (7%)
  blocking collectives  13.3 us (4%)
    all_to_all x1, waiting for transfers between devices, body(): lax.all_to_all(results.reshape(shape), ('ep', 'tp'), split_axis=0, concat...  118 us
    all_to_all x1, waiting for transfers between devices, body(): lax.all_to_all(outgoing.reshape(shape), ('ep', 'tp'), split_axis=0, conca...  103 us
    all_to_all x1, starting transfers between devices, body(): lax.all_to_all(outgoing.reshape(shape), ('ep', 'tp'), split_axis=0, conca...  31 us
    pallas_call x1, Pallas kernels, expert(): pl.pallas_call(functools.partial(expert_kernel, n_tp=n_tp, per_part=per_p...  12.8 us
    all_to_all x1, starting transfers between devices, body(): lax.all_to_all(results.reshape(shape), ('ep', 'tp'), split_axis=0, concat...  12.2 us
    all_gather x1, blocking collectives, body(): lax.all_gather(norm_gain.astype(jnp.float32), 'tp', tiled=True)[None, :]  9.61 us
  transfers between devices with their start and end apart: 5, of which 2 were waited for; matrix products, arithmetic and copies ran while one was open for 0% of the time, Pallas kernels for 0%

profile of v2, /device:TPU:33, one launch (start us, length us, event | category | flops | bytes accessed | tf_op | source)
XLA Modules:
  0.0 304.4 jit_solution(7494167119634185310)
XLA Ops:
  0.0 5.2 %dispatch.1 = (bf16[1280,8,128]{2,1,0:T(8,128)(2,1)}, s32[2,256]{1,0:T(2,128)}) custom-call(s32[2,256]{1,0:T(2,128)} %bitcast.15, bf16[256,1024]{1,0:T(8,128)(2,1)} %tok_ref.1), custom_call_target="tpu_custom_call" | custom-call | tf_op jit(solution)/shard_map/dispatch/pallas_call | solution.py:45
  5.2 0.0 copy-start.2
  5.2 31.0 %all-to-all-start = ((bf16[128,10,8,128]{3,2,1,0:T(8,128)(2,1)}), bf16[128,10,8,128]{3,2,1,0:T(8,128)(2,1)S(1)}, u32[]{:S(2)}, u32[]{:S(2)}) async-start(bf16[128,10,8,128]{3,2,1,0:T(8,128)(2,1)} %bitcast.13), calls=%async_computation | async-start | bytes 5242880 | tf_op jit(solution)/shard_map/all_to_all | solution.py:272
  36.2 2.7 collective-permute-start
  38.9 0.2 collective-permute-start.1
  39.0 0.4 collective-permute-start.2
  39.4 0.0 copy-done.2
  39.4 9.6 %all_gather.9 = f32[2048]{0:T(1024)S(1)} all-gather(f32[1024]{0:T(1024)S(1)} %convert_element_type.3), channel_id=1, replica_groups=mesh['grp'=2,'ep'=64,'tp'=2] {'tp'}, dimensions={0}, use_global_device_ids=true | all-gather | bytes 12288 | tf_op jit(solution)/shard_map/all_gather | solution.py:268
  49.0 0.0 collective-permute-done.wg1
  49.0 0.0 copy-start.4
  49.0 0.0 collective-permute-done.1.wu1
  49.0 1.3 copy-done.4
  50.4 0.0 copy-start.5
  50.4 1.4 copy-done.5
  51.7 0.0 collective-permute-done.2.wd1
  51.7 102.6 %all-to-all-done = bf16[128,10,8,128]{3,2,1,0:T(8,128)(2,1)S(1)} async-done(((bf16[128,10,8,128]{3,2,1,0:T(8,128)(2,1)}), bf16[128,10,8,128]{3,2,1,0:T(8,128)(2,1)S(1)}, u32[]{:S(2)}, u32[]{:S(2)}) %all-to-all-start) | async-done | bytes 2621472 | tf_op jit(solution)/shard_map/all_to_all | solution.py:272
  154.4 12.8 %expert.1 = bf16[64,2,10,8,128]{4,3,2,1,0:T(8,128)(2,1)} custom-call(bf16[1280,8,128]{2,1,0:T(8,128)(2,1)S(1)} %bitcast.9, f32[1,2048]{1,0:T(1,128)S(1)} %bitcast.11, bf16[1,2048,512]{2,1,0:T(8,128)(2,1)} %wg0.1, bf16[1,2048,512]{2,1,0:T(8,128)(2,1)} %copy-done.4, bf16[1,2048,512]{2,1,0:T(8,128)(2,1)} %wu0.1, bf16[1,2048,512]{2,1,0:T(8,128)(2,1)} %copy-done.5, ...), custom_call_target="tpu_custom_call" | custom-call | flops 8053063680 | bytes 17825792 | tf_op jit(solution)/shard_map/expert/pallas_call | solution.py:169
  167.2 0.0 copy-start.3
  167.2 0.0 copy-start
  167.2 0.0 copy-start.1
  167.2 12.2 %all-to-all-start.1 = ((bf16[128,10,8,128]{3,2,1,0:T(8,128)(2,1)}), bf16[128,10,8,128]{3,2,1,0:T(8,128)(2,1)S(1)}, u32[]{:S(2)}, u32[]{:S(2)}) async-start(bf16[128,10,8,128]{3,2,1,0:T(8,128)(2,1)} %bitcast.14), calls=%async_computation.1 | async-start | bytes 5242880 | tf_op jit(solution)/shard_map/all_to_all | solution.py:279
  179.4 0.0 copy-done.3
  179.5 118.1 %all-to-all-done.1 = bf16[128,10,8,128]{3,2,1,0:T(8,128)(2,1)S(1)} async-done(((bf16[128,10,8,128]{3,2,1,0:T(8,128)(2,1)}), bf16[128,10,8,128]{3,2,1,0:T(8,128)(2,1)S(1)}, u32[]{:S(2)}, u32[]{:S(2)}) %all-to-all-start.1) | async-done | bytes 2621472 | tf_op jit(solution)/shard_map/all_to_all | solution.py:279
  297.6 0.0 copy-done
  297.6 0.0 copy-done.1
  297.6 2.1 combine.1
  299.7 3.7 %all-gather = f32[512,1]{1,0:T(8,128)S(1)} all-gather(f32[256,1]{1,0:T(8,128)S(1)} %get-tuple-element.12), channel_id=2, replica_groups=mesh['grp'=2,'ep'=64,'tp'=2] {'tp'}, dimensions={0}, use_global_device_ids=true | all-gather | bytes 3072 | tf_op jit(solution)/shard_map/all_gather | solution.py:283
  303.5 1.0 finish.1
  (2 shorter events, 0.0 us)
Async XLA Ops:
  5.2 34.2 %copy-start.2 = (bf16[1024]{0:T(1024)(128)(2,1)S(1)}, bf16[1024]{0:T(1024)(128)(2,1)}, u32[]{:S(2)}) copy-start(bf16[1024]{0:T(1024)(128)(2,1)} %param.9) | copy-start | bytes 6148
  5.2 149.2 %all-to-all-start = ((bf16[128,10,8,128]{3,2,1,0:T(8,128)(2,1)}), bf16[128,10,8,128]{3,2,1,0:T(8,128)(2,1)S(1)}, u32[]{:S(2)}, u32[]{:S(2)}) async-start(bf16[128,10,8,128]{3,2,1,0:T(8,128)(2,1)} %bitcast.13), calls=%async_computation | async-start | bytes 5242880 | tf_op jit(solution)/shard_map/all_to_all | solution.py:272
  36.2 12.8 %collective-permute-start = (bf16[1,2048,512]{2,1,0:T(8,128)(2,1)}, bf16[1,2048,512]{2,1,0:T(8,128)(2,1)S(1)}, u32[]{:S(2)}, u32[]{:S(2)}) collective-permute-start(bf16[1,2048,512]{2,1,0:T(8,128)(2,1)} %wg0.1), channel_id=1, source_target_pairs={{0,1},{1,0},{2,3},{3,2},{4,5},{5,4},{6,7},{7,6},{8,9},{9,8},{10,11... | collective-permute-start | bytes 6291464 | tf_op jit(solution)/shard_map/ppermute | solution.py:267
  38.9 10.1 %collective-permute-start.1 = (bf16[1,2048,512]{2,1,0:T(8,128)(2,1)}, bf16[1,2048,512]{2,1,0:T(8,128)(2,1)S(1)}, u32[]{:S(2)}, u32[]{:S(2)}) collective-permute-start(bf16[1,2048,512]{2,1,0:T(8,128)(2,1)} %wu0.1), channel_id=1, source_target_pairs={{0,1},{1,0},{2,3},{3,2},{4,5},{5,4},{6,7},{7,6},{8,9},{9,8},{10,11... | collective-permute-start | bytes 6291464 | tf_op jit(solution)/shard_map/ppermute | solution.py:267
  39.0 12.7 %collective-permute-start.2 = (bf16[1,512,2048]{2,1,0:T(8,128)(2,1)}, bf16[1,512,2048]{2,1,0:T(8,128)(2,1)}, u32[]{:S(2)}, u32[]{:S(2)}) collective-permute-start(bf16[1,512,2048]{2,1,0:T(8,128)(2,1)} %wd0.1), channel_id=1, source_target_pairs={{0,1},{1,0},{2,3},{3,2},{4,5},{5,4},{6,7},{7,6},{8,9},{9,8},{10,11... | collective-permute-start | bytes 6291464 | tf_op jit(solution)/shard_map/ppermute | solution.py:267
  49.0 1.3 copy-start.4
  50.4 1.4 copy-start.5
  167.2 12.3 %copy-start.3 = (bf16[1024]{0:T(1024)(128)(2,1)S(1)}, bf16[1024]{0:T(1024)(128)(2,1)}, u32[]{:S(2)}) copy-start(bf16[1024]{0:T(1024)(128)(2,1)} %param.15) | copy-start | bytes 6148
  167.2 130.4 %copy-start = (f32[256,2]{0,1:T(2,128)S(1)}, f32[256,2]{0,1:T(2,128)}, u32[]{:S(2)}) copy-start(f32[256,2]{0,1:T(2,128)} %param.14) | copy-start | bytes 6148
  167.2 130.4 %copy-start.1 = (s32[2,256]{1,0:T(2,128)S(1)}, s32[2,256]{1,0:T(2,128)}, u32[]{:S(2)}) copy-start(s32[2,256]{1,0:T(2,128)} %get-tuple-element.9.pos_ref) | copy-start | bytes 6148
  167.2 130.4 %all-to-all-start.1 = ((bf16[128,10,8,128]{3,2,1,0:T(8,128)(2,1)}), bf16[128,10,8,128]{3,2,1,0:T(8,128)(2,1)S(1)}, u32[]{:S(2)}, u32[]{:S(2)}) async-start(bf16[128,10,8,128]{3,2,1,0:T(8,128)(2,1)} %bitcast.14), calls=%async_computation.1 | async-start | bytes 5242880 | tf_op jit(solution)/shard_map/all_to_all | solution.py:279

commit v3 on v2

--- a/solution.py
+++ b/solution.py
@@ -5,9 +5,13 @@
 from jax import lax
 from jax.experimental import pallas as pl
 from jax.experimental.pallas import tpu as pltpu
+from jax.sharding import Mesh
 from jax.sharding import PartitionSpec as P
 
+
 GROUPS = 4
+ROW = 4
+NEAR = 10
 EPS = 1e-06
 LANES = 128
 DISPATCH_VMEM = 60 * 1024 * 1024
@@ -15,16 +19,27 @@
 COMBINE_VMEM = 8 * 1024 * 1024
 
 
-def dispatch_kernel(ids_ref, tok_ref, out_ref, pos_ref, tiles_ref, next_ref, *, capacity):
+def offsets(n_z):
+    return [(i + 1) // 2 if i % 2 else -(i // 2) for i in range(n_z)]
+
+
+def dispatch_kernel(z_ref, ids_ref, tok_ref, *refs, capacity):
+    *out_refs, pos_ref, tiles_ref, rows_ref, next_ref, sems = refs
     tok_dev, half = tok_ref.shape
     sub = half // LANES
     top = ids_ref.shape[0]
+    n_z = len(out_refs)
+    block = ROW * capacity
     for j in range(sub):
-        block = tok_ref[:, j * LANES : (j + 1) * LANES].astype(jnp.float32)
-        tiles_ref[pl.ds(j, tok_dev, stride=sub), :] = block
-
-    for e in range(next_ref.shape[0]):
-        next_ref[e] = e * capacity
+        part = tok_ref[:, j * LANES : (j + 1) * LANES].astype(jnp.float32)
+        tiles_ref[pl.ds(j, tok_dev, stride=sub), :] = part
+    z = z_ref[0]
+    for row in range(n_z):
+        away = row - z
+        away = jnp.where(away < 0, away + n_z, away)
+        place_in = jnp.where(away * 2 > n_z, 2 * (n_z - away), jnp.maximum(2 * away - 1, 0))
+        for x in range(ROW):
+            next_ref[row * ROW + x] = place_in * block + x * capacity
 
     def place(t, carry):
         row = tiles_ref[pl.ds(pl.multiple_of(t * sub, sub), sub), :].astype(jnp.bfloat16)
@@ -33,36 +48,46 @@
             slot = next_ref[e]
             next_ref[e] = slot + 1
             pos_ref[k, t] = slot
-            out_ref[slot] = row
+            rows_ref[slot] = row
         return carry
 
     lax.fori_loop(0, tok_dev, place, 0, unroll=8)
-
-
-def dispatch(ids, tokens, experts, capacity):
+    copies = []
+    for i, out_ref in enumerate(out_refs):
+        part = rows_ref.at[pl.ds(i * block, block)]
+        copies.append(pltpu.make_async_copy(part, out_ref, sems.at[i]))
+    for copy in copies:
+        copy.start()
+    for copy in copies:
+        copy.wait()
+
+
+def dispatch(z, ids, tokens, experts, capacity):
     tok_dev, half = tokens.shape
     sub = half // LANES
+    n_z = experts // ROW
     return pl.pallas_call(
         functools.partial(dispatch_kernel, capacity=capacity),
-        out_shape=(
-            jax.ShapeDtypeStruct((experts * capacity, sub, LANES), jnp.bfloat16),
-            jax.ShapeDtypeStruct(ids.shape, jnp.int32),
-        ),
+        out_shape=tuple(
+            pltpu.HBM((ROW * capacity, sub, LANES), jnp.bfloat16) for _ in range(n_z)
+        )
+        + (jax.ShapeDtypeStruct(ids.shape, jnp.int32),),
         in_specs=[
+            pl.BlockSpec(memory_space=pltpu.SMEM),
             pl.BlockSpec(memory_space=pltpu.SMEM),
             pl.BlockSpec(memory_space=pltpu.VMEM),
         ],
-        out_specs=(
-            pl.BlockSpec(memory_space=pltpu.VMEM),
-            pl.BlockSpec(memory_space=pltpu.SMEM),
-        ),
+        out_specs=tuple(pl.BlockSpec(memory_space=pltpu.HBM) for _ in range(n_z))
+        + (pl.BlockSpec(memory_space=pltpu.SMEM),),
         scratch_shapes=[
             pltpu.VMEM((tok_dev * sub, LANES), jnp.float32),
+            pltpu.VMEM((experts * capacity, sub, LANES), jnp.bfloat16),
             pltpu.SMEM((experts,), jnp.int32),
+            pltpu.SemaphoreType.DMA((n_z,)),
         ],
         compiler_params=pltpu.CompilerParams(vmem_limit_bytes=DISPATCH_VMEM),
         name="dispatch",
-    )(ids, tokens)
+    )(z, ids, tokens)
 
 
 def expert_kernel(
@@ -83,14 +108,18 @@
         copy.start()
         copies.append(copy)
 
-    def spread(s, carry):
+    unit = 20
+    pieces = per_part // unit
+
+    def spread(i, carry):
+        s, p = i // pieces, i % pieces
         for c in range(n_tp):
-            part = arr_ref[pl.ds((s * n_tp + c) * per_part, per_part)].astype(jnp.float32)
-            at = pl.multiple_of(s * (per_part * sub), per_part * sub)
-            tiles_ref[c, pl.ds(at, per_part * sub), :] = part.reshape(per_part * sub, LANES)
+            part = arr_ref[pl.ds((s * n_tp + c) * per_part + p * unit, unit)].astype(jnp.float32)
+            at = pl.multiple_of(i * (unit * sub), unit * sub)
+            tiles_ref[c, pl.ds(at, unit * sub), :] = part.reshape(unit * sub, LANES)
         return carry
 
-    lax.fori_loop(0, sources, spread, 0, unroll=8)
+    lax.fori_loop(0, sources * pieces, spread, 0)
 
     block = 80
 
@@ -140,13 +169,14 @@
                 j = n * (step // LANES) + i
                 tiles_ref[c, pl.ds(j, rows, stride=sub), :] = total[:, i * LANES : (i + 1) * LANES]
 
-        def gather(s, carry):
-            at = pl.multiple_of(s * (per_part * sub), per_part * sub)
-            part = tiles_ref[c, pl.ds(at, per_part * sub), :].reshape(per_part, sub, LANES)
-            rows_ref[c, s] = part.astype(jnp.bfloat16)
+        def gather(i, carry):
+            s, p = i // pieces, i % pieces
+            at = pl.multiple_of(i * (unit * sub), unit * sub)
+            part = tiles_ref[c, pl.ds(at, unit * sub), :].reshape(unit, sub, LANES)
+            rows_ref[c, s, pl.ds(p * unit, unit)] = part.astype(jnp.bfloat16)
             return carry
 
-        lax.fori_loop(0, sources, gather, 0, unroll=8)
+        lax.fori_loop(0, sources * pieces, gather, 0)
         sends.append(pltpu.make_async_copy(rows_ref.at[c], out_ref.at[:, c], out_sems.at[c]))
         sends[c].start()
     for send in sends:
@@ -192,9 +222,19 @@
     )(in_vmem(arrived), gain, *[in_hbm(w) for w in (*gates, *uppers, *downs)])
 
 
-def combine_kernel(pos_ref, mix_ref, ret_ref, out_ref, sq_ref, tiles_ref):
+def combine_kernel(pos_ref, mix_ref, *refs):
+    *parts, out_ref, sq_ref, ret_ref, tiles_ref, sems = refs
     top, tok_dev = pos_ref.shape
     sub = ret_ref.shape[1]
+    block = parts[0].shape[0]
+    copies = []
+    for i, part in enumerate(parts):
+        into = ret_ref.at[pl.ds(i * block, block)]
+        copies.append(pltpu.make_async_copy(part, into, sems.at[i]))
+    for copy in copies:
+        copy.start()
+    for copy in copies:
+        copy.wait()
 
     def pick(t, carry):
         total = mix_ref[0, t] * ret_ref[pos_ref[0, t]].astype(jnp.float32)
@@ -214,7 +254,7 @@
 
 def combined(pos, mix, returned):
     _, tok_dev = pos.shape
-    _, sub, lanes = returned.shape
+    block, sub, lanes = returned[0].shape
     return pl.pallas_call(
         combine_kernel,
         out_shape=(
@@ -224,16 +264,20 @@
         in_specs=[
             pl.BlockSpec(memory_space=pltpu.SMEM),
             pl.BlockSpec(memory_space=pltpu.SMEM),
-            pl.BlockSpec(memory_space=pltpu.VMEM),
-        ],
+        ]
+        + [pl.BlockSpec(memory_space=pl.ANY)] * len(returned),
         out_specs=(
             pl.BlockSpec(memory_space=pltpu.VMEM),
             pl.BlockSpec(memory_space=pltpu.VMEM),
         ),
-        scratch_shapes=[pltpu.VMEM((tok_dev * sub, lanes), jnp.float32)],
+        scratch_shapes=[
+            pltpu.VMEM((len(returned) * block, sub, lanes), jnp.bfloat16),
+            pltpu.VMEM((tok_dev * sub, lanes), jnp.float32),
+            pltpu.SemaphoreType.DMA((len(returned),)),
+        ],
         compiler_params=pltpu.CompilerParams(vmem_limit_bytes=COMBINE_VMEM),
         name="combine",
-    )(pos, mix, in_vmem(returned))
+    )(pos, mix, *returned)
 
 
 def finish_kernel(mix_ref, tot_ref, gain_ref, out_ref, *, width):
@@ -255,46 +299,63 @@
 
 def body(tokens, norm_gain, w_gate, w_up, w_down, expert_ids, combine, final_gain):
     tok_dev, half = tokens.shape
-    n_ep = lax.axis_size("ep")
+    n_z = lax.axis_size("z")
     n_tp = lax.axis_size("tp")
     width = half * n_tp
-    experts = w_gate.shape[0] * n_ep
+    experts = w_gate.shape[0] * n_z * ROW
     capacity = tok_dev // 8 * 5 * 2 // (experts // GROUPS)
-    per_part = capacity // n_tp
+    per_core = capacity // n_tp
     sub = half // LANES
+    away = offsets(n_z)
+    chunks = (range(NEAR), range(NEAR, n_z))
+
+    def shift(x, by):
+        if by % n_z == 0:
+            return x
+        return lax.ppermute(x, "z", [(i, (i + by) % n_z) for i in range(n_z)])
+
+    def exchange(x):
+        return lax.all_to_all(x, ("x", "tp"), split_axis=0, concat_axis=0, tiled=True)
 
     swap = [(i, (i + 1) % n_tp) for i in range(n_tp)]
-    others = [lax.ppermute(w, "tp", swap) for w in (w_gate, w_up, w_down)]
+    others = []
+    for w in (w_gate, w_up, w_down):
+        others.append(lax.ppermute(w, "tp", swap))
     gain = lax.all_gather(norm_gain.astype(jnp.float32), "tp", tiled=True)[None, :]
-
-    outgoing, pos = dispatch(expert_ids.T, tokens, experts, capacity)
-    shape = (n_ep * n_tp, per_part, sub, LANES)
-    arrived = lax.all_to_all(
-        outgoing.reshape(shape), ("ep", "tp"), split_axis=0, concat_axis=0, tiled=True
-    )
-    results = expert(
-        arrived.reshape(-1, sub, LANES), gain, (w_gate, others[0]), (w_up, others[1]),
-        (w_down, others[2]), per_part, n_tp,
-    )
-    returned = lax.all_to_all(
-        results.reshape(shape), ("ep", "tp"), split_axis=0, concat_axis=0, tiled=True
-    )
-    mixed, squares = combined(pos, combine.T, returned.reshape(-1, sub, LANES))
+    z = lax.axis_index("z").astype(jnp.int32).reshape(1)
+    *outgoing, pos = dispatch(z, expert_ids.T, tokens, experts, capacity)
+    came = [shift(x, by) for x, by in zip(outgoing, away)]
+    returned = []
+    for chunk in chunks:
+        parts = [came[i].reshape(ROW * n_tp, per_core, sub, LANES) for i in chunk]
+        arrived = exchange(jnp.stack(parts, axis=1))
+        results = expert(
+            arrived.reshape(-1, sub, LANES), gain, (w_gate, others[0]),
+            (w_up, others[1]), (w_down, others[2]), per_core * len(chunk), n_tp,
+        )
+        back = exchange(results.reshape(arrived.shape))
+        for k, i in enumerate(chunk):
+            part = back[:, k].reshape(ROW * capacity, sub, LANES)
+            returned.append(shift(part, -away[i]))
+    mixed, squares = combined(pos, combine.T, returned)
     totals = lax.all_gather(squares, "tp")
     return finished(mixed, totals, final_gain, width)
 
 
 def solution(mesh):
+    grp, ep, tp = mesh.devices.shape
+    fine = Mesh(mesh.devices.reshape(grp, ep // ROW, ROW, tp), ("grp", "z", "x", "tp"))
+    spot = ("z", "x")
     placed = (
-        P(("grp", "ep"), "tp"),
+        P(("grp", "z", "x"), "tp"),
         P("tp"),
-        P("ep", None, "tp"),
-        P("ep", None, "tp"),
-        P("ep", "tp", None),
-        P(("grp", "ep"), None),
-        P(("grp", "ep"), None),
+        P(spot, None, "tp"),
+        P(spot, None, "tp"),
+        P(spot, "tp", None),
+        P(("grp", "z", "x"), None),
+        P(("grp", "z", "x"), None),
         P("tp"),
     )
     return jax.shard_map(
-        body, mesh=mesh, in_specs=placed, out_specs=P(("grp", "ep"), "tp"), check_vma=False
+        body, mesh=fine, in_specs=placed, out_specs=P(("grp", "z", "x"), "tp"), check_vma=False
     )

time: 305 us -> 370 us (1.21)
  starting transfers between devices: 46.4 us -> 178 us
  waiting for transfers between devices: 221 us -> 148 us
  blocking collectives: 13.3 us -> 4.29 us
  Pallas kernels: 21.1 us -> 29.7 us
  local copies, waits for them, and re-layouts: 2.73 us -> 9.16 us
    all_to_all x2 -> x4, waiting for transfers between devices: 221 us -> 16.6 us  [exchange(): lax.all_to_all(x, ('x', 'tp'), split_axis=0, concat_axis=0, tiled=True)]
    ppermute x3 -> x33, starting transfers between devices: 3.21 us -> 154 us  [the longest x30 150 us: shift(): return lax.ppermute(x, 'z', [(i, (i + by) % n_z) for i in range(n_z)])]
    ppermute x3 -> x33, waiting for transfers between devices: 0.01 us -> 131 us  [the longest x30 131 us: shift(): return lax.ppermute(x, 'z', [(i, (i + by) % n_z) for i in range(n_z)])]
    all_to_all x2 -> x4, starting transfers between devices: 43.2 us -> 23.7 us  [exchange(): lax.all_to_all(x, ('x', 'tp'), split_axis=0, concat_axis=0, tiled=True)]
    all_gather x1, blocking collectives: 9.61 us -> 1.87 us  [body(): lax.all_gather(norm_gain.astype(jnp.float32), 'tp', tiled=True)[None, :]]
    pallas_call x1 -> x2, Pallas kernels: 12.8 us -> 17.1 us  [expert(): pl.pallas_call(functools.partial(expert_kernel, n_tp=n_tp, per_part=per_p...]
    unnamed x12 -> x30, local copies, waits for them, and re-layouts: 2.72 us -> 6.91 us
  transfers between devices with their start and end apart: 5 -> 37, of which waited for: 2 -> 15; matrix products, arithmetic and copies ran while one was open for 0% -> 2% of each run, Pallas kernels for 0% -> 5%
where the time goes in v3:
time: 370 us; the launch traced here: 369 us
  starting transfers between devices  178 us (48%)
  waiting for transfers between devices  148 us (40%)
  Pallas kernels  29.7 us (8%)
  local copies, waits for them, and re-layouts  9.16 us (2%)
  blocking collectives  4.29 us (1%)
    ppermute x30, starting transfers between devices, shift(): return lax.ppermute(x, 'z', [(i, (i + by) % n_z) for i in range(n_z)])  150 us
    ppermute x30, waiting for transfers between devices, shift(): return lax.ppermute(x, 'z', [(i, (i + by) % n_z) for i in range(n_z)])  131 us
    all_to_all x4, starting transfers between devices, exchange(): lax.all_to_all(x, ('x', 'tp'), split_axis=0, concat_axis=0, tiled=True)  23.7 us
    pallas_call x2, Pallas kernels, expert(): pl.pallas_call(functools.partial(expert_kernel, n_tp=n_tp, per_part=per_p...  17.1 us
    all_to_all x4, waiting for transfers between devices, exchange(): lax.all_to_all(x, ('x', 'tp'), split_axis=0, concat_axis=0, tiled=True)  16.6 us
  transfers between devices with their start and end apart: 37, of which 15 were waited for; matrix products, arithmetic and copies ran while one was open for 2% of the time, Pallas kernels for 5%

profile of v3, /device:TPU:33, one launch (start us, length us, event | category | flops | bytes accessed | tf_op | source)
XLA Modules:
  0.0 368.8 jit_solution(4928064107875805527)
XLA Ops:
  0.0 5.9 %dispatch.1 = (bf16[80,8,128]{2,1,0:T(8,128)(2,1)}, bf16[80,8,128]{2,1,0:T(8,128)(2,1)}, bf16[80,8,128]{2,1,0:T(8,128)(2,1)}, bf16[80,8,128]{2,1,0:T(8,128)(2,1)...) custom-call(s32[1]{0:T(128)} %bitcast.z_ref, ...), custom_call_target="tpu_custom_call" | custom-call | tf_op jit(solution)/shard_map/dispatch/pallas_call | solution.py:69
  5.9 22.6 %collective-permute-start.21 = (bf16[80,8,128]{2,1,0:T(8,128)(2,1)}, bf16[80,8,128]{2,1,0:T(8,128)(2,1)S(1)}, u32[]{:S(2)}, u32[]{:S(2)}) collective-permute-start(bf16[80,8,128]{2,1,0:T(8,128)(2,1)} %get-tuple-element.35), channel_id=1, source_target_pairs={{0,88},{8,96},{16,104},{24,112},{32,120},{40,0},{48,8},{56,16},{64... | collective-permute-start | bytes 491528 | tf_op jit(solution)/shard_map/ppermute | solution.py:315
  28.8 2.3 collective-permute-start.1
  32.7 13.8 %collective-permute-done.21 = bf16[80,8,128]{2,1,0:T(8,128)(2,1)S(1)} collective-permute-done((bf16[80,8,128]{2,1,0:T(8,128)(2,1)}, bf16[80,8,128]{2,1,0:T(8,128)(2,1)S(1)}, u32[]{:S(2)}, u32[]{:S(2)}) %collective-permute-start.21) | collective-permute-done | bytes 163872 | tf_op jit(solution)/shard_map/ppermute | solution.py:315
  47.2 15.3 %collective-permute-done.22 = bf16[80,8,128]{2,1,0:T(8,128)(2,1)S(1)} collective-permute-done((bf16[80,8,128]{2,1,0:T(8,128)(2,1)}, bf16[80,8,128]{2,1,0:T(8,128)(2,1)S(1)}, u32[]{:S(2)}, u32[]{:S(2)}) %collective-permute-start.22) | collective-permute-done | bytes 163872 | tf_op jit(solution)/shard_map/ppermute | solution.py:315
  62.6 3.5 collective-permute-start.24
  67.1 8.8 %collective-permute-start.25 = (bf16[80,8,128]{2,1,0:T(8,128)(2,1)}, bf16[80,8,128]{2,1,0:T(8,128)(2,1)S(1)}, u32[]{:S(2)}, u32[]{:S(2)}) collective-permute-start(bf16[80,8,128]{2,1,0:T(8,128)(2,1)} %get-tuple-element.39), channel_id=1, source_target_pairs={{0,72},{8,80},{16,88},{24,96},{32,104},{40,112},{48,120},{56,0},{6... | collective-permute-start | bytes 491528 | tf_op jit(solution)/shard_map/ppermute | solution.py:315
  76.7 17.0 %collective-permute-done.24 = bf16[80,8,128]{2,1,0:T(8,128)(2,1)S(1)} collective-permute-done((bf16[80,8,128]{2,1,0:T(8,128)(2,1)}, bf16[80,8,128]{2,1,0:T(8,128)(2,1)S(1)}, u32[]{:S(2)}, u32[]{:S(2)}) %collective-permute-start.24) | collective-permute-done | bytes 163872 | tf_op jit(solution)/shard_map/ppermute | solution.py:315
  93.7 2.8 collective-permute-start.26
  97.2 3.3 collective-permute-start.10
  101.2 12.9 %collective-permute-done.26 = bf16[80,8,128]{2,1,0:T(8,128)(2,1)S(1)} collective-permute-done((bf16[80,8,128]{2,1,0:T(8,128)(2,1)}, bf16[80,8,128]{2,1,0:T(8,128)(2,1)S(1)}, u32[]{:S(2)}, u32[]{:S(2)}) %collective-permute-start.26) | collective-permute-done | bytes 163872 | tf_op jit(solution)/shard_map/ppermute | solution.py:315
  115.3 3.8 %all-to-all-start.2 = ((bf16[8,6,10,8,128]{4,3,2,1,0:T(8,128)(2,1)}), bf16[8,6,10,8,128]{4,3,2,1,0:T(8,128)(2,1)S(1)}, u32[]{:S(2)}, u32[]{:S(2)}) async-start(bf16[8,6,10,8,128]{4,3,2,1,0:T(8,128)(2,1)} %constant_dynamic-update-slice_fusion.10), calls=%async_computation.2 | async-start | bytes 1966080 | tf_op jit(solution)/shard_map/all_to_all | solution.py:318
  119.6 9.9 %collective-permute-start.4 = (bf16[80,8,128]{2,1,0:T(8,128)(2,1)}, bf16[80,8,128]{2,1,0:T(8,128)(2,1)S(1)}, u32[]{:S(2)}, u32[]{:S(2)}) collective-permute-start(bf16[80,8,128]{2,1,0:T(8,128)(2,1)} %get-tuple-element.30), channel_id=1, source_target_pairs={{0,24},{8,32},{16,40},{24,48},{32,56},{40,64},{48,72},{56,80},{64,... | collective-permute-start | bytes 491528 | tf_op jit(solution)/shard_map/ppermute | solution.py:315
  129.5 8.3 %collective-permute-start.5 = (bf16[80,8,128]{2,1,0:T(8,128)(2,1)}, bf16[80,8,128]{2,1,0:T(8,128)(2,1)S(1)}, u32[]{:S(2)}, u32[]{:S(2)}) collective-permute-start(bf16[80,8,128]{2,1,0:T(8,128)(2,1)} %get-tuple-element.31), channel_id=1, source_target_pairs={{0,104},{8,112},{16,120},{24,0},{32,8},{40,16},{48,24},{56,32},{64... | collective-permute-start | bytes 491528 | tf_op jit(solution)/shard_map/ppermute | solution.py:315
  137.9 8.9 %collective-permute-start.6 = (bf16[80,8,128]{2,1,0:T(8,128)(2,1)}, bf16[80,8,128]{2,1,0:T(8,128)(2,1)S(1)}, u32[]{:S(2)}, u32[]{:S(2)}) collective-permute-start(bf16[80,8,128]{2,1,0:T(8,128)(2,1)} %get-tuple-element.32), channel_id=1, source_target_pairs={{0,32},{8,40},{16,48},{24,56},{32,64},{40,72},{48,80},{56,88},{64,... | collective-permute-start | bytes 491528 | tf_op jit(solution)/shard_map/ppermute | solution.py:315
  146.8 7.2 %collective-permute-start.7 = (bf16[80,8,128]{2,1,0:T(8,128)(2,1)S(1)}, bf16[80,8,128]{2,1,0:T(8,128)(2,1)S(1)}, u32[]{:S(2)}, u32[]{:S(2)}) collective-permute-start(bf16[80,8,128]{2,1,0:T(8,128)(2,1)S(1)} %copy-done.7), channel_id=1, source_target_pairs={{0,96},{8,104},{16,112},{24,120},{32,0},{40,8},{48,16},{56,24},{64... | collective-permute-start | bytes 491528 | tf_op jit(solution)/shard_map/ppermute | solution.py:315
  154.1 5.0 %collective-permute-done.6 = bf16[80,8,128]{2,1,0:T(8,128)(2,1)S(1)} collective-permute-done((bf16[80,8,128]{2,1,0:T(8,128)(2,1)}, bf16[80,8,128]{2,1,0:T(8,128)(2,1)S(1)}, u32[]{:S(2)}, u32[]{:S(2)}) %collective-permute-start.6) | collective-permute-done | bytes 163872 | tf_op jit(solution)/shard_map/ppermute | solution.py:315
  159.1 3.3 collective-permute-start.8
  162.4 4.0 %collective-permute-done.7 = bf16[80,8,128]{2,1,0:T(8,128)(2,1)S(1)} collective-permute-done((bf16[80,8,128]{2,1,0:T(8,128)(2,1)S(1)}, bf16[80,8,128]{2,1,0:T(8,128)(2,1)S(1)}, u32[]{:S(2)}, u32[]{:S(2)}) %collective-permute-start.7) | collective-permute-done | bytes 163872 | tf_op jit(solution)/shard_map/ppermute | solution.py:315
  166.5 5.4 %collective-permute-done.8 = bf16[80,8,128]{2,1,0:T(8,128)(2,1)S(1)} collective-permute-done((bf16[80,8,128]{2,1,0:T(8,128)(2,1)S(1)}, bf16[80,8,128]{2,1,0:T(8,128)(2,1)S(1)}, u32[]{:S(2)}, u32[]{:S(2)}) %collective-permute-start.8) | collective-permute-done | bytes 163872 | tf_op jit(solution)/shard_map/ppermute | solution.py:315
  171.9 1.2 copy-done.3
  173.2 11.0 %all-to-all-start = ((bf16[8,10,10,8,128]{4,3,2,1,0:T(8,128)(2,1)}), bf16[8,10,10,8,128]{4,3,2,1,0:T(8,128)(2,1)S(1)}, u32[]{:S(2)}, u32[]{:S(2)}) async-start(bf16[8,10,10,8,128]{4,3,2,1,0:T(8,128)(2,1)} %copy-done.3), calls=%async_computation | async-start | bytes 3276800 | tf_op jit(solution)/shard_map/all_to_all | solution.py:318
  184.2 1.9 all_gather.9
  186.1 7.3 %expert.3 = bf16[4,2,60,8,128]{4,3,2,1,0:T(8,128)(2,1)} custom-call(bf16[480,8,128]{2,1,0:T(8,128)(2,1)S(1)} %bitcast.73, f32[1,2048]{1,0:T(1,128)S(1)} %bitcast.77, bf16[1,2048,512]{2,1,0:T(8,128)(2,1)} %wg0.3, bf16[1,2048,512]{2,1,0:T(8,128)(2,1)} %collective-permute-done.9.wg1, bf16[1,2048,512]{2,1,0:T(8,128)(2,1)} %wu0.3, ...), custom_call_target="tpu_custom_call" | custom-call | flops 3019898880 | bytes 14548992 | tf_op jit(solution)/shard_map/expert/pallas_call | solution.py:199
  193.4 12.1 %all-to-all-done = bf16[8,10,10,8,128]{4,3,2,1,0:T(8,128)(2,1)S(1)} async-done(((bf16[8,10,10,8,128]{4,3,2,1,0:T(8,128)(2,1)}), bf16[8,10,10,8,128]{4,3,2,1,0:T(8,128)(2,1)S(1)}, u32[]{:S(2)}, u32[]{:S(2)}) %all-to-all-start) | async-done | bytes 1638432 | tf_op jit(solution)/shard_map/all_to_all | solution.py:318
  205.5 4.4 %all-to-all-start.3 = ((bf16[8,6,10,8,128]{4,3,2,1,0:T(8,128)(2,1)}), bf16[8,6,10,8,128]{4,3,2,1,0:T(8,128)(2,1)S(1)}, u32[]{:S(2)}, u32[]{:S(2)}) async-start(bf16[8,6,10,8,128]{4,3,2,1,0:T(8,128)(2,1)} %bitcast.80), calls=%async_computation.3 | async-start | bytes 1966080 | tf_op jit(solution)/shard_map/all_to_all | solution.py:318
  209.9 9.8 %expert.2 = bf16[4,2,100,8,128]{4,3,2,1,0:T(8,128)(2,1)} custom-call(bf16[800,8,128]{2,1,0:T(8,128)(2,1)S(1)} %bitcast.74, f32[1,2048]{1,0:T(1,128)S(1)} %bitcast.78, bf16[1,2048,512]{2,1,0:T(8,128)(2,1)} %wg0.3, bf16[1,2048,512]{2,1,0:T(8,128)(2,1)} %collective-permute-done.9.wg1, bf16[1,2048,512]{2,1,0:T(8,128)(2,1)} %wu0.3, ...), custom_call_target="tpu_custom_call" | custom-call | flops 5033164800 | bytes 15859712 | tf_op jit(solution)/shard_map/expert/pallas_call | solution.py:199
  219.7 4.6 %all-to-all-done.3 = bf16[8,6,10,8,128]{4,3,2,1,0:T(8,128)(2,1)S(1)} async-done(((bf16[8,6,10,8,128]{4,3,2,1,0:T(8,128)(2,1)}), bf16[8,6,10,8,128]{4,3,2,1,0:T(8,128)(2,1)S(1)}, u32[]{:S(2)}, u32[]{:S(2)}) %all-to-all-start.3) | async-done | bytes 983072 | tf_op jit(solution)/shard_map/all_to_all | solution.py:318
  224.3 1.0 copy-done.2
  225.2 4.5 %all-to-all-start.1 = ((bf16[8,10,10,8,128]{4,3,2,1,0:T(8,128)(2,1)}), bf16[8,10,10,8,128]{4,3,2,1,0:T(8,128)(2,1)S(1)}, u32[]{:S(2)}, u32[]{:S(2)}) async-start(bf16[8,10,10,8,128]{4,3,2,1,0:T(8,128)(2,1)} %bitcast.81), calls=%async_computation.1 | async-start | bytes 3276800 | tf_op jit(solution)/shard_map/all_to_all | solution.py:318
  229.7 1.4 fusion.1
  231.1 6.0 %collective-permute-start.27 = (bf16[80,8,128]{2,1,0:T(8,128)(2,1)S(1)}, bf16[80,8,128]{2,1,0:T(8,128)(2,1)S(1)}, u32[]{:S(2)}, u32[]{:S(2)}) collective-permute-start(bf16[80,8,128]{2,1,0:T(8,128)(2,1)S(1)} %bitcast.112), channel_id=1, source_target_pairs={{0,40},{8,48},{16,56},{24,64},{32,72},{40,80},{48,88},{56,96},{64,... | collective-permute-start | bytes 491528 | tf_op jit(solution)/shard_map/ppermute | solution.py:315
  237.1 7.2 %collective-permute-start.29 = (bf16[80,8,128]{2,1,0:T(8,128)(2,1)S(1)}, bf16[80,8,128]{2,1,0:T(8,128)(2,1)S(1)}, u32[]{:S(2)}, u32[]{:S(2)}) collective-permute-start(bf16[80,8,128]{2,1,0:T(8,128)(2,1)S(1)} %bitcast.110), channel_id=1, source_target_pairs={{0,48},{8,56},{16,64},{24,72},{32,80},{40,88},{48,96},{56,104},{64... | collective-permute-start | bytes 491528 | tf_op jit(solution)/shard_map/ppermute | solution.py:315
  244.2 8.6 %collective-permute-start.30 = (bf16[80,8,128]{2,1,0:T(8,128)(2,1)S(1)}, bf16[80,8,128]{2,1,0:T(8,128)(2,1)S(1)}, u32[]{:S(2)}, u32[]{:S(2)}) collective-permute-start(bf16[80,8,128]{2,1,0:T(8,128)(2,1)S(1)} %bitcast.109), channel_id=1, source_target_pairs={{0,72},{8,80},{16,88},{24,96},{32,104},{40,112},{48,120},{56,0},{6... | collective-permute-start | bytes 491528 | tf_op jit(solution)/shard_map/ppermute | solution.py:315
  252.8 2.3 collective-permute-start.31
  255.3 18.9 %collective-permute-start.32 = (bf16[80,8,128]{2,1,0:T(8,128)(2,1)S(1)}, bf16[80,8,128]{2,1,0:T(8,128)(2,1)S(1)}, u32[]{:S(2)}, u32[]{:S(2)}) collective-permute-start(bf16[80,8,128]{2,1,0:T(8,128)(2,1)S(1)} %bitcast.107), channel_id=1, source_target_pairs={{0,64},{8,72},{16,80},{24,88},{32,96},{40,104},{48,112},{56,120},{... | collective-permute-start | bytes 491528 | tf_op jit(solution)/shard_map/ppermute | solution.py:315
  274.2 8.3 %collective-permute-start.12 = (bf16[80,8,128]{2,1,0:T(8,128)(2,1)S(1)}, bf16[80,8,128]{2,1,0:T(8,128)(2,1)S(1)}, u32[]{:S(2)}, u32[]{:S(2)}) collective-permute-start(bf16[80,8,128]{2,1,0:T(8,128)(2,1)S(1)} %bitcast.90), channel_id=1, source_target_pairs={{0,120},{8,0},{16,8},{24,16},{32,24},{40,32},{48,40},{56,48},{64,5... | collective-permute-start | bytes 491528 | tf_op jit(solution)/shard_map/ppermute | solution.py:315
  282.4 9.3 %collective-permute-done.30.refs_13_ = bf16[80,8,128]{2,1,0:T(8,128)(2,1)S(1)} collective-permute-done((bf16[80,8,128]{2,1,0:T(8,128)(2,1)S(1)}, bf16[80,8,128]{2,1,0:T(8,128)(2,1)S(1)}, u32[]{:S(2)}, u32[]{:S(2)}) %collective-permute-start.30) | collective-permute-done | bytes 163872 | tf_op jit(solution)/shard_map/ppermute | solution.py:315
  291.8 11.6 %collective-permute-done.31.refs_14_ = bf16[80,8,128]{2,1,0:T(8,128)(2,1)S(1)} collective-permute-done((bf16[80,8,128]{2,1,0:T(8,128)(2,1)S(1)}, bf16[80,8,128]{2,1,0:T(8,128)(2,1)S(1)}, u32[]{:S(2)}, u32[]{:S(2)}) %collective-permute-start.31) | collective-permute-done | bytes 163872 | tf_op jit(solution)/shard_map/ppermute | solution.py:315
  303.4 4.7 %collective-permute-start.15 = (bf16[80,8,128]{2,1,0:T(8,128)(2,1)S(1)}, bf16[80,8,128]{2,1,0:T(8,128)(2,1)S(1)}, u32[]{:S(2)}, u32[]{:S(2)}) collective-permute-start(bf16[80,8,128]{2,1,0:T(8,128)(2,1)S(1)} %bitcast.87), channel_id=1, source_target_pairs={{0,16},{8,24},{16,32},{24,40},{32,48},{40,56},{48,64},{56,72},{64,... | collective-permute-start | bytes 491528 | tf_op jit(solution)/shard_map/ppermute | solution.py:315
  308.1 13.0 %collective-permute-done.32.refs_15_ = bf16[80,8,128]{2,1,0:T(8,128)(2,1)S(1)} collective-permute-done((bf16[80,8,128]{2,1,0:T(8,128)(2,1)S(1)}, bf16[80,8,128]{2,1,0:T(8,128)(2,1)S(1)}, u32[]{:S(2)}, u32[]{:S(2)}) %collective-permute-start.32) | collective-permute-done | bytes 163872 | tf_op jit(solution)/shard_map/ppermute | solution.py:315
  321.1 3.3 collective-permute-start.17
  324.3 5.4 %collective-permute-start.19 = (bf16[80,8,128]{2,1,0:T(8,128)(2,1)S(1)}, bf16[80,8,128]{2,1,0:T(8,128)(2,1)S(1)}, u32[]{:S(2)}, u32[]{:S(2)}) collective-permute-start(bf16[80,8,128]{2,1,0:T(8,128)(2,1)S(1)} %bitcast.83), channel_id=1, source_target_pairs={{0,32},{8,40},{16,48},{24,56},{32,64},{40,72},{48,80},{56,88},{64,... | collective-permute-start | bytes 491528 | tf_op jit(solution)/shard_map/ppermute | solution.py:315
  329.7 6.9 %collective-permute-start.20 = (bf16[80,8,128]{2,1,0:T(8,128)(2,1)S(1)}, bf16[80,8,128]{2,1,0:T(8,128)(2,1)S(1)}, u32[]{:S(2)}, u32[]{:S(2)}) collective-permute-start(bf16[80,8,128]{2,1,0:T(8,128)(2,1)S(1)} %bitcast.82), channel_id=1, source_target_pairs={{0,88},{8,96},{16,104},{24,112},{32,120},{40,0},{48,8},{56,16},{64... | collective-permute-start | bytes 491528 | tf_op jit(solution)/shard_map/ppermute | solution.py:315
  336.6 8.7 %collective-permute-done.16.refs_5_ = bf16[80,8,128]{2,1,0:T(8,128)(2,1)S(1)} collective-permute-done((bf16[80,8,128]{2,1,0:T(8,128)(2,1)S(1)}, bf16[80,8,128]{2,1,0:T(8,128)(2,1)S(1)}, u32[]{:S(2)}, u32[]{:S(2)}) %collective-permute-start.16) | collective-permute-done | bytes 163872 | tf_op jit(solution)/shard_map/ppermute | solution.py:315
  345.3 14.3 %collective-permute-done.20.refs_9_ = bf16[80,8,128]{2,1,0:T(8,128)(2,1)S(1)} collective-permute-done((bf16[80,8,128]{2,1,0:T(8,128)(2,1)S(1)}, bf16[80,8,128]{2,1,0:T(8,128)(2,1)S(1)}, u32[]{:S(2)}, u32[]{:S(2)}) %collective-permute-start.20) | collective-permute-done | bytes 163872 | tf_op jit(solution)/shard_map/ppermute | solution.py:315
  359.7 5.7 %combine.1 = (f32[256,1024]{1,0:T(8,128)S(1)}, f32[256,1]{1,0:T(8,128)S(1)}) custom-call(s32[2,256]{1,0:T(2,128)S(1)} %copy-done.1, f32[2,256]{1,0:T(2,128)S(1)} %bitcast.79, bf16[80,8,128]{2,1,0:T(8,128)(2,1)S(1)} %bitcast.76, bf16[80,8,128]{2,1,0:T(8,128)(2,1)S(1)} %collective-permute-done.12.refs_1_, ...), custom_call_target="tpu_custom_call" | custom-call | tf_op jit(solution)/shard_map/combine/pallas_call | solution.py:258
  365.4 2.4 all-gather
  (69 shorter events, 9.0 us)
Async XLA Ops:
  5.9 40.6 %collective-permute-start.21 = (bf16[80,8,128]{2,1,0:T(8,128)(2,1)}, bf16[80,8,128]{2,1,0:T(8,128)(2,1)S(1)}, u32[]{:S(2)}, u32[]{:S(2)}) collective-permute-start(bf16[80,8,128]{2,1,0:T(8,128)(2,1)} %get-tuple-element.35), channel_id=1, source_target_pairs={{0,88},{8,96},{16,104},{24,112},{32,120},{40,0},{48,8},{56,16},{64... | collective-permute-start | bytes 491528 | tf_op jit(solution)/shard_map/ppermute | solution.py:315
  28.5 90.6 %collective-permute-start = (bf16[80,8,128]{2,1,0:T(8,128)(2,1)}, bf16[80,8,128]{2,1,0:T(8,128)(2,1)S(1)}, u32[]{:S(2)}, u32[]{:S(2)}) collective-permute-start(bf16[80,8,128]{2,1,0:T(8,128)(2,1)} %get-tuple-element.26), channel_id=1, source_target_pairs={{0,8},{8,16},{16,24},{24,32},{32,40},{40,48},{48,56},{56,64},{64,7... | collective-permute-start | bytes 491528 | tf_op jit(solution)/shard_map/ppermute | solution.py:315
  28.8 90.5 %collective-permute-start.1 = (bf16[80,8,128]{2,1,0:T(8,128)(2,1)}, bf16[80,8,128]{2,1,0:T(8,128)(2,1)S(1)}, u32[]{:S(2)}, u32[]{:S(2)}) collective-permute-start(bf16[80,8,128]{2,1,0:T(8,128)(2,1)} %get-tuple-element.27), channel_id=1, source_target_pairs={{0,120},{8,0},{16,8},{24,16},{32,24},{40,32},{48,40},{56,48},{64,5... | collective-permute-start | bytes 491528 | tf_op jit(solution)/shard_map/ppermute | solution.py:315
  31.1 88.4 %collective-permute-start.2 = (bf16[80,8,128]{2,1,0:T(8,128)(2,1)}, bf16[80,8,128]{2,1,0:T(8,128)(2,1)S(1)}, u32[]{:S(2)}, u32[]{:S(2)}) collective-permute-start(bf16[80,8,128]{2,1,0:T(8,128)(2,1)} %get-tuple-element.28), channel_id=1, source_target_pairs={{0,16},{8,24},{16,32},{24,40},{32,48},{40,56},{48,64},{56,72},{64,... | collective-permute-start | bytes 491528 | tf_op jit(solution)/shard_map/ppermute | solution.py:315
  31.8 30.8 %collective-permute-start.22 = (bf16[80,8,128]{2,1,0:T(8,128)(2,1)}, bf16[80,8,128]{2,1,0:T(8,128)(2,1)S(1)}, u32[]{:S(2)}, u32[]{:S(2)}) collective-permute-start(bf16[80,8,128]{2,1,0:T(8,128)(2,1)} %get-tuple-element.36), channel_id=1, source_target_pairs={{0,48},{8,56},{16,64},{24,72},{32,80},{40,88},{48,96},{56,104},{64... | collective-permute-start | bytes 491528 | tf_op jit(solution)/shard_map/ppermute | solution.py:315
  46.5 20.6 %collective-permute-start.23 = (bf16[80,8,128]{2,1,0:T(8,128)(2,1)}, bf16[80,8,128]{2,1,0:T(8,128)(2,1)S(1)}, u32[]{:S(2)}, u32[]{:S(2)}) collective-permute-start(bf16[80,8,128]{2,1,0:T(8,128)(2,1)} %get-tuple-element.37), channel_id=1, source_target_pairs={{0,80},{8,88},{16,96},{24,104},{32,112},{40,120},{48,0},{56,8},{64... | collective-permute-start | bytes 491528 | tf_op jit(solution)/shard_map/ppermute | solution.py:315
  62.6 31.1 %collective-permute-start.24 = (bf16[80,8,128]{2,1,0:T(8,128)(2,1)}, bf16[80,8,128]{2,1,0:T(8,128)(2,1)S(1)}, u32[]{:S(2)}, u32[]{:S(2)}) collective-permute-start(bf16[80,8,128]{2,1,0:T(8,128)(2,1)} %get-tuple-element.38), channel_id=1, source_target_pairs={{0,56},{8,64},{16,72},{24,80},{32,88},{40,96},{48,104},{56,112},{6... | collective-permute-start | bytes 491528 | tf_op jit(solution)/shard_map/ppermute | solution.py:315
  67.1 30.0 %collective-permute-start.25 = (bf16[80,8,128]{2,1,0:T(8,128)(2,1)}, bf16[80,8,128]{2,1,0:T(8,128)(2,1)S(1)}, u32[]{:S(2)}, u32[]{:S(2)}) collective-permute-start(bf16[80,8,128]{2,1,0:T(8,128)(2,1)} %get-tuple-element.39), channel_id=1, source_target_pairs={{0,72},{8,80},{16,88},{24,96},{32,104},{40,112},{48,120},{56,0},{6... | collective-permute-start | bytes 491528 | tf_op jit(solution)/shard_map/ppermute | solution.py:315
  93.7 20.4 %collective-permute-start.26 = (bf16[80,8,128]{2,1,0:T(8,128)(2,1)}, bf16[80,8,128]{2,1,0:T(8,128)(2,1)S(1)}, u32[]{:S(2)}, u32[]{:S(2)}) collective-permute-start(bf16[80,8,128]{2,1,0:T(8,128)(2,1)} %get-tuple-element.40), channel_id=1, source_target_pairs={{0,64},{8,72},{16,80},{24,88},{32,96},{40,104},{48,112},{56,120},{... | collective-permute-start | bytes 491528 | tf_op jit(solution)/shard_map/ppermute | solution.py:315
  97.2 88.9 %collective-permute-start.10 = (bf16[1,2048,512]{2,1,0:T(8,128)(2,1)}, bf16[1,2048,512]{2,1,0:T(8,128)(2,1)}, u32[]{:S(2)}, u32[]{:S(2)}) collective-permute-start(bf16[1,2048,512]{2,1,0:T(8,128)(2,1)} %wu0.3), channel_id=1, source_target_pairs={{0,1},{1,0},{2,3},{3,2},{4,5},{5,4},{6,7},{7,6},{8,9},{9,8},{10,11... | collective-permute-start | bytes 6291464 | tf_op jit(solution)/shard_map/ppermute | solution.py:323
  114.1 72.0 %collective-permute-start.11 = (bf16[1,512,2048]{2,1,0:T(8,128)(2,1)}, bf16[1,512,2048]{2,1,0:T(8,128)(2,1)}, u32[]{:S(2)}, u32[]{:S(2)}) collective-permute-start(bf16[1,512,2048]{2,1,0:T(8,128)(2,1)} %wd0.3), channel_id=1, source_target_pairs={{0,1},{1,0},{2,3},{3,2},{4,5},{5,4},{6,7},{7,6},{8,9},{9,8},{10,11... | collective-permute-start | bytes 6291464 | tf_op jit(solution)/shard_map/ppermute | solution.py:323
  115.3 31.6 %copy-start.7 = (bf16[80,8,128]{2,1,0:T(8,128)(2,1)S(1)}, bf16[80,8,128]{2,1,0:T(8,128)(2,1)}, u32[]{:S(2)}) copy-start(bf16[80,8,128]{2,1,0:T(8,128)(2,1)} %get-tuple-element.33) | copy-start | bytes 491524
  115.3 43.8 %copy-start.6 = (bf16[80,8,128]{2,1,0:T(8,128)(2,1)S(1)}, bf16[80,8,128]{2,1,0:T(8,128)(2,1)}, u32[]{:S(2)}) copy-start(bf16[80,8,128]{2,1,0:T(8,128)(2,1)} %get-tuple-element.34) | copy-start | bytes 491524
  115.3 57.9 %all-to-all-start.2 = ((bf16[8,6,10,8,128]{4,3,2,1,0:T(8,128)(2,1)}), bf16[8,6,10,8,128]{4,3,2,1,0:T(8,128)(2,1)S(1)}, u32[]{:S(2)}, u32[]{:S(2)}) async-start(bf16[8,6,10,8,128]{4,3,2,1,0:T(8,128)(2,1)} %constant_dynamic-update-slice_fusion.10), calls=%async_computation.2 | async-start | bytes 1966080 | tf_op jit(solution)/shard_map/all_to_all | solution.py:318
  119.1 67.0 %collective-permute-start.9 = (bf16[1,2048,512]{2,1,0:T(8,128)(2,1)}, bf16[1,2048,512]{2,1,0:T(8,128)(2,1)}, u32[]{:S(2)}, u32[]{:S(2)}) collective-permute-start(bf16[1,2048,512]{2,1,0:T(8,128)(2,1)} %wg0.3), channel_id=1, source_target_pairs={{0,1},{1,0},{2,3},{3,2},{4,5},{5,4},{6,7},{7,6},{8,9},{9,8},{10,11... | collective-permute-start | bytes 6291464 | tf_op jit(solution)/shard_map/ppermute | solution.py:323
  119.4 10.1 %collective-permute-start.3 = (bf16[80,8,128]{2,1,0:T(8,128)(2,1)}, bf16[80,8,128]{2,1,0:T(8,128)(2,1)S(1)}, u32[]{:S(2)}, u32[]{:S(2)}) collective-permute-start(bf16[80,8,128]{2,1,0:T(8,128)(2,1)} %get-tuple-element.29), channel_id=1, source_target_pairs={{0,112},{8,120},{16,0},{24,8},{32,16},{40,24},{48,32},{56,40},{64,... | collective-permute-start | bytes 491528 | tf_op jit(solution)/shard_map/ppermute | solution.py:315
  119.6 18.3 %collective-permute-start.4 = (bf16[80,8,128]{2,1,0:T(8,128)(2,1)}, bf16[80,8,128]{2,1,0:T(8,128)(2,1)S(1)}, u32[]{:S(2)}, u32[]{:S(2)}) collective-permute-start(bf16[80,8,128]{2,1,0:T(8,128)(2,1)} %get-tuple-element.30), channel_id=1, source_target_pairs={{0,24},{8,32},{16,40},{24,48},{32,56},{40,64},{48,72},{56,80},{64,... | collective-permute-start | bytes 491528 | tf_op jit(solution)/shard_map/ppermute | solution.py:315
  129.5 17.3 %collective-permute-start.5 = (bf16[80,8,128]{2,1,0:T(8,128)(2,1)}, bf16[80,8,128]{2,1,0:T(8,128)(2,1)S(1)}, u32[]{:S(2)}, u32[]{:S(2)}) collective-permute-start(bf16[80,8,128]{2,1,0:T(8,128)(2,1)} %get-tuple-element.31), channel_id=1, source_target_pairs={{0,104},{8,112},{16,120},{24,0},{32,8},{40,16},{48,24},{56,32},{64... | collective-permute-start | bytes 491528 | tf_op jit(solution)/shard_map/ppermute | solution.py:315
  137.9 21.2 %collective-permute-start.6 = (bf16[80,8,128]{2,1,0:T(8,128)(2,1)}, bf16[80,8,128]{2,1,0:T(8,128)(2,1)S(1)}, u32[]{:S(2)}, u32[]{:S(2)}) collective-permute-start(bf16[80,8,128]{2,1,0:T(8,128)(2,1)} %get-tuple-element.32), channel_id=1, source_target_pairs={{0,32},{8,40},{16,48},{24,56},{32,64},{40,72},{48,80},{56,88},{64,... | collective-permute-start | bytes 491528 | tf_op jit(solution)/shard_map/ppermute | solution.py:315
  146.8 19.6 %collective-permute-start.7 = (bf16[80,8,128]{2,1,0:T(8,128)(2,1)S(1)}, bf16[80,8,128]{2,1,0:T(8,128)(2,1)S(1)}, u32[]{:S(2)}, u32[]{:S(2)}) collective-permute-start(bf16[80,8,128]{2,1,0:T(8,128)(2,1)S(1)} %copy-done.7), channel_id=1, source_target_pairs={{0,96},{8,104},{16,112},{24,120},{32,0},{40,8},{48,16},{56,24},{64... | collective-permute-start | bytes 491528 | tf_op jit(solution)/shard_map/ppermute | solution.py:315
  159.1 12.8 %collective-permute-start.8 = (bf16[80,8,128]{2,1,0:T(8,128)(2,1)S(1)}, bf16[80,8,128]{2,1,0:T(8,128)(2,1)S(1)}, u32[]{:S(2)}, u32[]{:S(2)}) collective-permute-start(bf16[80,8,128]{2,1,0:T(8,128)(2,1)S(1)} %copy-done.6), channel_id=1, source_target_pairs={{0,40},{8,48},{16,56},{24,64},{32,72},{40,80},{48,88},{56,96},{64,... | collective-permute-start | bytes 491528 | tf_op jit(solution)/shard_map/ppermute | solution.py:315
  171.9 1.2 copy-start.3
  173.2 11.0 %copy-start.4 = (bf16[1024]{0:T(1024)(128)(2,1)S(1)}, bf16[1024]{0:T(1024)(128)(2,1)}, u32[]{:S(2)}) copy-start(bf16[1024]{0:T(1024)(128)(2,1)} %param.9) | copy-start | bytes 6148
  173.2 32.3 %all-to-all-start = ((bf16[8,10,10,8,128]{4,3,2,1,0:T(8,128)(2,1)}), bf16[8,10,10,8,128]{4,3,2,1,0:T(8,128)(2,1)S(1)}, u32[]{:S(2)}, u32[]{:S(2)}) async-start(bf16[8,10,10,8,128]{4,3,2,1,0:T(8,128)(2,1)} %copy-done.3), calls=%async_computation | async-start | bytes 3276800 | tf_op jit(solution)/shard_map/all_to_all | solution.py:318
  205.5 18.8 %all-to-all-start.3 = ((bf16[8,6,10,8,128]{4,3,2,1,0:T(8,128)(2,1)}), bf16[8,6,10,8,128]{4,3,2,1,0:T(8,128)(2,1)S(1)}, u32[]{:S(2)}, u32[]{:S(2)}) async-start(bf16[8,6,10,8,128]{4,3,2,1,0:T(8,128)(2,1)} %bitcast.80), calls=%async_computation.3 | async-start | bytes 1966080 | tf_op jit(solution)/shard_map/all_to_all | solution.py:318
  224.3 1.0 copy-start.2
  225.2 29.9 %all-to-all-start.1 = ((bf16[8,10,10,8,128]{4,3,2,1,0:T(8,128)(2,1)}), bf16[8,10,10,8,128]{4,3,2,1,0:T(8,128)(2,1)S(1)}, u32[]{:S(2)}, u32[]{:S(2)}) async-start(bf16[8,10,10,8,128]{4,3,2,1,0:T(8,128)(2,1)} %bitcast.81), calls=%async_computation.1 | async-start | bytes 3276800 | tf_op jit(solution)/shard_map/all_to_all | solution.py:318
  231.1 24.2 %collective-permute-start.27 = (bf16[80,8,128]{2,1,0:T(8,128)(2,1)S(1)}, bf16[80,8,128]{2,1,0:T(8,128)(2,1)S(1)}, u32[]{:S(2)}, u32[]{:S(2)}) collective-permute-start(bf16[80,8,128]{2,1,0:T(8,128)(2,1)S(1)} %bitcast.112), channel_id=1, source_target_pairs={{0,40},{8,48},{16,56},{24,64},{32,72},{40,80},{48,88},{56,96},{64,... | collective-permute-start | bytes 491528 | tf_op jit(solution)/shard_map/ppermute | solution.py:315
  237.1 37.1 %collective-permute-start.28 = (bf16[80,8,128]{2,1,0:T(8,128)(2,1)S(1)}, bf16[80,8,128]{2,1,0:T(8,128)(2,1)S(1)}, u32[]{:S(2)}, u32[]{:S(2)}) collective-permute-start(bf16[80,8,128]{2,1,0:T(8,128)(2,1)S(1)} %bitcast.111), channel_id=1, source_target_pairs={{0,80},{8,88},{16,96},{24,104},{32,112},{40,120},{48,0},{56,8},{64... | collective-permute-start | bytes 491528 | tf_op jit(solution)/shard_map/ppermute | solution.py:315
  237.1 45.4 %collective-permute-start.29 = (bf16[80,8,128]{2,1,0:T(8,128)(2,1)S(1)}, bf16[80,8,128]{2,1,0:T(8,128)(2,1)S(1)}, u32[]{:S(2)}, u32[]{:S(2)}) collective-permute-start(bf16[80,8,128]{2,1,0:T(8,128)(2,1)S(1)} %bitcast.110), channel_id=1, source_target_pairs={{0,48},{8,56},{16,64},{24,72},{32,80},{40,88},{48,96},{56,104},{64... | collective-permute-start | bytes 491528 | tf_op jit(solution)/shard_map/ppermute | solution.py:315
  244.2 47.5 %collective-permute-start.30 = (bf16[80,8,128]{2,1,0:T(8,128)(2,1)S(1)}, bf16[80,8,128]{2,1,0:T(8,128)(2,1)S(1)}, u32[]{:S(2)}, u32[]{:S(2)}) collective-permute-start(bf16[80,8,128]{2,1,0:T(8,128)(2,1)S(1)} %bitcast.109), channel_id=1, source_target_pairs={{0,72},{8,80},{16,88},{24,96},{32,104},{40,112},{48,120},{56,0},{6... | collective-permute-start | bytes 491528 | tf_op jit(solution)/shard_map/ppermute | solution.py:315
  252.8 83.8 %copy-start.5 = (bf16[1024]{0:T(1024)(128)(2,1)S(1)}, bf16[1024]{0:T(1024)(128)(2,1)}, u32[]{:S(2)}) copy-start(bf16[1024]{0:T(1024)(128)(2,1)} %param.15) | copy-start | bytes 6148
  252.8 106.9 %copy-start = (f32[256,2]{0,1:T(2,128)S(1)}, f32[256,2]{0,1:T(2,128)}, u32[]{:S(2)}) copy-start(f32[256,2]{0,1:T(2,128)} %param.14) | copy-start | bytes 6148
  252.8 106.9 %copy-start.1 = (s32[2,256]{1,0:T(2,128)S(1)}, s32[2,256]{1,0:T(2,128)}, u32[]{:S(2)}) copy-start(s32[2,256]{1,0:T(2,128)} %get-tuple-element.24.pos_ref) | copy-start | bytes 6148
  252.8 50.6 %collective-permute-start.31 = (bf16[80,8,128]{2,1,0:T(8,128)(2,1)S(1)}, bf16[80,8,128]{2,1,0:T(8,128)(2,1)S(1)}, u32[]{:S(2)}, u32[]{:S(2)}) collective-permute-start(bf16[80,8,128]{2,1,0:T(8,128)(2,1)S(1)} %bitcast.108), channel_id=1, source_target_pairs={{0,56},{8,64},{16,72},{24,80},{32,88},{40,96},{48,104},{56,112},{6... | collective-permute-start | bytes 491528 | tf_op jit(solution)/shard_map/ppermute | solution.py:315
  255.3 65.8 %collective-permute-start.32 = (bf16[80,8,128]{2,1,0:T(8,128)(2,1)S(1)}, bf16[80,8,128]{2,1,0:T(8,128)(2,1)S(1)}, u32[]{:S(2)}, u32[]{:S(2)}) collective-permute-start(bf16[80,8,128]{2,1,0:T(8,128)(2,1)S(1)} %bitcast.107), channel_id=1, source_target_pairs={{0,64},{8,72},{16,80},{24,88},{32,96},{40,104},{48,112},{56,120},{... | collective-permute-start | bytes 491528 | tf_op jit(solution)/shard_map/ppermute | solution.py:315
  274.2 46.9 %collective-permute-start.12 = (bf16[80,8,128]{2,1,0:T(8,128)(2,1)S(1)}, bf16[80,8,128]{2,1,0:T(8,128)(2,1)S(1)}, u32[]{:S(2)}, u32[]{:S(2)}) collective-permute-start(bf16[80,8,128]{2,1,0:T(8,128)(2,1)S(1)} %bitcast.90), channel_id=1, source_target_pairs={{0,120},{8,0},{16,8},{24,16},{32,24},{40,32},{48,40},{56,48},{64,5... | collective-permute-start | bytes 491528 | tf_op jit(solution)/shard_map/ppermute | solution.py:315
  282.4 41.9 %collective-permute-start.13 = (bf16[80,8,128]{2,1,0:T(8,128)(2,1)S(1)}, bf16[80,8,128]{2,1,0:T(8,128)(2,1)S(1)}, u32[]{:S(2)}, u32[]{:S(2)}) collective-permute-start(bf16[80,8,128]{2,1,0:T(8,128)(2,1)S(1)} %bitcast.89), channel_id=1, source_target_pairs={{0,8},{8,16},{16,24},{24,32},{32,40},{40,48},{48,56},{56,64},{64,7... | collective-permute-start | bytes 491528 | tf_op jit(solution)/shard_map/ppermute | solution.py:315
  291.8 32.6 %collective-permute-start.14 = (bf16[80,8,128]{2,1,0:T(8,128)(2,1)S(1)}, bf16[80,8,128]{2,1,0:T(8,128)(2,1)S(1)}, u32[]{:S(2)}, u32[]{:S(2)}) collective-permute-start(bf16[80,8,128]{2,1,0:T(8,128)(2,1)S(1)} %bitcast.88), channel_id=1, source_target_pairs={{0,112},{8,120},{16,0},{24,8},{32,16},{40,24},{48,32},{56,40},{64,... | collective-permute-start | bytes 491528 | tf_op jit(solution)/shard_map/ppermute | solution.py:315
  303.4 26.3 %collective-permute-start.15 = (bf16[80,8,128]{2,1,0:T(8,128)(2,1)S(1)}, bf16[80,8,128]{2,1,0:T(8,128)(2,1)S(1)}, u32[]{:S(2)}, u32[]{:S(2)}) collective-permute-start(bf16[80,8,128]{2,1,0:T(8,128)(2,1)S(1)} %bitcast.87), channel_id=1, source_target_pairs={{0,16},{8,24},{16,32},{24,40},{32,48},{40,56},{48,64},{56,72},{64,... | collective-permute-start | bytes 491528 | tf_op jit(solution)/shard_map/ppermute | solution.py:315
  321.0 24.3 %collective-permute-start.16 = (bf16[80,8,128]{2,1,0:T(8,128)(2,1)S(1)}, bf16[80,8,128]{2,1,0:T(8,128)(2,1)S(1)}, u32[]{:S(2)}, u32[]{:S(2)}) collective-permute-start(bf16[80,8,128]{2,1,0:T(8,128)(2,1)S(1)} %bitcast.86), channel_id=1, source_target_pairs={{0,104},{8,112},{16,120},{24,0},{32,8},{40,16},{48,24},{56,32},{64... | collective-permute-start | bytes 491528 | tf_op jit(solution)/shard_map/ppermute | solution.py:315
  321.1 24.3 %collective-permute-start.17 = (bf16[80,8,128]{2,1,0:T(8,128)(2,1)S(1)}, bf16[80,8,128]{2,1,0:T(8,128)(2,1)S(1)}, u32[]{:S(2)}, u32[]{:S(2)}) collective-permute-start(bf16[80,8,128]{2,1,0:T(8,128)(2,1)S(1)} %bitcast.85), channel_id=1, source_target_pairs={{0,24},{8,32},{16,40},{24,48},{32,56},{40,64},{48,72},{56,80},{64,... | collective-permute-start | bytes 491528 | tf_op jit(solution)/shard_map/ppermute | solution.py:315
  324.3 21.0 %collective-permute-start.18 = (bf16[80,8,128]{2,1,0:T(8,128)(2,1)S(1)}, bf16[80,8,128]{2,1,0:T(8,128)(2,1)S(1)}, u32[]{:S(2)}, u32[]{:S(2)}) collective-permute-start(bf16[80,8,128]{2,1,0:T(8,128)(2,1)S(1)} %bitcast.84), channel_id=1, source_target_pairs={{0,96},{8,104},{16,112},{24,120},{32,0},{40,8},{48,16},{56,24},{64... | collective-permute-start | bytes 491528 | tf_op jit(solution)/shard_map/ppermute | solution.py:315
  324.3 21.0 %collective-permute-start.19 = (bf16[80,8,128]{2,1,0:T(8,128)(2,1)S(1)}, bf16[80,8,128]{2,1,0:T(8,128)(2,1)S(1)}, u32[]{:S(2)}, u32[]{:S(2)}) collective-permute-start(bf16[80,8,128]{2,1,0:T(8,128)(2,1)S(1)} %bitcast.83), channel_id=1, source_target_pairs={{0,32},{8,40},{16,48},{24,56},{32,64},{40,72},{48,80},{56,88},{64,... | collective-permute-start | bytes 491528 | tf_op jit(solution)/shard_map/ppermute | solution.py:315
  329.7 30.0 %collective-permute-start.20 = (bf16[80,8,128]{2,1,0:T(8,128)(2,1)S(1)}, bf16[80,8,128]{2,1,0:T(8,128)(2,1)S(1)}, u32[]{:S(2)}, u32[]{:S(2)}) collective-permute-start(bf16[80,8,128]{2,1,0:T(8,128)(2,1)S(1)} %bitcast.82), channel_id=1, source_target_pairs={{0,88},{8,96},{16,104},{24,112},{32,120},{40,0},{48,8},{56,16},{64... | collective-permute-start | bytes 491528 | tf_op jit(solution)/shard_map/ppermute | solution.py:315

commit v4 on v3

--- a/solution.py
+++ b/solution.py
@@ -11,7 +11,7 @@
 
 GROUPS = 4
 ROW = 4
-NEAR = 10
+NEAR = 11
 EPS = 1e-06
 LANES = 128
 DISPATCH_VMEM = 60 * 1024 * 1024
@@ -93,7 +93,7 @@
 def expert_kernel(
     arr_ref, gain_ref, wg0, wg1, wu0, wu1, wd0, wd1, out_ref,
     tiles_ref, x_ref, hid_ref, wg_ref, wu_ref, wd_ref, rows_ref, sems, out_sems,
-    *, n_tp, per_part, width,
+    *, n_tp, per_part, unit, width,
 ):
     rows = x_ref.shape[0]
     sub = arr_ref.shape[1]
@@ -108,7 +108,6 @@
         copy.start()
         copies.append(copy)
 
-    unit = 20
     pieces = per_part // unit
 
     def spread(i, carry):
@@ -119,55 +118,74 @@
             tiles_ref[c, pl.ds(at, unit * sub), :] = part.reshape(unit * sub, LANES)
         return carry
 
-    lax.fori_loop(0, sources * pieces, spread, 0)
+    lax.fori_loop(0, sources * pieces, spread, 0, unroll=2)
 
     block = 80
 
-    def normalize(b, carry):
+    def normalize_at(start, count):
         def piece(c, j):
-            return tiles_ref[c, pl.ds(b * (block * sub) + j, block, stride=sub), :]
-
-        squares = jnp.zeros((block, LANES), jnp.float32)
+            return tiles_ref[c, pl.ds(start * sub + j, count, stride=sub), :]
+
+        squares = jnp.zeros((count, LANES), jnp.float32)
         for c in range(n_tp):
             for j in range(sub):
                 v = piece(c, j)
                 squares += v * v
         scale = lax.rsqrt(jnp.sum(squares, axis=1, keepdims=True) / width + EPS)
-        at = pl.ds(pl.multiple_of(b * block, block), block)
         for c in range(n_tp):
             for j in range(sub):
                 lo = c * half + j * LANES
                 v = piece(c, j) * scale * gain_ref[:, lo : lo + LANES]
-                x_ref[at, lo : lo + LANES] = v.astype(jnp.bfloat16)
+                x_ref[pl.ds(start, count), lo : lo + LANES] = v.astype(jnp.bfloat16)
+
+    def normalize(b, carry):
+        normalize_at(pl.multiple_of(b * block, block), block)
         return carry
 
     lax.fori_loop(0, rows // block, normalize, 0)
+    if rows % block:
+        normalize_at(rows - rows % block, rows % block)
 
     ff = wg_ref.shape[2]
     step = 256
-    for h in range(n_tp):
-        copies[2 * h].wait()
-        copies[2 * h + 1].wait()
-        for n in range(ff // step):
-            cols = slice(n * step, (n + 1) * step)
-            gate = jnp.dot(x_ref[...], wg_ref[h, :, cols], preferred_element_type=jnp.float32)
-            upper = jnp.dot(x_ref[...], wu_ref[h, :, cols], preferred_element_type=jnp.float32)
-            hidden = (gate / (1.0 + jnp.exp(-gate))) * upper
-            hid_ref[:, h * ff + n * step : h * ff + (n + 1) * step] = hidden.astype(jnp.bfloat16)
-    for h in range(n_tp):
-        copies[2 * n_tp + h].wait()
+    per_half = ff // step
+    for copy in copies[:2]:
+        copy.wait()
+
+    def hidden_block(i, carry):
+        h, n = i // per_half, i % per_half
+
+        @pl.when(i == per_half)
+        def _():
+            for copy in copies[2 : 2 * n_tp]:
+                copy.wait()
+
+        cols = pl.ds(pl.multiple_of(n * step, step), step)
+        gate = jnp.dot(x_ref[...], wg_ref[h, :, cols], preferred_element_type=jnp.float32)
+        upper = jnp.dot(x_ref[...], wu_ref[h, :, cols], preferred_element_type=jnp.float32)
+        hidden = (gate / (1.0 + jnp.exp(-gate))) * upper
+        hid_ref[:, pl.ds(pl.multiple_of(i * step, step), step)] = hidden.astype(jnp.bfloat16)
+        return carry
+
+    lax.fori_loop(0, n_tp * per_half, hidden_block, 0)
+    for copy in copies[2 * n_tp :]:
+        copy.wait()
     sends = []
     for c in range(n_tp):
-        for n in range(half // step):
-            lo = c * half + n * step
+
+        def down_block(n, carry):
+            cols = pl.ds(pl.multiple_of(c * half + n * step, step), step)
             total = jnp.dot(
                 hid_ref[...],
-                jnp.concatenate([wd_ref[h, :, lo : lo + step] for h in range(n_tp)], axis=0),
+                jnp.concatenate([wd_ref[h, :, cols] for h in range(n_tp)], axis=0),
                 preferred_element_type=jnp.float32,
             )
             for i in range(step // LANES):
                 j = n * (step // LANES) + i
                 tiles_ref[c, pl.ds(j, rows, stride=sub), :] = total[:, i * LANES : (i + 1) * LANES]
+            return carry
+
+        lax.fori_loop(0, half // step, down_block, 0)
 
         def gather(i, carry):
             s, p = i // pieces, i % pieces
@@ -176,7 +194,7 @@
             rows_ref[c, s, pl.ds(p * unit, unit)] = part.astype(jnp.bfloat16)
             return carry
 
-        lax.fori_loop(0, sources * pieces, gather, 0)
+        lax.fori_loop(0, sources * pieces, gather, 0, unroll=2)
         sends.append(pltpu.make_async_copy(rows_ref.at[c], out_ref.at[:, c], out_sems.at[c]))
         sends[c].start()
     for send in sends:
@@ -191,13 +209,15 @@
     return pltpu.with_memory_space_constraint(x, pltpu.HBM)
 
 
-def expert(arrived, gain, gates, uppers, downs, per_part, n_tp):
+def expert(arrived, gain, gates, uppers, downs, per_part, unit, n_tp):
     total, sub, lanes = arrived.shape
     rows = total // n_tp
     _, width, ff = gates[0].shape
     anywhere = pl.BlockSpec(memory_space=pltpu.HBM)
     return pl.pallas_call(
-        functools.partial(expert_kernel, n_tp=n_tp, per_part=per_part, width=width),
+        functools.partial(
+            expert_kernel, n_tp=n_tp, per_part=per_part, unit=unit, width=width
+        ),
         out_shape=pltpu.HBM((rows // per_part, n_tp, per_part, sub, lanes), jnp.bfloat16),
         in_specs=[pl.BlockSpec(memory_space=pltpu.VMEM), pl.BlockSpec(memory_space=pltpu.VMEM)]
         + [anywhere] * (3 * n_tp),
@@ -222,10 +242,60 @@
     )(in_vmem(arrived), gain, *[in_hbm(w) for w in (*gates, *uppers, *downs)])
 
 
-def combine_kernel(pos_ref, mix_ref, *refs):
-    *parts, out_ref, sq_ref, ret_ref, tiles_ref, sems = refs
-    top, tok_dev = pos_ref.shape
-    sub = ret_ref.shape[1]
+def stack_kernel(*refs):
+    *parts, out_ref, sems = refs
+    copies = [
+        pltpu.make_async_copy(part, out_ref.at[:, i], sems.at[i]) for i, part in enumerate(parts)
+    ]
+    for copy in copies:
+        copy.start()
+    for copy in copies:
+        copy.wait()
+
+
+def stacked(parts):
+    first, *rest = parts[0].shape
+    return pl.pallas_call(
+        stack_kernel,
+        out_shape=pltpu.HBM((first, len(parts), *rest), parts[0].dtype),
+        in_specs=[pl.BlockSpec(memory_space=pl.ANY)] * len(parts),
+        out_specs=pl.BlockSpec(memory_space=pltpu.HBM),
+        scratch_shapes=[pltpu.SemaphoreType.DMA((len(parts),))],
+        name="stack",
+    )(*parts)
+
+
+def unstack_kernel(in_ref, *refs):
+    *parts, sems = refs
+    copies = [
+        pltpu.make_async_copy(in_ref.at[:, i], part, sems.at[i]) for i, part in enumerate(parts)
+    ]
+    for copy in copies:
+        copy.start()
+    for copy in copies:
+        copy.wait()
+
+
+def unstacked(whole):
+    first, count, *rest = whole.shape
+    return pl.pallas_call(
+        unstack_kernel,
+        out_shape=tuple(pltpu.HBM((first, *rest), whole.dtype) for _ in range(count)),
+        in_specs=[pl.BlockSpec(memory_space=pl.ANY)],
+        out_specs=tuple(pl.BlockSpec(memory_space=pltpu.HBM) for _ in range(count)),
+        scratch_shapes=[pltpu.SemaphoreType.DMA((count,))],
+        name="unstack",
+    )(whole)
+
+
+def picked(pos_ref, mix_ref, ret_ref, k, t, first):
+    at = pos_ref[k, t] - first
+    held = (at >= 0) & (at < ret_ref.shape[0])
+    row = ret_ref[jnp.where(held, at, 0)].astype(jnp.float32)
+    return jnp.where(held, mix_ref[k, t] * row, 0.0)
+
+
+def fetch(parts, ret_ref, sems):
     block = parts[0].shape[0]
     copies = []
     for i, part in enumerate(parts):
@@ -236,11 +306,56 @@
     for copy in copies:
         copy.wait()
 
+
+def partial_kernel(pos_ref, mix_ref, *refs):
+    *parts, out_ref, ret_ref, sems = refs
+    top, tok_dev = pos_ref.shape
+    sub = ret_ref.shape[1]
+    fetch(parts, ret_ref, sems)
+
     def pick(t, carry):
-        total = mix_ref[0, t] * ret_ref[pos_ref[0, t]].astype(jnp.float32)
+        total = picked(pos_ref, mix_ref, ret_ref, 0, t, 0)
         for k in range(1, top):
-            total += mix_ref[k, t] * ret_ref[pos_ref[k, t]].astype(jnp.float32)
-        tiles_ref[pl.ds(pl.multiple_of(t * sub, sub), sub), :] = total
+            total += picked(pos_ref, mix_ref, ret_ref, k, t, 0)
+        out_ref[pl.ds(pl.multiple_of(t * sub, sub), sub), :] = total
+        return carry
+
+    lax.fori_loop(0, tok_dev, pick, 0, unroll=8)
+
+
+def partial(pos, mix, returned):
+    _, tok_dev = pos.shape
+    block, sub, lanes = returned[0].shape
+    return pl.pallas_call(
+        partial_kernel,
+        out_shape=pltpu.VMEM((tok_dev * sub, lanes), jnp.float32),
+        in_specs=[
+            pl.BlockSpec(memory_space=pltpu.SMEM),
+            pl.BlockSpec(memory_space=pltpu.SMEM),
+        ]
+        + [pl.BlockSpec(memory_space=pl.ANY)] * len(returned),
+        out_specs=pl.BlockSpec(memory_space=pltpu.VMEM),
+        scratch_shapes=[
+            pltpu.VMEM((len(returned) * block, sub, lanes), jnp.bfloat16),
+            pltpu.SemaphoreType.DMA((len(returned),)),
+        ],
+        compiler_params=pltpu.CompilerParams(vmem_limit_bytes=COMBINE_VMEM),
+        name="partial",
+    )(pos, mix, *returned)
+
+
+def combine_kernel(pos_ref, mix_ref, part_ref, *refs, first):
+    *parts, out_ref, sq_ref, ret_ref, tiles_ref, sems = refs
+    top, tok_dev = pos_ref.shape
+    sub = ret_ref.shape[1]
+    fetch(parts, ret_ref, sems)
+
+    def pick(t, carry):
+        at = pl.ds(pl.multiple_of(t * sub, sub), sub)
+        total = part_ref[at, :]
+        for k in range(top):
+            total += picked(pos_ref, mix_ref, ret_ref, k, t, first)
+        tiles_ref[at, :] = total
         return carry
 
     lax.fori_loop(0, tok_dev, pick, 0, unroll=8)
@@ -252,11 +367,11 @@
     sq_ref[...] = jnp.sum(squares, axis=1, keepdims=True)
 
 
-def combined(pos, mix, returned):
+def combined(pos, mix, part, returned, first):
     _, tok_dev = pos.shape
     block, sub, lanes = returned[0].shape
     return pl.pallas_call(
-        combine_kernel,
+        functools.partial(combine_kernel, first=first),
         out_shape=(
             pltpu.VMEM((tok_dev, sub * lanes), jnp.float32),
             jax.ShapeDtypeStruct((tok_dev, 1), jnp.float32),
@@ -264,6 +379,7 @@
         in_specs=[
             pl.BlockSpec(memory_space=pltpu.SMEM),
             pl.BlockSpec(memory_space=pltpu.SMEM),
+            pl.BlockSpec(memory_space=pltpu.VMEM),
         ]
         + [pl.BlockSpec(memory_space=pl.ANY)] * len(returned),
         out_specs=(
@@ -277,7 +393,7 @@
         ],
         compiler_params=pltpu.CompilerParams(vmem_limit_bytes=COMBINE_VMEM),
         name="combine",
-    )(pos, mix, *returned)
+    )(pos, mix, in_vmem(part), *returned)
 
 
 def finish_kernel(mix_ref, tot_ref, gain_ref, out_ref, *, width):
@@ -328,16 +444,19 @@
     returned = []
     for chunk in chunks:
         parts = [came[i].reshape(ROW * n_tp, per_core, sub, LANES) for i in chunk]
-        arrived = exchange(jnp.stack(parts, axis=1))
+        leaving = stacked(parts)
+        arrived = exchange(leaving)
         results = expert(
             arrived.reshape(-1, sub, LANES), gain, (w_gate, others[0]),
-            (w_up, others[1]), (w_down, others[2]), per_core * len(chunk), n_tp,
+            (w_up, others[1]), (w_down, others[2]), per_core * len(chunk), per_core, n_tp,
         )
         back = exchange(results.reshape(arrived.shape))
-        for k, i in enumerate(chunk):
-            part = back[:, k].reshape(ROW * capacity, sub, LANES)
-            returned.append(shift(part, -away[i]))
-    mixed, squares = combined(pos, combine.T, returned)
+        parts = unstacked(back)
+        parts = [part.reshape(ROW * capacity, sub, LANES) for part in parts]
+        returned.append([shift(part, -away[i]) for part, i in zip(parts, chunk)])
+    mix = combine.T
+    part = partial(pos, mix, returned[0])
+    mixed, squares = combined(pos, mix, part, returned[1], NEAR * ROW * capacity)
     totals = lax.all_gather(squares, "tp")
     return finished(mixed, totals, final_gain, width)
 

time: 370 us -> 511 us (1.38)
  Pallas kernels: 29.7 us -> 200 us
  starting transfers between devices: 178 us -> 147 us
    pallas_call x1 -> x6, Pallas kernels: 5.74 us -> 173 us  [the longest x2 81.8 us: stacked(): pl.pallas_call(stack_kernel, out_shape=pltpu.HBM((first, len(parts), *res...]
    ppermute x30, starting transfers between devices: 150 us -> 127 us  [shift(): return lax.ppermute(x, 'z', [(i, (i + by) % n_z) for i in range(n_z)])]
    ppermute x30, waiting for transfers between devices: 131 us -> 137 us  [shift(): return lax.ppermute(x, 'z', [(i, (i + by) % n_z) for i in range(n_z)])]
  transfers between devices with their start and end apart: 37 -> 37, of which waited for: 15 -> 12; matrix products, arithmetic and copies ran while one was open for 2% -> 0% of each run, Pallas kernels for 5% -> 37%
where the time goes in v4:
time: 511 us; the launch traced here: 508 us
  Pallas kernels  200 us (39%)
  waiting for transfers between devices  151 us (30%)
  starting transfers between devices  147 us (29%)
    ppermute x30, waiting for transfers between devices, shift(): return lax.ppermute(x, 'z', [(i, (i + by) % n_z) for i in range(n_z)])  137 us
    ppermute x30, starting transfers between devices, shift(): return lax.ppermute(x, 'z', [(i, (i + by) % n_z) for i in range(n_z)])  127 us
    pallas_call x2, Pallas kernels, stacked(): pl.pallas_call(stack_kernel, out_shape=pltpu.HBM((first, len(parts), *res...  81.8 us
    pallas_call x2, Pallas kernels, unstacked(): pl.pallas_call(unstack_kernel, out_shape=tuple((pltpu.HBM((first, *rest),...  81.8 us
    pallas_call x2, Pallas kernels, expert(): pl.pallas_call(functools.partial(expert_kernel, n_tp=n_tp, per_part=per_p...  20.4 us
    all_to_all x4, starting transfers between devices, exchange(): lax.all_to_all(x, ('x', 'tp'), split_axis=0, concat_axis=0, tiled=True)  18.8 us
    all_to_all x4, waiting for transfers between devices, exchange(): lax.all_to_all(x, ('x', 'tp'), split_axis=0, concat_axis=0, tiled=True)  14.7 us
  transfers between devices with their start and end apart: 37, of which 12 were waited for; matrix products, arithmetic and copies ran while one was open for 0% of the time, Pallas kernels for 37%

profile of v4, /device:TPU:33, one launch (start us, length us, event | category | flops | bytes accessed | tf_op | source)
XLA Modules:
  0.0 508.0 jit_solution(10839684739348818321)
XLA Ops:
  0.0 5.9 %dispatch.1 = (bf16[80,8,128]{2,1,0:T(8,128)(2,1)}, bf16[80,8,128]{2,1,0:T(8,128)(2,1)}, bf16[80,8,128]{2,1,0:T(8,128)(2,1)}, bf16[80,8,128]{2,1,0:T(8,128)(2,1)...) custom-call(s32[1]{0:T(128)} %bitcast.z_ref, ...), custom_call_target="tpu_custom_call" | custom-call | tf_op jit(solution)/shard_map/dispatch/pallas_call | solution.py:69
  5.9 11.3 %collective-permute-start.6 = (bf16[80,8,128]{2,1,0:T(8,128)(2,1)}, bf16[80,8,128]{2,1,0:T(8,128)(2,1)S(1)}, u32[]{:S(2)}, u32[]{:S(2)}) collective-permute-start(bf16[80,8,128]{2,1,0:T(8,128)(2,1)} %get-tuple-element.48), channel_id=1, source_target_pairs={{0,32},{8,40},{16,48},{24,56},{32,64},{40,72},{48,80},{56,88},{64,... | collective-permute-start | bytes 491528 | tf_op jit(solution)/shard_map/ppermute | solution.py:431
  17.2 10.6 %collective-permute-start.7 = (bf16[80,8,128]{2,1,0:T(8,128)(2,1)}, bf16[80,8,128]{2,1,0:T(8,128)(2,1)S(1)}, u32[]{:S(2)}, u32[]{:S(2)}) collective-permute-start(bf16[80,8,128]{2,1,0:T(8,128)(2,1)} %get-tuple-element.49), channel_id=1, source_target_pairs={{0,96},{8,104},{16,112},{24,120},{32,0},{40,8},{48,16},{56,24},{64... | collective-permute-start | bytes 491528 | tf_op jit(solution)/shard_map/ppermute | solution.py:431
  28.8 6.5 %collective-permute-start.9 = (bf16[80,8,128]{2,1,0:T(8,128)(2,1)}, bf16[80,8,128]{2,1,0:T(8,128)(2,1)S(1)}, u32[]{:S(2)}, u32[]{:S(2)}) collective-permute-start(bf16[80,8,128]{2,1,0:T(8,128)(2,1)} %get-tuple-element.51), channel_id=1, source_target_pairs={{0,88},{8,96},{16,104},{24,112},{32,120},{40,0},{48,8},{56,16},{64... | collective-permute-start | bytes 491528 | tf_op jit(solution)/shard_map/ppermute | solution.py:431
  35.7 9.8 %collective-permute-start.1 = (bf16[80,8,128]{2,1,0:T(8,128)(2,1)}, bf16[80,8,128]{2,1,0:T(8,128)(2,1)S(1)}, u32[]{:S(2)}, u32[]{:S(2)}) collective-permute-start(bf16[80,8,128]{2,1,0:T(8,128)(2,1)} %get-tuple-element.43), channel_id=1, source_target_pairs={{0,120},{8,0},{16,8},{24,16},{32,24},{40,32},{48,40},{56,48},{64,5... | collective-permute-start | bytes 491528 | tf_op jit(solution)/shard_map/ppermute | solution.py:431
  45.5 9.4 %collective-permute-start.2 = (bf16[80,8,128]{2,1,0:T(8,128)(2,1)}, bf16[80,8,128]{2,1,0:T(8,128)(2,1)S(1)}, u32[]{:S(2)}, u32[]{:S(2)}) collective-permute-start(bf16[80,8,128]{2,1,0:T(8,128)(2,1)} %get-tuple-element.44), channel_id=1, source_target_pairs={{0,16},{8,24},{16,32},{24,40},{32,48},{40,56},{48,64},{56,72},{64,... | collective-permute-start | bytes 491528 | tf_op jit(solution)/shard_map/ppermute | solution.py:431
  54.8 11.3 %collective-permute-done.8 = bf16[80,8,128]{2,1,0:T(8,128)(2,1)S(1)} collective-permute-done((bf16[80,8,128]{2,1,0:T(8,128)(2,1)}, bf16[80,8,128]{2,1,0:T(8,128)(2,1)S(1)}, u32[]{:S(2)}, u32[]{:S(2)}) %collective-permute-start.8) | collective-permute-done | bytes 163872 | tf_op jit(solution)/shard_map/ppermute | solution.py:431
  67.5 3.7 collective-permute-start.4
  71.2 1.3 collective-permute-done.3
  72.5 3.9 collective-permute-start.5
  76.4 11.5 %collective-permute-done.4 = bf16[80,8,128]{2,1,0:T(8,128)(2,1)S(1)} collective-permute-done((bf16[80,8,128]{2,1,0:T(8,128)(2,1)}, bf16[80,8,128]{2,1,0:T(8,128)(2,1)S(1)}, u32[]{:S(2)}, u32[]{:S(2)}) %collective-permute-start.4) | collective-permute-done | bytes 163872 | tf_op jit(solution)/shard_map/ppermute | solution.py:431
  88.7 55.8 %stack.2 = bf16[8,11,10,8,128]{4,3,2,1,0:T(8,128)(2,1)} custom-call(bf16[8,10,8,128]{3,2,1,0:T(8,128)(2,1)} %bitcast.51, bf16[8,10,8,128]{3,2,1,0:T(8,128)(2,1)} %bitcast.56, bf16[8,10,8,128]{3,2,1,0:T(8,128)(2,1)} %bitcast.57, bf16[8,10,8,128]{3,2,1,0:T(8,128)(2,1)} %bitcast.58, bf16[8,10,8,128]{3,2,1,0:T(8,128)(2,1)} %bitcast.59, ...), custom_call_target="tpu_custom_call" | custom-call | tf_op jit(solution)/shard_map/stack/pallas_call | solution.py:258
  144.5 5.4 %all-to-all-start = ((bf16[8,11,10,8,128]{4,3,2,1,0:T(8,128)(2,1)}), bf16[8,11,10,8,128]{4,3,2,1,0:T(8,128)(2,1)S(1)}, u32[]{:S(2)}, u32[]{:S(2)}) async-start(bf16[8,11,10,8,128]{4,3,2,1,0:T(8,128)(2,1)} %stack.2), calls=%async_computation | async-start | bytes 3604480 | tf_op jit(solution)/shard_map/all_to_all | solution.py:434
  149.9 5.9 %collective-permute-start.23 = (bf16[80,8,128]{2,1,0:T(8,128)(2,1)S(1)}, bf16[80,8,128]{2,1,0:T(8,128)(2,1)S(1)}, u32[]{:S(2)}, u32[]{:S(2)}) collective-permute-start(bf16[80,8,128]{2,1,0:T(8,128)(2,1)S(1)} %copy-done.26), channel_id=1, source_target_pairs={{0,48},{8,56},{16,64},{24,72},{32,80},{40,88},{48,96},{56,104},{64... | collective-permute-start | bytes 491528 | tf_op jit(solution)/shard_map/ppermute | solution.py:431
  155.8 2.6 collective-permute-start.24
  158.4 17.9 %collective-permute-done.23 = bf16[80,8,128]{2,1,0:T(8,128)(2,1)S(1)} collective-permute-done((bf16[80,8,128]{2,1,0:T(8,128)(2,1)S(1)}, bf16[80,8,128]{2,1,0:T(8,128)(2,1)S(1)}, u32[]{:S(2)}, u32[]{:S(2)}) %collective-permute-start.23) | collective-permute-done | bytes 163872 | tf_op jit(solution)/shard_map/ppermute | solution.py:431
  176.7 9.0 %collective-permute-start.26 = (bf16[80,8,128]{2,1,0:T(8,128)(2,1)S(1)}, bf16[80,8,128]{2,1,0:T(8,128)(2,1)S(1)}, u32[]{:S(2)}, u32[]{:S(2)}) collective-permute-start(bf16[80,8,128]{2,1,0:T(8,128)(2,1)S(1)} %copy-done.23), channel_id=1, source_target_pairs={{0,72},{8,80},{16,88},{24,96},{32,104},{40,112},{48,120},{56,0},{6... | collective-permute-start | bytes 491528 | tf_op jit(solution)/shard_map/ppermute | solution.py:431
  185.7 19.3 %collective-permute-done.25 = bf16[80,8,128]{2,1,0:T(8,128)(2,1)S(1)} collective-permute-done((bf16[80,8,128]{2,1,0:T(8,128)(2,1)S(1)}, bf16[80,8,128]{2,1,0:T(8,128)(2,1)S(1)}, u32[]{:S(2)}, u32[]{:S(2)}) %collective-permute-start.25) | collective-permute-done | bytes 163872 | tf_op jit(solution)/shard_map/ppermute | solution.py:431
  205.6 18.8 %collective-permute-done.27 = bf16[80,8,128]{2,1,0:T(8,128)(2,1)S(1)} collective-permute-done((bf16[80,8,128]{2,1,0:T(8,128)(2,1)S(1)}, bf16[80,8,128]{2,1,0:T(8,128)(2,1)S(1)}, u32[]{:S(2)}, u32[]{:S(2)}) %collective-permute-start.27) | collective-permute-done | bytes 163872 | tf_op jit(solution)/shard_map/ppermute | solution.py:431
  225.1 26.0 %stack.3 = bf16[8,5,10,8,128]{4,3,2,1,0:T(8,128)(2,1)} custom-call(bf16[8,10,8,128]{3,2,1,0:T(8,128)(2,1)} %bitcast.62, bf16[8,10,8,128]{3,2,1,0:T(8,128)(2,1)} %bitcast.63, bf16[8,10,8,128]{3,2,1,0:T(8,128)(2,1)} %bitcast.64, bf16[8,10,8,128]{3,2,1,0:T(8,128)(2,1)} %bitcast.65, bf16[8,10,8,128]{3,2,1,0:T(8,128)(2,1)} %bitcast.66), custom_call_target="tpu_custom_call" | custom-call | tf_op jit(solution)/shard_map/stack/pallas_call | solution.py:258
  251.0 4.0 all-to-all-start.2
  255.1 1.9 all_gather.9
  257.0 12.0 %expert.2 = bf16[4,2,110,8,128]{4,3,2,1,0:T(8,128)(2,1)} custom-call(bf16[880,8,128]{2,1,0:T(8,128)(2,1)S(1)} %bitcast.42, f32[1,2048]{1,0:T(1,128)S(1)} %bitcast.45, bf16[1,2048,512]{2,1,0:T(8,128)(2,1)} %wg0.3, bf16[1,2048,512]{2,1,0:T(8,128)(2,1)} %collective-permute-done.10.wg1, bf16[1,2048,512]{2,1,0:T(8,128)(2,1)} %wu0.3, ...), custom_call_target="tpu_custom_call" | custom-call | flops 5536481280 | bytes 16187392 | tf_op jit(solution)/shard_map/expert/pallas_call | solution.py:217
  269.0 4.9 all-to-all-start.1
  273.9 8.4 %expert.3 = bf16[4,2,50,8,128]{4,3,2,1,0:T(8,128)(2,1)} custom-call(bf16[400,8,128]{2,1,0:T(8,128)(2,1)S(1)} %bitcast.41, f32[1,2048]{1,0:T(1,128)S(1)} %bitcast.46, bf16[1,2048,512]{2,1,0:T(8,128)(2,1)} %wg0.3, bf16[1,2048,512]{2,1,0:T(8,128)(2,1)} %collective-permute-done.10.wg1, bf16[1,2048,512]{2,1,0:T(8,128)(2,1)} %wu0.3, ...), custom_call_target="tpu_custom_call" | custom-call | flops 2516582400 | bytes 14221312 | tf_op jit(solution)/shard_map/expert/pallas_call | solution.py:217
  282.2 14.7 %all-to-all-done.1.in_ref = bf16[8,11,10,8,128]{4,3,2,1,0:T(8,128)(2,1)S(1)} async-done(((bf16[8,11,10,8,128]{4,3,2,1,0:T(8,128)(2,1)}), bf16[8,11,10,8,128]{4,3,2,1,0:T(8,128)(2,1)S(1)}, u32[]{:S(2)}, u32[]{:S(2)}) %all-to-all-start.1) | async-done | bytes 1802272 | tf_op jit(solution)/shard_map/all_to_all | solution.py:434
  296.9 1.2 copy-done.3
  298.2 4.6 all-to-all-start.3
  302.7 55.8 %unstack.2 = (bf16[8,10,8,128]{3,2,1,0:T(8,128)(2,1)}, bf16[8,10,8,128]{3,2,1,0:T(8,128)(2,1)}, bf16[8,10,8,128]{3,2,1,0:T(8,128)(2,1)}, bf16[8,10,8,128]{3,2,1,...) custom-call(bf16[8,11,10,8,128]{4,3,2,1,0:T(8,128)(2,1)} %copy-done.3), custom_call_target="tpu_custom_call" | custom-call | tf_op jit(solution)/shard_map/unstack/pallas_call | solution.py:281
  358.5 6.5 %collective-permute-start.13 = (bf16[80,8,128]{2,1,0:T(8,128)(2,1)}, bf16[80,8,128]{2,1,0:T(8,128)(2,1)S(1)}, u32[]{:S(2)}, u32[]{:S(2)}) collective-permute-start(bf16[80,8,128]{2,1,0:T(8,128)(2,1)} %bitcast.82), channel_id=1, source_target_pairs={{0,120},{8,0},{16,8},{24,16},{32,24},{40,32},{48,40},{56,48},{64,5... | collective-permute-start | bytes 491528 | tf_op jit(solution)/shard_map/ppermute | solution.py:431
  365.0 1.3 collective-permute-start.15
  366.3 1.0 collective-permute-start.16
  367.4 2.6 collective-permute-start.17
  370.0 3.7 collective-permute-start.18
  373.6 1.2 collective-permute-start.19
  375.4 5.5 %collective-permute-start.20 = (bf16[80,8,128]{2,1,0:T(8,128)(2,1)}, bf16[80,8,128]{2,1,0:T(8,128)(2,1)S(1)}, u32[]{:S(2)}, u32[]{:S(2)}) collective-permute-start(bf16[80,8,128]{2,1,0:T(8,128)(2,1)} %bitcast.70), channel_id=1, source_target_pairs={{0,32},{8,40},{16,48},{24,56},{32,64},{40,72},{48,80},{56,88},{64,... | collective-permute-start | bytes 491528 | tf_op jit(solution)/shard_map/ppermute | solution.py:431
  380.9 3.4 collective-permute-start.21
  384.3 20.6 %collective-permute-done.17.refs_5_ = bf16[80,8,128]{2,1,0:T(8,128)(2,1)S(1)} collective-permute-done((bf16[80,8,128]{2,1,0:T(8,128)(2,1)}, bf16[80,8,128]{2,1,0:T(8,128)(2,1)S(1)}, u32[]{:S(2)}, u32[]{:S(2)}) %collective-permute-start.17) | collective-permute-done | bytes 163872 | tf_op jit(solution)/shard_map/ppermute | solution.py:431
  405.9 26.0 %unstack.3 = (bf16[8,10,8,128]{3,2,1,0:T(8,128)(2,1)}, bf16[8,10,8,128]{3,2,1,0:T(8,128)(2,1)}, bf16[8,10,8,128]{3,2,1,0:T(8,128)(2,1)}, bf16[8,10,8,128]{3,2,1,0:T(8,128)(2,1)}, bf16[8,10,8,128]{3,2,1,0:T(8,128)(2,1)}) custom-call(bf16[8,5,10,8,128]{4,3,2,1,0:T(8,128)(2,1)} %copy-done.4), custom_call_target="tpu_custom_call" | custom-call | tf_op jit(solution)/shard_map/unstack/pallas_call | solution.py:281
  432.0 7.1 %collective-permute-start.29 = (bf16[80,8,128]{2,1,0:T(8,128)(2,1)}, bf16[80,8,128]{2,1,0:T(8,128)(2,1)S(1)}, u32[]{:S(2)}, u32[]{:S(2)}) collective-permute-start(bf16[80,8,128]{2,1,0:T(8,128)(2,1)} %bitcast.76), channel_id=1, source_target_pairs={{0,48},{8,56},{16,64},{24,72},{32,80},{40,88},{48,96},{56,104},{64... | collective-permute-start | bytes 491528 | tf_op jit(solution)/shard_map/ppermute | solution.py:431
  439.2 7.7 %collective-permute-start.30 = (bf16[80,8,128]{2,1,0:T(8,128)(2,1)}, bf16[80,8,128]{2,1,0:T(8,128)(2,1)S(1)}, u32[]{:S(2)}, u32[]{:S(2)}) collective-permute-start(bf16[80,8,128]{2,1,0:T(8,128)(2,1)} %bitcast.75), channel_id=1, source_target_pairs={{0,72},{8,80},{16,88},{24,96},{32,104},{40,112},{48,120},{56,0},{6... | collective-permute-start | bytes 491528 | tf_op jit(solution)/shard_map/ppermute | solution.py:431
  446.9 1.4 collective-permute-start.31
  448.3 10.7 %collective-permute-start.32 = (bf16[80,8,128]{2,1,0:T(8,128)(2,1)}, bf16[80,8,128]{2,1,0:T(8,128)(2,1)S(1)}, u32[]{:S(2)}, u32[]{:S(2)}) collective-permute-start(bf16[80,8,128]{2,1,0:T(8,128)(2,1)} %bitcast.73), channel_id=1, source_target_pairs={{0,64},{8,72},{16,80},{24,88},{32,96},{40,104},{48,112},{56,120},{... | collective-permute-start | bytes 491528 | tf_op jit(solution)/shard_map/ppermute | solution.py:431
  460.0 5.1 partial.1.part_ref
  465.1 12.9 %collective-permute-done.30.refs_2_ = bf16[80,8,128]{2,1,0:T(8,128)(2,1)S(1)} collective-permute-done((bf16[80,8,128]{2,1,0:T(8,128)(2,1)}, bf16[80,8,128]{2,1,0:T(8,128)(2,1)S(1)}, u32[]{:S(2)}, u32[]{:S(2)}) %collective-permute-start.30) | collective-permute-done | bytes 163872 | tf_op jit(solution)/shard_map/ppermute | solution.py:431
  478.0 21.9 %collective-permute-done.31.refs_3_ = bf16[80,8,128]{2,1,0:T(8,128)(2,1)S(1)} collective-permute-done((bf16[80,8,128]{2,1,0:T(8,128)(2,1)}, bf16[80,8,128]{2,1,0:T(8,128)(2,1)S(1)}, u32[]{:S(2)}, u32[]{:S(2)}) %collective-permute-start.31) | collective-permute-done | bytes 163872 | tf_op jit(solution)/shard_map/ppermute | solution.py:431
  500.0 4.2 combine.1
  504.1 2.9 all-gather
  (94 shorter events, 8.6 us)
Async XLA Ops:
  5.9 29.8 %collective-permute-start.6 = (bf16[80,8,128]{2,1,0:T(8,128)(2,1)}, bf16[80,8,128]{2,1,0:T(8,128)(2,1)S(1)}, u32[]{:S(2)}, u32[]{:S(2)}) collective-permute-start(bf16[80,8,128]{2,1,0:T(8,128)(2,1)} %get-tuple-element.48), channel_id=1, source_target_pairs={{0,32},{8,40},{16,48},{24,56},{32,64},{40,72},{48,80},{56,88},{64,... | collective-permute-start | bytes 491528 | tf_op jit(solution)/shard_map/ppermute | solution.py:431
  17.2 28.3 %collective-permute-start.7 = (bf16[80,8,128]{2,1,0:T(8,128)(2,1)}, bf16[80,8,128]{2,1,0:T(8,128)(2,1)S(1)}, u32[]{:S(2)}, u32[]{:S(2)}) collective-permute-start(bf16[80,8,128]{2,1,0:T(8,128)(2,1)} %get-tuple-element.49), channel_id=1, source_target_pairs={{0,96},{8,104},{16,112},{24,120},{32,0},{40,8},{48,16},{56,24},{64... | collective-permute-start | bytes 491528 | tf_op jit(solution)/shard_map/ppermute | solution.py:431
  27.8 38.3 %collective-permute-start.8 = (bf16[80,8,128]{2,1,0:T(8,128)(2,1)}, bf16[80,8,128]{2,1,0:T(8,128)(2,1)S(1)}, u32[]{:S(2)}, u32[]{:S(2)}) collective-permute-start(bf16[80,8,128]{2,1,0:T(8,128)(2,1)} %get-tuple-element.50), channel_id=1, source_target_pairs={{0,40},{8,48},{16,56},{24,64},{32,72},{40,80},{48,88},{56,96},{64,... | collective-permute-start | bytes 491528 | tf_op jit(solution)/shard_map/ppermute | solution.py:431
  28.8 37.3 %collective-permute-start.9 = (bf16[80,8,128]{2,1,0:T(8,128)(2,1)}, bf16[80,8,128]{2,1,0:T(8,128)(2,1)S(1)}, u32[]{:S(2)}, u32[]{:S(2)}) collective-permute-start(bf16[80,8,128]{2,1,0:T(8,128)(2,1)} %get-tuple-element.51), channel_id=1, source_target_pairs={{0,88},{8,96},{16,104},{24,112},{32,120},{40,0},{48,8},{56,16},{64... | collective-permute-start | bytes 491528 | tf_op jit(solution)/shard_map/ppermute | solution.py:431
  35.3 31.7 %collective-permute-start = (bf16[80,8,128]{2,1,0:T(8,128)(2,1)}, bf16[80,8,128]{2,1,0:T(8,128)(2,1)S(1)}, u32[]{:S(2)}, u32[]{:S(2)}) collective-permute-start(bf16[80,8,128]{2,1,0:T(8,128)(2,1)} %get-tuple-element.42), channel_id=1, source_target_pairs={{0,8},{8,16},{16,24},{24,32},{32,40},{40,48},{48,56},{56,64},{64,7... | collective-permute-start | bytes 491528 | tf_op jit(solution)/shard_map/ppermute | solution.py:431
  35.7 52.3 %copy-start.5 = (bf16[80,8,128]{2,1,0:T(8,128)(2,1)}, bf16[80,8,128]{2,1,0:T(8,128)(2,1)S(1)}, u32[]{:S(2)}) copy-start(bf16[80,8,128]{2,1,0:T(8,128)(2,1)S(1)} %collective-permute-done.6) | copy-start | bytes 491524
  35.7 31.5 %collective-permute-start.1 = (bf16[80,8,128]{2,1,0:T(8,128)(2,1)}, bf16[80,8,128]{2,1,0:T(8,128)(2,1)S(1)}, u32[]{:S(2)}, u32[]{:S(2)}) collective-permute-start(bf16[80,8,128]{2,1,0:T(8,128)(2,1)} %get-tuple-element.43), channel_id=1, source_target_pairs={{0,120},{8,0},{16,8},{24,16},{32,24},{40,32},{48,40},{56,48},{64,5... | collective-permute-start | bytes 491528 | tf_op jit(solution)/shard_map/ppermute | solution.py:431
  45.5 42.5 %copy-start.6 = (bf16[80,8,128]{2,1,0:T(8,128)(2,1)}, bf16[80,8,128]{2,1,0:T(8,128)(2,1)S(1)}, u32[]{:S(2)}) copy-start(bf16[80,8,128]{2,1,0:T(8,128)(2,1)S(1)} %collective-permute-done.7) | copy-start | bytes 491524
  45.5 22.0 %collective-permute-start.2 = (bf16[80,8,128]{2,1,0:T(8,128)(2,1)}, bf16[80,8,128]{2,1,0:T(8,128)(2,1)S(1)}, u32[]{:S(2)}, u32[]{:S(2)}) collective-permute-start(bf16[80,8,128]{2,1,0:T(8,128)(2,1)} %get-tuple-element.44), channel_id=1, source_target_pairs={{0,16},{8,24},{16,32},{24,40},{32,48},{40,56},{48,64},{56,72},{64,... | collective-permute-start | bytes 491528 | tf_op jit(solution)/shard_map/ppermute | solution.py:431
  66.1 6.4 %collective-permute-start.3 = (bf16[80,8,128]{2,1,0:T(8,128)(2,1)}, bf16[80,8,128]{2,1,0:T(8,128)(2,1)S(1)}, u32[]{:S(2)}, u32[]{:S(2)}) collective-permute-start(bf16[80,8,128]{2,1,0:T(8,128)(2,1)} %get-tuple-element.45), channel_id=1, source_target_pairs={{0,112},{8,120},{16,0},{24,8},{32,16},{40,24},{48,32},{56,40},{64,... | collective-permute-start | bytes 491528 | tf_op jit(solution)/shard_map/ppermute | solution.py:431
  66.1 190.8 %collective-permute-start.10 = (bf16[1,2048,512]{2,1,0:T(8,128)(2,1)}, bf16[1,2048,512]{2,1,0:T(8,128)(2,1)}, u32[]{:S(2)}, u32[]{:S(2)}) collective-permute-start(bf16[1,2048,512]{2,1,0:T(8,128)(2,1)} %wg0.3), channel_id=1, source_target_pairs={{0,1},{1,0},{2,3},{3,2},{4,5},{5,4},{6,7},{7,6},{8,9},{9,8},{10,11... | collective-permute-start | bytes 6291464 | tf_op jit(solution)/shard_map/ppermute | solution.py:439
  67.0 190.0 %collective-permute-start.11 = (bf16[1,2048,512]{2,1,0:T(8,128)(2,1)}, bf16[1,2048,512]{2,1,0:T(8,128)(2,1)}, u32[]{:S(2)}, u32[]{:S(2)}) collective-permute-start(bf16[1,2048,512]{2,1,0:T(8,128)(2,1)} %wu0.3), channel_id=1, source_target_pairs={{0,1},{1,0},{2,3},{3,2},{4,5},{5,4},{6,7},{7,6},{8,9},{9,8},{10,11... | collective-permute-start | bytes 6291464 | tf_op jit(solution)/shard_map/ppermute | solution.py:439
  67.2 189.8 %collective-permute-start.12 = (bf16[1,512,2048]{2,1,0:T(8,128)(2,1)}, bf16[1,512,2048]{2,1,0:T(8,128)(2,1)}, u32[]{:S(2)}, u32[]{:S(2)}) collective-permute-start(bf16[1,512,2048]{2,1,0:T(8,128)(2,1)} %wd0.3), channel_id=1, source_target_pairs={{0,1},{1,0},{2,3},{3,2},{4,5},{5,4},{6,7},{7,6},{8,9},{9,8},{10,11... | collective-permute-start | bytes 6291464 | tf_op jit(solution)/shard_map/ppermute | solution.py:439
  67.5 20.5 %collective-permute-start.4 = (bf16[80,8,128]{2,1,0:T(8,128)(2,1)}, bf16[80,8,128]{2,1,0:T(8,128)(2,1)S(1)}, u32[]{:S(2)}, u32[]{:S(2)}) collective-permute-start(bf16[80,8,128]{2,1,0:T(8,128)(2,1)} %get-tuple-element.46), channel_id=1, source_target_pairs={{0,24},{8,32},{16,40},{24,48},{32,56},{40,64},{48,72},{56,80},{64,... | collective-permute-start | bytes 491528 | tf_op jit(solution)/shard_map/ppermute | solution.py:431
  72.5 15.5 %collective-permute-start.5 = (bf16[80,8,128]{2,1,0:T(8,128)(2,1)}, bf16[80,8,128]{2,1,0:T(8,128)(2,1)S(1)}, u32[]{:S(2)}, u32[]{:S(2)}) collective-permute-start(bf16[80,8,128]{2,1,0:T(8,128)(2,1)} %get-tuple-element.47), channel_id=1, source_target_pairs={{0,104},{8,112},{16,120},{24,0},{32,8},{40,16},{48,24},{56,32},{64... | collective-permute-start | bytes 491528 | tf_op jit(solution)/shard_map/ppermute | solution.py:431
  144.5 31.8 %copy-start.24 = (bf16[80,8,128]{2,1,0:T(8,128)(2,1)S(1)}, bf16[80,8,128]{2,1,0:T(8,128)(2,1)}, u32[]{:S(2)}) copy-start(bf16[80,8,128]{2,1,0:T(8,128)(2,1)} %get-tuple-element.65) | copy-start | bytes 491524
  144.5 32.2 %copy-start.23 = (bf16[80,8,128]{2,1,0:T(8,128)(2,1)S(1)}, bf16[80,8,128]{2,1,0:T(8,128)(2,1)}, u32[]{:S(2)}) copy-start(bf16[80,8,128]{2,1,0:T(8,128)(2,1)} %get-tuple-element.66) | copy-start | bytes 491524
  144.5 60.5 %copy-start.22 = (bf16[80,8,128]{2,1,0:T(8,128)(2,1)S(1)}, bf16[80,8,128]{2,1,0:T(8,128)(2,1)}, u32[]{:S(2)}) copy-start(bf16[80,8,128]{2,1,0:T(8,128)(2,1)} %get-tuple-element.67) | copy-start | bytes 491524
  144.5 106.5 %all-to-all-start = ((bf16[8,11,10,8,128]{4,3,2,1,0:T(8,128)(2,1)}), bf16[8,11,10,8,128]{4,3,2,1,0:T(8,128)(2,1)S(1)}, u32[]{:S(2)}, u32[]{:S(2)}) async-start(bf16[8,11,10,8,128]{4,3,2,1,0:T(8,128)(2,1)} %stack.2), calls=%async_computation | async-start | bytes 3604480 | tf_op jit(solution)/shard_map/all_to_all | solution.py:434
  149.9 105.2 %copy-start.20 = (bf16[1024]{0:T(1024)(128)(2,1)S(1)}, bf16[1024]{0:T(1024)(128)(2,1)}, u32[]{:S(2)}) copy-start(bf16[1024]{0:T(1024)(128)(2,1)} %param.9) | copy-start | bytes 6148
  149.9 26.4 %collective-permute-start.23 = (bf16[80,8,128]{2,1,0:T(8,128)(2,1)S(1)}, bf16[80,8,128]{2,1,0:T(8,128)(2,1)S(1)}, u32[]{:S(2)}, u32[]{:S(2)}) collective-permute-start(bf16[80,8,128]{2,1,0:T(8,128)(2,1)S(1)} %copy-done.26), channel_id=1, source_target_pairs={{0,48},{8,56},{16,64},{24,72},{32,80},{40,88},{48,96},{56,104},{64... | collective-permute-start | bytes 491528 | tf_op jit(solution)/shard_map/ppermute | solution.py:431
  155.8 20.9 %collective-permute-start.24 = (bf16[80,8,128]{2,1,0:T(8,128)(2,1)S(1)}, bf16[80,8,128]{2,1,0:T(8,128)(2,1)S(1)}, u32[]{:S(2)}, u32[]{:S(2)}) collective-permute-start(bf16[80,8,128]{2,1,0:T(8,128)(2,1)S(1)} %copy-done.25), channel_id=1, source_target_pairs={{0,80},{8,88},{16,96},{24,104},{32,112},{40,120},{48,0},{56,8},{64... | collective-permute-start | bytes 491528 | tf_op jit(solution)/shard_map/ppermute | solution.py:431
  176.3 48.1 %copy-start.15 = (bf16[80,8,128]{2,1,0:T(8,128)(2,1)}, bf16[80,8,128]{2,1,0:T(8,128)(2,1)S(1)}, u32[]{:S(2)}) copy-start(bf16[80,8,128]{2,1,0:T(8,128)(2,1)S(1)} %collective-permute-done.23) | copy-start | bytes 491524
  176.3 28.7 %collective-permute-start.25 = (bf16[80,8,128]{2,1,0:T(8,128)(2,1)S(1)}, bf16[80,8,128]{2,1,0:T(8,128)(2,1)S(1)}, u32[]{:S(2)}, u32[]{:S(2)}) collective-permute-start(bf16[80,8,128]{2,1,0:T(8,128)(2,1)S(1)} %copy-done.24), channel_id=1, source_target_pairs={{0,56},{8,64},{16,72},{24,80},{32,88},{40,96},{48,104},{56,112},{6... | collective-permute-start | bytes 491528 | tf_op jit(solution)/shard_map/ppermute | solution.py:431
  176.7 47.7 %copy-start.16 = (bf16[80,8,128]{2,1,0:T(8,128)(2,1)}, bf16[80,8,128]{2,1,0:T(8,128)(2,1)S(1)}, u32[]{:S(2)}) copy-start(bf16[80,8,128]{2,1,0:T(8,128)(2,1)S(1)} %collective-permute-done.24) | copy-start | bytes 491524
  176.7 28.9 %collective-permute-start.26 = (bf16[80,8,128]{2,1,0:T(8,128)(2,1)S(1)}, bf16[80,8,128]{2,1,0:T(8,128)(2,1)S(1)}, u32[]{:S(2)}, u32[]{:S(2)}) collective-permute-start(bf16[80,8,128]{2,1,0:T(8,128)(2,1)S(1)} %copy-done.23), channel_id=1, source_target_pairs={{0,72},{8,80},{16,88},{24,96},{32,104},{40,112},{48,120},{56,0},{6... | collective-permute-start | bytes 491528 | tf_op jit(solution)/shard_map/ppermute | solution.py:431
  205.1 19.4 %collective-permute-start.27 = (bf16[80,8,128]{2,1,0:T(8,128)(2,1)S(1)}, bf16[80,8,128]{2,1,0:T(8,128)(2,1)S(1)}, u32[]{:S(2)}, u32[]{:S(2)}) collective-permute-start(bf16[80,8,128]{2,1,0:T(8,128)(2,1)S(1)} %copy-done.22), channel_id=1, source_target_pairs={{0,64},{8,72},{16,80},{24,88},{32,96},{40,104},{48,112},{56,120},{... | collective-permute-start | bytes 491528 | tf_op jit(solution)/shard_map/ppermute | solution.py:431
  251.0 17.9 %all-to-all-start.2 = ((bf16[8,5,10,8,128]{4,3,2,1,0:T(8,128)(2,1)}), bf16[8,5,10,8,128]{4,3,2,1,0:T(8,128)(2,1)S(1)}, u32[]{:S(2)}, u32[]{:S(2)}) async-start(bf16[8,5,10,8,128]{4,3,2,1,0:T(8,128)(2,1)} %stack.3), calls=%async_computation.2 | async-start | bytes 1638400 | tf_op jit(solution)/shard_map/all_to_all | solution.py:434
  269.0 27.9 %all-to-all-start.1 = ((bf16[8,11,10,8,128]{4,3,2,1,0:T(8,128)(2,1)}), bf16[8,11,10,8,128]{4,3,2,1,0:T(8,128)(2,1)S(1)}, u32[]{:S(2)}, u32[]{:S(2)}) async-start(bf16[8,11,10,8,128]{4,3,2,1,0:T(8,128)(2,1)} %bitcast.50), calls=%async_computation.1 | async-start | bytes 3604480 | tf_op jit(solution)/shard_map/all_to_all | solution.py:434
  298.2 160.9 %copy-start.21 = (bf16[1024]{0:T(1024)(128)(2,1)S(1)}, bf16[1024]{0:T(1024)(128)(2,1)}, u32[]{:S(2)}) copy-start(bf16[1024]{0:T(1024)(128)(2,1)} %param.15) | copy-start | bytes 6148
  298.2 160.9 %copy-start.1 = (f32[256,2]{0,1:T(2,128)S(1)}, f32[256,2]{0,1:T(2,128)}, u32[]{:S(2)}) copy-start(f32[256,2]{0,1:T(2,128)} %param.14) | copy-start | bytes 6148
  298.2 160.9 %copy-start.2 = (s32[2,256]{1,0:T(2,128)S(1)}, s32[2,256]{1,0:T(2,128)}, u32[]{:S(2)}) copy-start(s32[2,256]{1,0:T(2,128)} %get-tuple-element.40.pos_ref) | copy-start | bytes 6148
  298.2 106.8 %all-to-all-start.3 = ((bf16[8,5,10,8,128]{4,3,2,1,0:T(8,128)(2,1)}), bf16[8,5,10,8,128]{4,3,2,1,0:T(8,128)(2,1)S(1)}, u32[]{:S(2)}, u32[]{:S(2)}) async-start(bf16[8,5,10,8,128]{4,3,2,1,0:T(8,128)(2,1)} %bitcast.49), calls=%async_computation.3 | async-start | bytes 1638400 | tf_op jit(solution)/shard_map/all_to_all | solution.py:434
  358.5 11.5 %collective-permute-start.13 = (bf16[80,8,128]{2,1,0:T(8,128)(2,1)}, bf16[80,8,128]{2,1,0:T(8,128)(2,1)S(1)}, u32[]{:S(2)}, u32[]{:S(2)}) collective-permute-start(bf16[80,8,128]{2,1,0:T(8,128)(2,1)} %bitcast.82), channel_id=1, source_target_pairs={{0,120},{8,0},{16,8},{24,16},{32,24},{40,32},{48,40},{56,48},{64,5... | collective-permute-start | bytes 491528 | tf_op jit(solution)/shard_map/ppermute | solution.py:431
  365.0 8.6 %collective-permute-start.14 = (bf16[80,8,128]{2,1,0:T(8,128)(2,1)}, bf16[80,8,128]{2,1,0:T(8,128)(2,1)S(1)}, u32[]{:S(2)}, u32[]{:S(2)}) collective-permute-start(bf16[80,8,128]{2,1,0:T(8,128)(2,1)} %bitcast.81), channel_id=1, source_target_pairs={{0,8},{8,16},{16,24},{24,32},{32,40},{40,48},{48,56},{56,64},{64,7... | collective-permute-start | bytes 491528 | tf_op jit(solution)/shard_map/ppermute | solution.py:431
  365.0 10.3 %collective-permute-start.15 = (bf16[80,8,128]{2,1,0:T(8,128)(2,1)}, bf16[80,8,128]{2,1,0:T(8,128)(2,1)S(1)}, u32[]{:S(2)}, u32[]{:S(2)}) collective-permute-start(bf16[80,8,128]{2,1,0:T(8,128)(2,1)} %bitcast.80), channel_id=1, source_target_pairs={{0,112},{8,120},{16,0},{24,8},{32,16},{40,24},{48,32},{56,40},{64,... | collective-permute-start | bytes 491528 | tf_op jit(solution)/shard_map/ppermute | solution.py:431
  366.3 14.6 %collective-permute-start.16 = (bf16[80,8,128]{2,1,0:T(8,128)(2,1)}, bf16[80,8,128]{2,1,0:T(8,128)(2,1)S(1)}, u32[]{:S(2)}, u32[]{:S(2)}) collective-permute-start(bf16[80,8,128]{2,1,0:T(8,128)(2,1)} %bitcast.79), channel_id=1, source_target_pairs={{0,16},{8,24},{16,32},{24,40},{32,48},{40,56},{48,64},{56,72},{64,... | collective-permute-start | bytes 491528 | tf_op jit(solution)/shard_map/ppermute | solution.py:431
  367.4 37.6 %collective-permute-start.17 = (bf16[80,8,128]{2,1,0:T(8,128)(2,1)}, bf16[80,8,128]{2,1,0:T(8,128)(2,1)S(1)}, u32[]{:S(2)}, u32[]{:S(2)}) collective-permute-start(bf16[80,8,128]{2,1,0:T(8,128)(2,1)} %bitcast.78), channel_id=1, source_target_pairs={{0,104},{8,112},{16,120},{24,0},{32,8},{40,16},{48,24},{56,32},{64... | collective-permute-start | bytes 491528 | tf_op jit(solution)/shard_map/ppermute | solution.py:431
  370.0 61.9 %collective-permute-start.18 = (bf16[80,8,128]{2,1,0:T(8,128)(2,1)}, bf16[80,8,128]{2,1,0:T(8,128)(2,1)S(1)}, u32[]{:S(2)}, u32[]{:S(2)}) collective-permute-start(bf16[80,8,128]{2,1,0:T(8,128)(2,1)} %bitcast.72), channel_id=1, source_target_pairs={{0,24},{8,32},{16,40},{24,48},{32,56},{40,64},{48,72},{56,80},{64,... | collective-permute-start | bytes 491528 | tf_op jit(solution)/shard_map/ppermute | solution.py:431
  373.6 58.4 %collective-permute-start.19 = (bf16[80,8,128]{2,1,0:T(8,128)(2,1)}, bf16[80,8,128]{2,1,0:T(8,128)(2,1)S(1)}, u32[]{:S(2)}, u32[]{:S(2)}) collective-permute-start(bf16[80,8,128]{2,1,0:T(8,128)(2,1)} %bitcast.71), channel_id=1, source_target_pairs={{0,96},{8,104},{16,112},{24,120},{32,0},{40,8},{48,16},{56,24},{64... | collective-permute-start | bytes 491528 | tf_op jit(solution)/shard_map/ppermute | solution.py:431
  375.4 63.8 %collective-permute-start.20 = (bf16[80,8,128]{2,1,0:T(8,128)(2,1)}, bf16[80,8,128]{2,1,0:T(8,128)(2,1)S(1)}, u32[]{:S(2)}, u32[]{:S(2)}) collective-permute-start(bf16[80,8,128]{2,1,0:T(8,128)(2,1)} %bitcast.70), channel_id=1, source_target_pairs={{0,32},{8,40},{16,48},{24,56},{32,64},{40,72},{48,80},{56,88},{64,... | collective-permute-start | bytes 491528 | tf_op jit(solution)/shard_map/ppermute | solution.py:431
  380.9 66.0 %collective-permute-start.21 = (bf16[80,8,128]{2,1,0:T(8,128)(2,1)}, bf16[80,8,128]{2,1,0:T(8,128)(2,1)S(1)}, u32[]{:S(2)}, u32[]{:S(2)}) collective-permute-start(bf16[80,8,128]{2,1,0:T(8,128)(2,1)} %bitcast.69), channel_id=1, source_target_pairs={{0,88},{8,96},{16,104},{24,112},{32,120},{40,0},{48,8},{56,16},{64... | collective-permute-start | bytes 491528 | tf_op jit(solution)/shard_map/ppermute | solution.py:431
  404.9 43.4 %collective-permute-start.22 = (bf16[80,8,128]{2,1,0:T(8,128)(2,1)}, bf16[80,8,128]{2,1,0:T(8,128)(2,1)S(1)}, u32[]{:S(2)}, u32[]{:S(2)}) collective-permute-start(bf16[80,8,128]{2,1,0:T(8,128)(2,1)} %bitcast.68), channel_id=1, source_target_pairs={{0,40},{8,48},{16,56},{24,64},{32,72},{40,80},{48,88},{56,96},{64,... | collective-permute-start | bytes 491528 | tf_op jit(solution)/shard_map/ppermute | solution.py:431
  431.9 33.2 %collective-permute-start.28 = (bf16[80,8,128]{2,1,0:T(8,128)(2,1)}, bf16[80,8,128]{2,1,0:T(8,128)(2,1)S(1)}, u32[]{:S(2)}, u32[]{:S(2)}) collective-permute-start(bf16[80,8,128]{2,1,0:T(8,128)(2,1)} %bitcast.77), channel_id=1, source_target_pairs={{0,80},{8,88},{16,96},{24,104},{32,112},{40,120},{48,0},{56,8},{64... | collective-permute-start | bytes 491528 | tf_op jit(solution)/shard_map/ppermute | solution.py:431
  432.0 33.1 %collective-permute-start.29 = (bf16[80,8,128]{2,1,0:T(8,128)(2,1)}, bf16[80,8,128]{2,1,0:T(8,128)(2,1)S(1)}, u32[]{:S(2)}, u32[]{:S(2)}) collective-permute-start(bf16[80,8,128]{2,1,0:T(8,128)(2,1)} %bitcast.76), channel_id=1, source_target_pairs={{0,48},{8,56},{16,64},{24,72},{32,80},{40,88},{48,96},{56,104},{64... | collective-permute-start | bytes 491528 | tf_op jit(solution)/shard_map/ppermute | solution.py:431
  439.2 38.9 %collective-permute-start.30 = (bf16[80,8,128]{2,1,0:T(8,128)(2,1)}, bf16[80,8,128]{2,1,0:T(8,128)(2,1)S(1)}, u32[]{:S(2)}, u32[]{:S(2)}) collective-permute-start(bf16[80,8,128]{2,1,0:T(8,128)(2,1)} %bitcast.75), channel_id=1, source_target_pairs={{0,72},{8,80},{16,88},{24,96},{32,104},{40,112},{48,120},{56,0},{6... | collective-permute-start | bytes 491528 | tf_op jit(solution)/shard_map/ppermute | solution.py:431
  446.9 53.1 %collective-permute-start.31 = (bf16[80,8,128]{2,1,0:T(8,128)(2,1)}, bf16[80,8,128]{2,1,0:T(8,128)(2,1)S(1)}, u32[]{:S(2)}, u32[]{:S(2)}) collective-permute-start(bf16[80,8,128]{2,1,0:T(8,128)(2,1)} %bitcast.74), channel_id=1, source_target_pairs={{0,56},{8,64},{16,72},{24,80},{32,88},{40,96},{48,104},{56,112},{6... | collective-permute-start | bytes 491528 | tf_op jit(solution)/shard_map/ppermute | solution.py:431
  448.3 51.6 %collective-permute-start.32 = (bf16[80,8,128]{2,1,0:T(8,128)(2,1)}, bf16[80,8,128]{2,1,0:T(8,128)(2,1)S(1)}, u32[]{:S(2)}, u32[]{:S(2)}) collective-permute-start(bf16[80,8,128]{2,1,0:T(8,128)(2,1)} %bitcast.73), channel_id=1, source_target_pairs={{0,64},{8,72},{16,80},{24,88},{32,96},{40,104},{48,112},{56,120},{... | collective-permute-start | bytes 491528 | tf_op jit(solution)/shard_map/ppermute | solution.py:431
  (16 other events, 181.7 us)

commit v5 on v4

--- a/solution.py
+++ b/solution.py
@@ -11,16 +11,22 @@
 
 GROUPS = 4
 ROW = 4
-NEAR = 11
+CUTS = (11,)
 EPS = 1e-06
 LANES = 128
 DISPATCH_VMEM = 60 * 1024 * 1024
 EXPERT_VMEM = 40 * 1024 * 1024
 COMBINE_VMEM = 8 * 1024 * 1024
+SMALL_VMEM = 1024 * 1024
 
 
 def offsets(n_z):
     return [(i + 1) // 2 if i % 2 else -(i // 2) for i in range(n_z)]
+
+
+def chunks_of(n_z):
+    bounds = (0, *CUTS, n_z)
+    return [range(lo, hi) for lo, hi in zip(bounds, bounds[1:])]
 
 
 def dispatch_kernel(z_ref, ids_ref, tok_ref, *refs, capacity):
@@ -258,11 +264,12 @@
     return pl.pallas_call(
         stack_kernel,
         out_shape=pltpu.HBM((first, len(parts), *rest), parts[0].dtype),
-        in_specs=[pl.BlockSpec(memory_space=pl.ANY)] * len(parts),
+        in_specs=[pl.BlockSpec(memory_space=pltpu.VMEM)] * len(parts),
         out_specs=pl.BlockSpec(memory_space=pltpu.HBM),
         scratch_shapes=[pltpu.SemaphoreType.DMA((len(parts),))],
+        compiler_params=pltpu.CompilerParams(vmem_limit_bytes=SMALL_VMEM),
         name="stack",
-    )(*parts)
+    )(*[in_vmem(part) for part in parts])
 
 
 def unstack_kernel(in_ref, *refs):
@@ -281,11 +288,12 @@
     return pl.pallas_call(
         unstack_kernel,
         out_shape=tuple(pltpu.HBM((first, *rest), whole.dtype) for _ in range(count)),
-        in_specs=[pl.BlockSpec(memory_space=pl.ANY)],
+        in_specs=[pl.BlockSpec(memory_space=pltpu.VMEM)],
         out_specs=tuple(pl.BlockSpec(memory_space=pltpu.HBM) for _ in range(count)),
         scratch_shapes=[pltpu.SemaphoreType.DMA((count,))],
+        compiler_params=pltpu.CompilerParams(vmem_limit_bytes=SMALL_VMEM),
         name="unstack",
-    )(whole)
+    )(in_vmem(whole))
 
 
 def picked(pos_ref, mix_ref, ret_ref, k, t, first):
@@ -295,23 +303,17 @@
     return jnp.where(held, mix_ref[k, t] * row, 0.0)
 
 
-def fetch(parts, ret_ref, sems):
+def fetch(parts, ret_ref):
     block = parts[0].shape[0]
-    copies = []
     for i, part in enumerate(parts):
-        into = ret_ref.at[pl.ds(i * block, block)]
-        copies.append(pltpu.make_async_copy(part, into, sems.at[i]))
-    for copy in copies:
-        copy.start()
-    for copy in copies:
-        copy.wait()
+        ret_ref[i * block : (i + 1) * block] = part[...]
 
 
 def partial_kernel(pos_ref, mix_ref, *refs):
-    *parts, out_ref, ret_ref, sems = refs
+    *parts, out_ref, ret_ref = refs
     top, tok_dev = pos_ref.shape
     sub = ret_ref.shape[1]
-    fetch(parts, ret_ref, sems)
+    fetch(parts, ret_ref)
 
     def pick(t, carry):
         total = picked(pos_ref, mix_ref, ret_ref, 0, t, 0)
@@ -333,22 +335,21 @@
             pl.BlockSpec(memory_space=pltpu.SMEM),
             pl.BlockSpec(memory_space=pltpu.SMEM),
         ]
-        + [pl.BlockSpec(memory_space=pl.ANY)] * len(returned),
+        + [pl.BlockSpec(memory_space=pltpu.VMEM)] * len(returned),
         out_specs=pl.BlockSpec(memory_space=pltpu.VMEM),
         scratch_shapes=[
             pltpu.VMEM((len(returned) * block, sub, lanes), jnp.bfloat16),
-            pltpu.SemaphoreType.DMA((len(returned),)),
         ],
         compiler_params=pltpu.CompilerParams(vmem_limit_bytes=COMBINE_VMEM),
         name="partial",
-    )(pos, mix, *returned)
+    )(pos, mix, *[in_vmem(x) for x in returned])
 
 
 def combine_kernel(pos_ref, mix_ref, part_ref, *refs, first):
-    *parts, out_ref, sq_ref, ret_ref, tiles_ref, sems = refs
+    *parts, out_ref, sq_ref, ret_ref, tiles_ref = refs
     top, tok_dev = pos_ref.shape
     sub = ret_ref.shape[1]
-    fetch(parts, ret_ref, sems)
+    fetch(parts, ret_ref)
 
     def pick(t, carry):
         at = pl.ds(pl.multiple_of(t * sub, sub), sub)
@@ -381,7 +382,7 @@
             pl.BlockSpec(memory_space=pltpu.SMEM),
             pl.BlockSpec(memory_space=pltpu.VMEM),
         ]
-        + [pl.BlockSpec(memory_space=pl.ANY)] * len(returned),
+        + [pl.BlockSpec(memory_space=pltpu.VMEM)] * len(returned),
         out_specs=(
             pl.BlockSpec(memory_space=pltpu.VMEM),
             pl.BlockSpec(memory_space=pltpu.VMEM),
@@ -389,11 +390,10 @@
         scratch_shapes=[
             pltpu.VMEM((len(returned) * block, sub, lanes), jnp.bfloat16),
             pltpu.VMEM((tok_dev * sub, lanes), jnp.float32),
-            pltpu.SemaphoreType.DMA((len(returned),)),
         ],
         compiler_params=pltpu.CompilerParams(vmem_limit_bytes=COMBINE_VMEM),
         name="combine",
-    )(pos, mix, in_vmem(part), *returned)
+    )(pos, mix, in_vmem(part), *[in_vmem(x) for x in returned])
 
 
 def finish_kernel(mix_ref, tot_ref, gain_ref, out_ref, *, width):
@@ -423,7 +423,7 @@
     per_core = capacity // n_tp
     sub = half // LANES
     away = offsets(n_z)
-    chunks = (range(NEAR), range(NEAR, n_z))
+    chunks = chunks_of(n_z)
 
     def shift(x, by):
         if by % n_z == 0:
@@ -455,8 +455,8 @@
         parts = [part.reshape(ROW * capacity, sub, LANES) for part in parts]
         returned.append([shift(part, -away[i]) for part, i in zip(parts, chunk)])
     mix = combine.T
-    part = partial(pos, mix, returned[0])
-    mixed, squares = combined(pos, mix, part, returned[1], NEAR * ROW * capacity)
+    part = partial(pos, mix, [x for chunk in returned[:-1] for x in chunk])
+    mixed, squares = combined(pos, mix, part, returned[-1], CUTS[-1] * ROW * capacity)
     totals = lax.all_gather(squares, "tp")
     return finished(mixed, totals, final_gain, width)
 

time: 511 us -> 358 us (0.70)
  Pallas kernels: 200 us -> 37.6 us
  waiting for transfers between devices: 151 us -> 163 us
    pallas_call x2, Pallas kernels: 81.8 us -> 2.22 us  [unstacked(): pl.pallas_call(unstack_kernel, out_shape=tuple((pltpu.HBM((first, *rest),...]
    pallas_call x2, Pallas kernels: 81.8 us -> 2.36 us  [stacked(): pl.pallas_call(stack_kernel, out_shape=pltpu.HBM((first, len(parts), *res...]
    ppermute x30, waiting for transfers between devices: 137 us -> 149 us  [shift(): return lax.ppermute(x, 'z', [(i, (i + by) % n_z) for i in range(n_z)])]
  transfers between devices with their start and end apart: 37 -> 37, of which waited for: 12 -> 15; matrix products, arithmetic and copies ran while one was open for 0% -> 0% of each run, Pallas kernels for 37% -> 8%
where the time goes in v5:
time: 358 us; the launch traced here: 357 us
  waiting for transfers between devices  163 us (46%)
  starting transfers between devices  150 us (42%)
  Pallas kernels  37.6 us (11%)
  blocking collectives  4.58 us (1%)
    ppermute x30, waiting for transfers between devices, shift(): return lax.ppermute(x, 'z', [(i, (i + by) % n_z) for i in range(n_z)])  149 us
    ppermute x30, starting transfers between devices, shift(): return lax.ppermute(x, 'z', [(i, (i + by) % n_z) for i in range(n_z)])  130 us
    pallas_call x2, Pallas kernels, expert(): pl.pallas_call(functools.partial(expert_kernel, n_tp=n_tp, per_part=per_p...  20.4 us
    all_to_all x4, starting transfers between devices, exchange(): lax.all_to_all(x, ('x', 'tp'), split_axis=0, concat_axis=0, tiled=True)  18.8 us
    all_to_all x4, waiting for transfers between devices, exchange(): lax.all_to_all(x, ('x', 'tp'), split_axis=0, concat_axis=0, tiled=True)  14.7 us
  transfers between devices with their start and end apart: 37, of which 15 were waited for; matrix products, arithmetic and copies ran while one was open for 0% of the time, Pallas kernels for 8%

profile of v5, /device:TPU:33, one launch (start us, length us, event | category | flops | bytes accessed | tf_op | source)
XLA Modules:
  0.0 357.3 jit_solution(13873894578476622808)
XLA Ops:
  0.0 5.8 %dispatch.1 = (bf16[80,8,128]{2,1,0:T(8,128)(2,1)}, bf16[80,8,128]{2,1,0:T(8,128)(2,1)}, bf16[80,8,128]{2,1,0:T(8,128)(2,1)}, bf16[80,8,128]{2,1,0:T(8,128)(2,1)...) custom-call(s32[1]{0:T(128)} %bitcast.z_ref, ...), custom_call_target="tpu_custom_call" | custom-call | tf_op jit(solution)/shard_map/dispatch/pallas_call | solution.py:75
  5.9 11.3 %collective-permute-start.6 = (bf16[80,8,128]{2,1,0:T(8,128)(2,1)}, bf16[80,8,128]{2,1,0:T(8,128)(2,1)S(1)}, u32[]{:S(2)}, u32[]{:S(2)}) collective-permute-start(bf16[80,8,128]{2,1,0:T(8,128)(2,1)} %get-tuple-element.48), channel_id=1, source_target_pairs={{0,32},{8,40},{16,48},{24,56},{32,64},{40,72},{48,80},{56,88},{64,... | collective-permute-start | bytes 491528 | tf_op jit(solution)/shard_map/ppermute | solution.py:431
  17.1 10.6 %collective-permute-start.7 = (bf16[80,8,128]{2,1,0:T(8,128)(2,1)}, bf16[80,8,128]{2,1,0:T(8,128)(2,1)S(1)}, u32[]{:S(2)}, u32[]{:S(2)}) collective-permute-start(bf16[80,8,128]{2,1,0:T(8,128)(2,1)} %get-tuple-element.49), channel_id=1, source_target_pairs={{0,96},{8,104},{16,112},{24,120},{32,0},{40,8},{48,16},{56,24},{64... | collective-permute-start | bytes 491528 | tf_op jit(solution)/shard_map/ppermute | solution.py:431
  28.8 6.5 %collective-permute-start.9 = (bf16[80,8,128]{2,1,0:T(8,128)(2,1)}, bf16[80,8,128]{2,1,0:T(8,128)(2,1)S(1)}, u32[]{:S(2)}, u32[]{:S(2)}) collective-permute-start(bf16[80,8,128]{2,1,0:T(8,128)(2,1)} %get-tuple-element.51), channel_id=1, source_target_pairs={{0,88},{8,96},{16,104},{24,112},{32,120},{40,0},{48,8},{56,16},{64... | collective-permute-start | bytes 491528 | tf_op jit(solution)/shard_map/ppermute | solution.py:431
  35.7 9.8 %collective-permute-start.1 = (bf16[80,8,128]{2,1,0:T(8,128)(2,1)}, bf16[80,8,128]{2,1,0:T(8,128)(2,1)S(1)}, u32[]{:S(2)}, u32[]{:S(2)}) collective-permute-start(bf16[80,8,128]{2,1,0:T(8,128)(2,1)} %get-tuple-element.43), channel_id=1, source_target_pairs={{0,120},{8,0},{16,8},{24,16},{32,24},{40,32},{48,40},{56,48},{64,5... | collective-permute-start | bytes 491528 | tf_op jit(solution)/shard_map/ppermute | solution.py:431
  45.4 9.3 %collective-permute-start.2 = (bf16[80,8,128]{2,1,0:T(8,128)(2,1)}, bf16[80,8,128]{2,1,0:T(8,128)(2,1)S(1)}, u32[]{:S(2)}, u32[]{:S(2)}) collective-permute-start(bf16[80,8,128]{2,1,0:T(8,128)(2,1)} %get-tuple-element.44), channel_id=1, source_target_pairs={{0,16},{8,24},{16,32},{24,40},{32,48},{40,56},{48,64},{56,72},{64,... | collective-permute-start | bytes 491528 | tf_op jit(solution)/shard_map/ppermute | solution.py:431
  54.7 11.4 %collective-permute-done.8 = bf16[80,8,128]{2,1,0:T(8,128)(2,1)S(1)} collective-permute-done((bf16[80,8,128]{2,1,0:T(8,128)(2,1)}, bf16[80,8,128]{2,1,0:T(8,128)(2,1)S(1)}, u32[]{:S(2)}, u32[]{:S(2)}) %collective-permute-start.8) | collective-permute-done | bytes 163872 | tf_op jit(solution)/shard_map/ppermute | solution.py:431
  67.3 3.9 %collective-permute-start.4 = (bf16[80,8,128]{2,1,0:T(8,128)(2,1)}, bf16[80,8,128]{2,1,0:T(8,128)(2,1)S(1)}, u32[]{:S(2)}, u32[]{:S(2)}) collective-permute-start(bf16[80,8,128]{2,1,0:T(8,128)(2,1)} %get-tuple-element.46), channel_id=1, source_target_pairs={{0,24},{8,32},{16,40},{24,48},{32,56},{40,64},{48,72},{56,80},{64,... | collective-permute-start | bytes 491528 | tf_op jit(solution)/shard_map/ppermute | solution.py:431
  71.2 1.3 collective-permute-done.3
  72.5 3.8 %collective-permute-start.5 = (bf16[80,8,128]{2,1,0:T(8,128)(2,1)}, bf16[80,8,128]{2,1,0:T(8,128)(2,1)S(1)}, u32[]{:S(2)}, u32[]{:S(2)}) collective-permute-start(bf16[80,8,128]{2,1,0:T(8,128)(2,1)} %get-tuple-element.47), channel_id=1, source_target_pairs={{0,104},{8,112},{16,120},{24,0},{32,8},{40,16},{48,24},{56,32},{64... | collective-permute-start | bytes 491528 | tf_op jit(solution)/shard_map/ppermute | solution.py:431
  76.3 11.7 %collective-permute-done.4 = bf16[80,8,128]{2,1,0:T(8,128)(2,1)S(1)} collective-permute-done((bf16[80,8,128]{2,1,0:T(8,128)(2,1)}, bf16[80,8,128]{2,1,0:T(8,128)(2,1)S(1)}, u32[]{:S(2)}, u32[]{:S(2)}) %collective-permute-start.4) | collective-permute-done | bytes 163872 | tf_op jit(solution)/shard_map/ppermute | solution.py:431
  88.9 1.4 stack.2
  90.3 5.3 %all-to-all-start = ((bf16[8,11,10,8,128]{4,3,2,1,0:T(8,128)(2,1)}), bf16[8,11,10,8,128]{4,3,2,1,0:T(8,128)(2,1)S(1)}, u32[]{:S(2)}, u32[]{:S(2)}) async-start(bf16[8,11,10,8,128]{4,3,2,1,0:T(8,128)(2,1)} %stack.2), calls=%async_computation | async-start | bytes 3604480 | tf_op jit(solution)/shard_map/all_to_all | solution.py:434
  95.6 5.9 %collective-permute-start.23 = (bf16[80,8,128]{2,1,0:T(8,128)(2,1)S(1)}, bf16[80,8,128]{2,1,0:T(8,128)(2,1)S(1)}, u32[]{:S(2)}, u32[]{:S(2)}) collective-permute-start(bf16[80,8,128]{2,1,0:T(8,128)(2,1)S(1)} %copy-done.10), channel_id=1, source_target_pairs={{0,48},{8,56},{16,64},{24,72},{32,80},{40,88},{48,96},{56,104},{64... | collective-permute-start | bytes 491528 | tf_op jit(solution)/shard_map/ppermute | solution.py:431
  101.6 2.5 collective-permute-start.24
  104.1 17.7 %collective-permute-done.23 = bf16[80,8,128]{2,1,0:T(8,128)(2,1)S(1)} collective-permute-done((bf16[80,8,128]{2,1,0:T(8,128)(2,1)S(1)}, bf16[80,8,128]{2,1,0:T(8,128)(2,1)S(1)}, u32[]{:S(2)}, u32[]{:S(2)}) %collective-permute-start.23) | collective-permute-done | bytes 163872 | tf_op jit(solution)/shard_map/ppermute | solution.py:431
  122.2 8.9 %collective-permute-start.26 = (bf16[80,8,128]{2,1,0:T(8,128)(2,1)S(1)}, bf16[80,8,128]{2,1,0:T(8,128)(2,1)S(1)}, u32[]{:S(2)}, u32[]{:S(2)}) collective-permute-start(bf16[80,8,128]{2,1,0:T(8,128)(2,1)S(1)} %copy-done.7), channel_id=1, source_target_pairs={{0,72},{8,80},{16,88},{24,96},{32,104},{40,112},{48,120},{56,0},{6... | collective-permute-start | bytes 491528 | tf_op jit(solution)/shard_map/ppermute | solution.py:431
  131.1 20.9 %collective-permute-done.25 = bf16[80,8,128]{2,1,0:T(8,128)(2,1)S(1)} collective-permute-done((bf16[80,8,128]{2,1,0:T(8,128)(2,1)S(1)}, bf16[80,8,128]{2,1,0:T(8,128)(2,1)S(1)}, u32[]{:S(2)}, u32[]{:S(2)}) %collective-permute-start.25) | collective-permute-done | bytes 163872 | tf_op jit(solution)/shard_map/ppermute | solution.py:431
  152.1 6.3 %collective-permute-start.27 = (bf16[80,8,128]{2,1,0:T(8,128)(2,1)S(1)}, bf16[80,8,128]{2,1,0:T(8,128)(2,1)S(1)}, u32[]{:S(2)}, u32[]{:S(2)}) collective-permute-start(bf16[80,8,128]{2,1,0:T(8,128)(2,1)S(1)} %copy-done.6), channel_id=1, source_target_pairs={{0,64},{8,72},{16,80},{24,88},{32,96},{40,104},{48,112},{56,120},{... | collective-permute-start | bytes 491528 | tf_op jit(solution)/shard_map/ppermute | solution.py:431
  158.4 14.8 %collective-permute-done.27 = bf16[80,8,128]{2,1,0:T(8,128)(2,1)S(1)} collective-permute-done((bf16[80,8,128]{2,1,0:T(8,128)(2,1)S(1)}, bf16[80,8,128]{2,1,0:T(8,128)(2,1)S(1)}, u32[]{:S(2)}, u32[]{:S(2)}) %collective-permute-start.27) | collective-permute-done | bytes 163872 | tf_op jit(solution)/shard_map/ppermute | solution.py:431
  174.2 4.0 %all-to-all-start.2 = ((bf16[8,5,10,8,128]{4,3,2,1,0:T(8,128)(2,1)}), bf16[8,5,10,8,128]{4,3,2,1,0:T(8,128)(2,1)S(1)}, u32[]{:S(2)}, u32[]{:S(2)}) async-start(bf16[8,5,10,8,128]{4,3,2,1,0:T(8,128)(2,1)} %stack.3), calls=%async_computation.2 | async-start | bytes 1638400 | tf_op jit(solution)/shard_map/all_to_all | solution.py:434
  178.2 1.9 all_gather.9
  180.1 12.0 %expert.2 = bf16[4,2,110,8,128]{4,3,2,1,0:T(8,128)(2,1)} custom-call(bf16[880,8,128]{2,1,0:T(8,128)(2,1)S(1)} %bitcast.42, f32[1,2048]{1,0:T(1,128)S(1)} %bitcast.61, bf16[1,2048,512]{2,1,0:T(8,128)(2,1)} %wg0.3, bf16[1,2048,512]{2,1,0:T(8,128)(2,1)} %collective-permute-done.10.wg1, bf16[1,2048,512]{2,1,0:T(8,128)(2,1)} %wu0.3, ...), custom_call_target="tpu_custom_call" | custom-call | flops 5536481280 | bytes 16187392 | tf_op jit(solution)/shard_map/expert/pallas_call | solution.py:223
  192.1 4.9 %all-to-all-start.1 = ((bf16[8,11,10,8,128]{4,3,2,1,0:T(8,128)(2,1)}), bf16[8,11,10,8,128]{4,3,2,1,0:T(8,128)(2,1)S(1)}, u32[]{:S(2)}, u32[]{:S(2)}) async-start(bf16[8,11,10,8,128]{4,3,2,1,0:T(8,128)(2,1)} %bitcast.66), calls=%async_computation.1 | async-start | bytes 3604480 | tf_op jit(solution)/shard_map/all_to_all | solution.py:434
  197.0 8.4 %expert.3 = bf16[4,2,50,8,128]{4,3,2,1,0:T(8,128)(2,1)} custom-call(bf16[400,8,128]{2,1,0:T(8,128)(2,1)S(1)} %bitcast.41, f32[1,2048]{1,0:T(1,128)S(1)} %bitcast.62, bf16[1,2048,512]{2,1,0:T(8,128)(2,1)} %wg0.3, bf16[1,2048,512]{2,1,0:T(8,128)(2,1)} %collective-permute-done.10.wg1, bf16[1,2048,512]{2,1,0:T(8,128)(2,1)} %wu0.3, ...), custom_call_target="tpu_custom_call" | custom-call | flops 2516582400 | bytes 14221312 | tf_op jit(solution)/shard_map/expert/pallas_call | solution.py:223
  205.4 14.7 %all-to-all-done.1.in_ref = bf16[8,11,10,8,128]{4,3,2,1,0:T(8,128)(2,1)S(1)} async-done(((bf16[8,11,10,8,128]{4,3,2,1,0:T(8,128)(2,1)}), bf16[8,11,10,8,128]{4,3,2,1,0:T(8,128)(2,1)S(1)}, u32[]{:S(2)}, u32[]{:S(2)}) %all-to-all-start.1) | async-done | bytes 1802272 | tf_op jit(solution)/shard_map/all_to_all | solution.py:434
  220.1 4.6 %all-to-all-start.3 = ((bf16[8,5,10,8,128]{4,3,2,1,0:T(8,128)(2,1)}), bf16[8,5,10,8,128]{4,3,2,1,0:T(8,128)(2,1)S(1)}, u32[]{:S(2)}, u32[]{:S(2)}) async-start(bf16[8,5,10,8,128]{4,3,2,1,0:T(8,128)(2,1)} %bitcast.65), calls=%async_computation.3 | async-start | bytes 1638400 | tf_op jit(solution)/shard_map/all_to_all | solution.py:434
  224.7 1.3 unstack.2
  226.0 4.5 %collective-permute-start.13 = (bf16[80,8,128]{2,1,0:T(8,128)(2,1)}, bf16[80,8,128]{2,1,0:T(8,128)(2,1)S(1)}, u32[]{:S(2)}, u32[]{:S(2)}) collective-permute-start(bf16[80,8,128]{2,1,0:T(8,128)(2,1)} %bitcast.82), channel_id=1, source_target_pairs={{0,120},{8,0},{16,8},{24,16},{32,24},{40,32},{48,40},{56,48},{64,5... | collective-permute-start | bytes 491528 | tf_op jit(solution)/shard_map/ppermute | solution.py:431
  230.4 1.3 collective-permute-start.15
  231.8 1.0 collective-permute-start.16
  232.8 2.4 collective-permute-start.17
  235.2 2.6 collective-permute-start.18
  237.8 2.5 collective-permute-start.19
  240.3 1.1 collective-permute-done.15.refs_3_
  241.4 2.6 collective-permute-start.20
  244.0 4.2 %collective-permute-start.21 = (bf16[80,8,128]{2,1,0:T(8,128)(2,1)}, bf16[80,8,128]{2,1,0:T(8,128)(2,1)S(1)}, u32[]{:S(2)}, u32[]{:S(2)}) collective-permute-start(bf16[80,8,128]{2,1,0:T(8,128)(2,1)} %bitcast.69), channel_id=1, source_target_pairs={{0,88},{8,96},{16,104},{24,112},{32,120},{40,0},{48,8},{56,16},{64... | collective-permute-start | bytes 491528 | tf_op jit(solution)/shard_map/ppermute | solution.py:431
  248.2 21.4 %collective-permute-done.17.refs_5_ = bf16[80,8,128]{2,1,0:T(8,128)(2,1)S(1)} collective-permute-done((bf16[80,8,128]{2,1,0:T(8,128)(2,1)}, bf16[80,8,128]{2,1,0:T(8,128)(2,1)S(1)}, u32[]{:S(2)}, u32[]{:S(2)}) %collective-permute-start.17) | collective-permute-done | bytes 163872 | tf_op jit(solution)/shard_map/ppermute | solution.py:431
  270.7 6.2 %collective-permute-done.19.refs_7_ = bf16[80,8,128]{2,1,0:T(8,128)(2,1)S(1)} collective-permute-done((bf16[80,8,128]{2,1,0:T(8,128)(2,1)}, bf16[80,8,128]{2,1,0:T(8,128)(2,1)S(1)}, u32[]{:S(2)}, u32[]{:S(2)}) %collective-permute-start.19) | collective-permute-done | bytes 163872 | tf_op jit(solution)/shard_map/ppermute | solution.py:431
  277.8 7.6 %collective-permute-start.30 = (bf16[80,8,128]{2,1,0:T(8,128)(2,1)}, bf16[80,8,128]{2,1,0:T(8,128)(2,1)S(1)}, u32[]{:S(2)}, u32[]{:S(2)}) collective-permute-start(bf16[80,8,128]{2,1,0:T(8,128)(2,1)} %bitcast.75), channel_id=1, source_target_pairs={{0,72},{8,80},{16,88},{24,96},{32,104},{40,112},{48,120},{56,0},{6... | collective-permute-start | bytes 491528 | tf_op jit(solution)/shard_map/ppermute | solution.py:431
  285.5 1.9 collective-permute-done.21.refs_9_
  287.4 19.7 %collective-permute-start.32 = (bf16[80,8,128]{2,1,0:T(8,128)(2,1)}, bf16[80,8,128]{2,1,0:T(8,128)(2,1)S(1)}, u32[]{:S(2)}, u32[]{:S(2)}) collective-permute-start(bf16[80,8,128]{2,1,0:T(8,128)(2,1)} %bitcast.73), channel_id=1, source_target_pairs={{0,64},{8,72},{16,80},{24,88},{32,96},{40,104},{48,112},{56,120},{... | collective-permute-start | bytes 491528 | tf_op jit(solution)/shard_map/ppermute | solution.py:431
  308.0 2.8 partial.1.part_ref
  310.8 5.5 %collective-permute-done.29.refs_1_ = bf16[80,8,128]{2,1,0:T(8,128)(2,1)S(1)} collective-permute-done((bf16[80,8,128]{2,1,0:T(8,128)(2,1)}, bf16[80,8,128]{2,1,0:T(8,128)(2,1)S(1)}, u32[]{:S(2)}, u32[]{:S(2)}) %collective-permute-start.29) | collective-permute-done | bytes 163872 | tf_op jit(solution)/shard_map/ppermute | solution.py:431
  316.3 26.4 %collective-permute-done.30.refs_2_ = bf16[80,8,128]{2,1,0:T(8,128)(2,1)S(1)} collective-permute-done((bf16[80,8,128]{2,1,0:T(8,128)(2,1)}, bf16[80,8,128]{2,1,0:T(8,128)(2,1)S(1)}, u32[]{:S(2)}, u32[]{:S(2)}) %collective-permute-start.30) | collective-permute-done | bytes 163872 | tf_op jit(solution)/shard_map/ppermute | solution.py:431
  342.7 7.8 %collective-permute-done.32.refs_4_ = bf16[80,8,128]{2,1,0:T(8,128)(2,1)S(1)} collective-permute-done((bf16[80,8,128]{2,1,0:T(8,128)(2,1)}, bf16[80,8,128]{2,1,0:T(8,128)(2,1)S(1)}, u32[]{:S(2)}, u32[]{:S(2)}) %collective-permute-start.32) | collective-permute-done | bytes 163872 | tf_op jit(solution)/shard_map/ppermute | solution.py:431
  350.5 3.1 combine.1
  353.6 2.7 all-gather
  (62 shorter events, 8.9 us)
Async XLA Ops:
  5.9 29.8 %collective-permute-start.6 = (bf16[80,8,128]{2,1,0:T(8,128)(2,1)}, bf16[80,8,128]{2,1,0:T(8,128)(2,1)S(1)}, u32[]{:S(2)}, u32[]{:S(2)}) collective-permute-start(bf16[80,8,128]{2,1,0:T(8,128)(2,1)} %get-tuple-element.48), channel_id=1, source_target_pairs={{0,32},{8,40},{16,48},{24,56},{32,64},{40,72},{48,80},{56,88},{64,... | collective-permute-start | bytes 491528 | tf_op jit(solution)/shard_map/ppermute | solution.py:431
  17.1 28.3 %collective-permute-start.7 = (bf16[80,8,128]{2,1,0:T(8,128)(2,1)}, bf16[80,8,128]{2,1,0:T(8,128)(2,1)S(1)}, u32[]{:S(2)}, u32[]{:S(2)}) collective-permute-start(bf16[80,8,128]{2,1,0:T(8,128)(2,1)} %get-tuple-element.49), channel_id=1, source_target_pairs={{0,96},{8,104},{16,112},{24,120},{32,0},{40,8},{48,16},{56,24},{64... | collective-permute-start | bytes 491528 | tf_op jit(solution)/shard_map/ppermute | solution.py:431
  27.8 38.3 %collective-permute-start.8 = (bf16[80,8,128]{2,1,0:T(8,128)(2,1)}, bf16[80,8,128]{2,1,0:T(8,128)(2,1)S(1)}, u32[]{:S(2)}, u32[]{:S(2)}) collective-permute-start(bf16[80,8,128]{2,1,0:T(8,128)(2,1)} %get-tuple-element.50), channel_id=1, source_target_pairs={{0,40},{8,48},{16,56},{24,64},{32,72},{40,80},{48,88},{56,96},{64,... | collective-permute-start | bytes 491528 | tf_op jit(solution)/shard_map/ppermute | solution.py:431
  28.8 37.3 %collective-permute-start.9 = (bf16[80,8,128]{2,1,0:T(8,128)(2,1)}, bf16[80,8,128]{2,1,0:T(8,128)(2,1)S(1)}, u32[]{:S(2)}, u32[]{:S(2)}) collective-permute-start(bf16[80,8,128]{2,1,0:T(8,128)(2,1)} %get-tuple-element.51), channel_id=1, source_target_pairs={{0,88},{8,96},{16,104},{24,112},{32,120},{40,0},{48,8},{56,16},{64... | collective-permute-start | bytes 491528 | tf_op jit(solution)/shard_map/ppermute | solution.py:431
  35.3 31.6 %collective-permute-start = (bf16[80,8,128]{2,1,0:T(8,128)(2,1)}, bf16[80,8,128]{2,1,0:T(8,128)(2,1)S(1)}, u32[]{:S(2)}, u32[]{:S(2)}) collective-permute-start(bf16[80,8,128]{2,1,0:T(8,128)(2,1)} %get-tuple-element.42), channel_id=1, source_target_pairs={{0,8},{8,16},{16,24},{24,32},{32,40},{40,48},{48,56},{56,64},{64,7... | collective-permute-start | bytes 491528 | tf_op jit(solution)/shard_map/ppermute | solution.py:431
  35.7 31.3 %collective-permute-start.1 = (bf16[80,8,128]{2,1,0:T(8,128)(2,1)}, bf16[80,8,128]{2,1,0:T(8,128)(2,1)S(1)}, u32[]{:S(2)}, u32[]{:S(2)}) collective-permute-start(bf16[80,8,128]{2,1,0:T(8,128)(2,1)} %get-tuple-element.43), channel_id=1, source_target_pairs={{0,120},{8,0},{16,8},{24,16},{32,24},{40,32},{48,40},{56,48},{64,5... | collective-permute-start | bytes 491528 | tf_op jit(solution)/shard_map/ppermute | solution.py:431
  45.4 21.9 %collective-permute-start.2 = (bf16[80,8,128]{2,1,0:T(8,128)(2,1)}, bf16[80,8,128]{2,1,0:T(8,128)(2,1)S(1)}, u32[]{:S(2)}, u32[]{:S(2)}) collective-permute-start(bf16[80,8,128]{2,1,0:T(8,128)(2,1)} %get-tuple-element.44), channel_id=1, source_target_pairs={{0,16},{8,24},{16,32},{24,40},{32,48},{40,56},{48,64},{56,72},{64,... | collective-permute-start | bytes 491528 | tf_op jit(solution)/shard_map/ppermute | solution.py:431
  66.1 6.4 %collective-permute-start.3 = (bf16[80,8,128]{2,1,0:T(8,128)(2,1)}, bf16[80,8,128]{2,1,0:T(8,128)(2,1)S(1)}, u32[]{:S(2)}, u32[]{:S(2)}) collective-permute-start(bf16[80,8,128]{2,1,0:T(8,128)(2,1)} %get-tuple-element.45), channel_id=1, source_target_pairs={{0,112},{8,120},{16,0},{24,8},{32,16},{40,24},{48,32},{56,40},{64,... | collective-permute-start | bytes 491528 | tf_op jit(solution)/shard_map/ppermute | solution.py:431
  66.1 114.0 %collective-permute-start.10 = (bf16[1,2048,512]{2,1,0:T(8,128)(2,1)}, bf16[1,2048,512]{2,1,0:T(8,128)(2,1)}, u32[]{:S(2)}, u32[]{:S(2)}) collective-permute-start(bf16[1,2048,512]{2,1,0:T(8,128)(2,1)} %wg0.3), channel_id=1, source_target_pairs={{0,1},{1,0},{2,3},{3,2},{4,5},{5,4},{6,7},{7,6},{8,9},{9,8},{10,11... | collective-permute-start | bytes 6291464 | tf_op jit(solution)/shard_map/ppermute | solution.py:439
  66.8 113.3 %collective-permute-start.11 = (bf16[1,2048,512]{2,1,0:T(8,128)(2,1)}, bf16[1,2048,512]{2,1,0:T(8,128)(2,1)}, u32[]{:S(2)}, u32[]{:S(2)}) collective-permute-start(bf16[1,2048,512]{2,1,0:T(8,128)(2,1)} %wu0.3), channel_id=1, source_target_pairs={{0,1},{1,0},{2,3},{3,2},{4,5},{5,4},{6,7},{7,6},{8,9},{9,8},{10,11... | collective-permute-start | bytes 6291464 | tf_op jit(solution)/shard_map/ppermute | solution.py:439
  67.0 113.1 %collective-permute-start.12 = (bf16[1,512,2048]{2,1,0:T(8,128)(2,1)}, bf16[1,512,2048]{2,1,0:T(8,128)(2,1)}, u32[]{:S(2)}, u32[]{:S(2)}) collective-permute-start(bf16[1,512,2048]{2,1,0:T(8,128)(2,1)} %wd0.3), channel_id=1, source_target_pairs={{0,1},{1,0},{2,3},{3,2},{4,5},{5,4},{6,7},{7,6},{8,9},{9,8},{10,11... | collective-permute-start | bytes 6291464 | tf_op jit(solution)/shard_map/ppermute | solution.py:439
  67.3 20.6 %collective-permute-start.4 = (bf16[80,8,128]{2,1,0:T(8,128)(2,1)}, bf16[80,8,128]{2,1,0:T(8,128)(2,1)S(1)}, u32[]{:S(2)}, u32[]{:S(2)}) collective-permute-start(bf16[80,8,128]{2,1,0:T(8,128)(2,1)} %get-tuple-element.46), channel_id=1, source_target_pairs={{0,24},{8,32},{16,40},{24,48},{32,56},{40,64},{48,72},{56,80},{64,... | collective-permute-start | bytes 491528 | tf_op jit(solution)/shard_map/ppermute | solution.py:431
  72.5 15.5 %collective-permute-start.5 = (bf16[80,8,128]{2,1,0:T(8,128)(2,1)}, bf16[80,8,128]{2,1,0:T(8,128)(2,1)S(1)}, u32[]{:S(2)}, u32[]{:S(2)}) collective-permute-start(bf16[80,8,128]{2,1,0:T(8,128)(2,1)} %get-tuple-element.47), channel_id=1, source_target_pairs={{0,104},{8,112},{16,120},{24,0},{32,8},{40,16},{48,24},{56,32},{64... | collective-permute-start | bytes 491528 | tf_op jit(solution)/shard_map/ppermute | solution.py:431
  87.9 0.9 copy-start
  90.2 5.4 %copy-start.10 = (bf16[80,8,128]{2,1,0:T(8,128)(2,1)S(1)}, bf16[80,8,128]{2,1,0:T(8,128)(2,1)}, u32[]{:S(2)}) copy-start(bf16[80,8,128]{2,1,0:T(8,128)(2,1)} %get-tuple-element.63) | copy-start | bytes 491524
  90.2 11.3 %copy-start.9 = (bf16[80,8,128]{2,1,0:T(8,128)(2,1)S(1)}, bf16[80,8,128]{2,1,0:T(8,128)(2,1)}, u32[]{:S(2)}) copy-start(bf16[80,8,128]{2,1,0:T(8,128)(2,1)} %get-tuple-element.64) | copy-start | bytes 491524
  90.3 31.6 %copy-start.8 = (bf16[80,8,128]{2,1,0:T(8,128)(2,1)S(1)}, bf16[80,8,128]{2,1,0:T(8,128)(2,1)}, u32[]{:S(2)}) copy-start(bf16[80,8,128]{2,1,0:T(8,128)(2,1)} %get-tuple-element.65) | copy-start | bytes 491524
  90.3 32.0 %copy-start.7 = (bf16[80,8,128]{2,1,0:T(8,128)(2,1)S(1)}, bf16[80,8,128]{2,1,0:T(8,128)(2,1)}, u32[]{:S(2)}) copy-start(bf16[80,8,128]{2,1,0:T(8,128)(2,1)} %get-tuple-element.66) | copy-start | bytes 491524
  90.3 61.8 %copy-start.6 = (bf16[80,8,128]{2,1,0:T(8,128)(2,1)S(1)}, bf16[80,8,128]{2,1,0:T(8,128)(2,1)}, u32[]{:S(2)}) copy-start(bf16[80,8,128]{2,1,0:T(8,128)(2,1)} %get-tuple-element.67) | copy-start | bytes 491524
  90.3 83.9 %all-to-all-start = ((bf16[8,11,10,8,128]{4,3,2,1,0:T(8,128)(2,1)}), bf16[8,11,10,8,128]{4,3,2,1,0:T(8,128)(2,1)S(1)}, u32[]{:S(2)}, u32[]{:S(2)}) async-start(bf16[8,11,10,8,128]{4,3,2,1,0:T(8,128)(2,1)} %stack.2), calls=%async_computation | async-start | bytes 3604480 | tf_op jit(solution)/shard_map/all_to_all | solution.py:434
  95.6 82.6 %copy-start.4 = (bf16[1024]{0:T(1024)(128)(2,1)S(1)}, bf16[1024]{0:T(1024)(128)(2,1)}, u32[]{:S(2)}) copy-start(bf16[1024]{0:T(1024)(128)(2,1)} %param.9) | copy-start | bytes 6148
  95.6 26.2 %collective-permute-start.23 = (bf16[80,8,128]{2,1,0:T(8,128)(2,1)S(1)}, bf16[80,8,128]{2,1,0:T(8,128)(2,1)S(1)}, u32[]{:S(2)}, u32[]{:S(2)}) collective-permute-start(bf16[80,8,128]{2,1,0:T(8,128)(2,1)S(1)} %copy-done.10), channel_id=1, source_target_pairs={{0,48},{8,56},{16,64},{24,72},{32,80},{40,88},{48,96},{56,104},{64... | collective-permute-start | bytes 491528 | tf_op jit(solution)/shard_map/ppermute | solution.py:431
  101.6 20.6 %collective-permute-start.24 = (bf16[80,8,128]{2,1,0:T(8,128)(2,1)S(1)}, bf16[80,8,128]{2,1,0:T(8,128)(2,1)S(1)}, u32[]{:S(2)}, u32[]{:S(2)}) collective-permute-start(bf16[80,8,128]{2,1,0:T(8,128)(2,1)S(1)} %copy-done.9), channel_id=1, source_target_pairs={{0,80},{8,88},{16,96},{24,104},{32,112},{40,120},{48,0},{56,8},{64... | collective-permute-start | bytes 491528 | tf_op jit(solution)/shard_map/ppermute | solution.py:431
  121.9 30.2 %collective-permute-start.25 = (bf16[80,8,128]{2,1,0:T(8,128)(2,1)S(1)}, bf16[80,8,128]{2,1,0:T(8,128)(2,1)S(1)}, u32[]{:S(2)}, u32[]{:S(2)}) collective-permute-start(bf16[80,8,128]{2,1,0:T(8,128)(2,1)S(1)} %copy-done.8), channel_id=1, source_target_pairs={{0,56},{8,64},{16,72},{24,80},{32,88},{40,96},{48,104},{56,112},{6... | collective-permute-start | bytes 491528 | tf_op jit(solution)/shard_map/ppermute | solution.py:431
  122.2 36.2 %collective-permute-start.26 = (bf16[80,8,128]{2,1,0:T(8,128)(2,1)S(1)}, bf16[80,8,128]{2,1,0:T(8,128)(2,1)S(1)}, u32[]{:S(2)}, u32[]{:S(2)}) collective-permute-start(bf16[80,8,128]{2,1,0:T(8,128)(2,1)S(1)} %copy-done.7), channel_id=1, source_target_pairs={{0,72},{8,80},{16,88},{24,96},{32,104},{40,112},{48,120},{56,0},{6... | collective-permute-start | bytes 491528 | tf_op jit(solution)/shard_map/ppermute | solution.py:431
  152.1 21.1 %collective-permute-start.27 = (bf16[80,8,128]{2,1,0:T(8,128)(2,1)S(1)}, bf16[80,8,128]{2,1,0:T(8,128)(2,1)S(1)}, u32[]{:S(2)}, u32[]{:S(2)}) collective-permute-start(bf16[80,8,128]{2,1,0:T(8,128)(2,1)S(1)} %copy-done.6), channel_id=1, source_target_pairs={{0,64},{8,72},{16,80},{24,88},{32,96},{40,104},{48,112},{56,120},{... | collective-permute-start | bytes 491528 | tf_op jit(solution)/shard_map/ppermute | solution.py:431
  174.2 17.9 %all-to-all-start.2 = ((bf16[8,5,10,8,128]{4,3,2,1,0:T(8,128)(2,1)}), bf16[8,5,10,8,128]{4,3,2,1,0:T(8,128)(2,1)S(1)}, u32[]{:S(2)}, u32[]{:S(2)}) async-start(bf16[8,5,10,8,128]{4,3,2,1,0:T(8,128)(2,1)} %stack.3), calls=%async_computation.2 | async-start | bytes 1638400 | tf_op jit(solution)/shard_map/all_to_all | solution.py:434
  192.1 27.9 %all-to-all-start.1 = ((bf16[8,11,10,8,128]{4,3,2,1,0:T(8,128)(2,1)}), bf16[8,11,10,8,128]{4,3,2,1,0:T(8,128)(2,1)S(1)}, u32[]{:S(2)}, u32[]{:S(2)}) async-start(bf16[8,11,10,8,128]{4,3,2,1,0:T(8,128)(2,1)} %bitcast.66), calls=%async_computation.1 | async-start | bytes 3604480 | tf_op jit(solution)/shard_map/all_to_all | solution.py:434
  220.1 87.0 %copy-start.5 = (bf16[1024]{0:T(1024)(128)(2,1)S(1)}, bf16[1024]{0:T(1024)(128)(2,1)}, u32[]{:S(2)}) copy-start(bf16[1024]{0:T(1024)(128)(2,1)} %param.15) | copy-start | bytes 6148
  220.1 87.0 %copy-start.2 = (f32[256,2]{0,1:T(2,128)S(1)}, f32[256,2]{0,1:T(2,128)}, u32[]{:S(2)}) copy-start(f32[256,2]{0,1:T(2,128)} %param.14) | copy-start | bytes 6148
  220.1 87.0 %copy-start.3 = (s32[2,256]{1,0:T(2,128)S(1)}, s32[2,256]{1,0:T(2,128)}, u32[]{:S(2)}) copy-start(s32[2,256]{1,0:T(2,128)} %get-tuple-element.40.pos_ref) | copy-start | bytes 6148
  220.1 49.5 %all-to-all-start.3 = ((bf16[8,5,10,8,128]{4,3,2,1,0:T(8,128)(2,1)}), bf16[8,5,10,8,128]{4,3,2,1,0:T(8,128)(2,1)S(1)}, u32[]{:S(2)}, u32[]{:S(2)}) async-start(bf16[8,5,10,8,128]{4,3,2,1,0:T(8,128)(2,1)} %bitcast.65), calls=%async_computation.3 | async-start | bytes 1638400 | tf_op jit(solution)/shard_map/all_to_all | solution.py:434
  226.0 9.2 %collective-permute-start.13 = (bf16[80,8,128]{2,1,0:T(8,128)(2,1)}, bf16[80,8,128]{2,1,0:T(8,128)(2,1)S(1)}, u32[]{:S(2)}, u32[]{:S(2)}) collective-permute-start(bf16[80,8,128]{2,1,0:T(8,128)(2,1)} %bitcast.82), channel_id=1, source_target_pairs={{0,120},{8,0},{16,8},{24,16},{32,24},{40,32},{48,40},{56,48},{64,5... | collective-permute-start | bytes 491528 | tf_op jit(solution)/shard_map/ppermute | solution.py:431
  230.4 7.4 %collective-permute-start.14 = (bf16[80,8,128]{2,1,0:T(8,128)(2,1)}, bf16[80,8,128]{2,1,0:T(8,128)(2,1)S(1)}, u32[]{:S(2)}, u32[]{:S(2)}) collective-permute-start(bf16[80,8,128]{2,1,0:T(8,128)(2,1)} %bitcast.81), channel_id=1, source_target_pairs={{0,8},{8,16},{16,24},{24,32},{32,40},{40,48},{48,56},{56,64},{64,7... | collective-permute-start | bytes 491528 | tf_op jit(solution)/shard_map/ppermute | solution.py:431
  230.4 11.0 %collective-permute-start.15 = (bf16[80,8,128]{2,1,0:T(8,128)(2,1)}, bf16[80,8,128]{2,1,0:T(8,128)(2,1)S(1)}, u32[]{:S(2)}, u32[]{:S(2)}) collective-permute-start(bf16[80,8,128]{2,1,0:T(8,128)(2,1)} %bitcast.80), channel_id=1, source_target_pairs={{0,112},{8,120},{16,0},{24,8},{32,16},{40,24},{48,32},{56,40},{64,... | collective-permute-start | bytes 491528 | tf_op jit(solution)/shard_map/ppermute | solution.py:431
  231.8 12.3 %collective-permute-start.16 = (bf16[80,8,128]{2,1,0:T(8,128)(2,1)}, bf16[80,8,128]{2,1,0:T(8,128)(2,1)S(1)}, u32[]{:S(2)}, u32[]{:S(2)}) collective-permute-start(bf16[80,8,128]{2,1,0:T(8,128)(2,1)} %bitcast.79), channel_id=1, source_target_pairs={{0,16},{8,24},{16,32},{24,40},{32,48},{40,56},{48,64},{56,72},{64,... | collective-permute-start | bytes 491528 | tf_op jit(solution)/shard_map/ppermute | solution.py:431
  232.8 36.8 %collective-permute-start.17 = (bf16[80,8,128]{2,1,0:T(8,128)(2,1)}, bf16[80,8,128]{2,1,0:T(8,128)(2,1)S(1)}, u32[]{:S(2)}, u32[]{:S(2)}) collective-permute-start(bf16[80,8,128]{2,1,0:T(8,128)(2,1)} %bitcast.78), channel_id=1, source_target_pairs={{0,104},{8,112},{16,120},{24,0},{32,8},{40,16},{48,24},{56,32},{64... | collective-permute-start | bytes 491528 | tf_op jit(solution)/shard_map/ppermute | solution.py:431
  235.2 35.3 %collective-permute-start.18 = (bf16[80,8,128]{2,1,0:T(8,128)(2,1)}, bf16[80,8,128]{2,1,0:T(8,128)(2,1)S(1)}, u32[]{:S(2)}, u32[]{:S(2)}) collective-permute-start(bf16[80,8,128]{2,1,0:T(8,128)(2,1)} %bitcast.72), channel_id=1, source_target_pairs={{0,24},{8,32},{16,40},{24,48},{32,56},{40,64},{48,72},{56,80},{64,... | collective-permute-start | bytes 491528 | tf_op jit(solution)/shard_map/ppermute | solution.py:431
  237.8 39.1 %collective-permute-start.19 = (bf16[80,8,128]{2,1,0:T(8,128)(2,1)}, bf16[80,8,128]{2,1,0:T(8,128)(2,1)S(1)}, u32[]{:S(2)}, u32[]{:S(2)}) collective-permute-start(bf16[80,8,128]{2,1,0:T(8,128)(2,1)} %bitcast.71), channel_id=1, source_target_pairs={{0,96},{8,104},{16,112},{24,120},{32,0},{40,8},{48,16},{56,24},{64... | collective-permute-start | bytes 491528 | tf_op jit(solution)/shard_map/ppermute | solution.py:431
  241.4 36.4 %collective-permute-start.20 = (bf16[80,8,128]{2,1,0:T(8,128)(2,1)}, bf16[80,8,128]{2,1,0:T(8,128)(2,1)S(1)}, u32[]{:S(2)}, u32[]{:S(2)}) collective-permute-start(bf16[80,8,128]{2,1,0:T(8,128)(2,1)} %bitcast.70), channel_id=1, source_target_pairs={{0,32},{8,40},{16,48},{24,56},{32,64},{40,72},{48,80},{56,88},{64,... | collective-permute-start | bytes 491528 | tf_op jit(solution)/shard_map/ppermute | solution.py:431
  244.0 43.4 %collective-permute-start.21 = (bf16[80,8,128]{2,1,0:T(8,128)(2,1)}, bf16[80,8,128]{2,1,0:T(8,128)(2,1)S(1)}, u32[]{:S(2)}, u32[]{:S(2)}) collective-permute-start(bf16[80,8,128]{2,1,0:T(8,128)(2,1)} %bitcast.69), channel_id=1, source_target_pairs={{0,88},{8,96},{16,104},{24,112},{32,120},{40,0},{48,8},{56,16},{64... | collective-permute-start | bytes 491528 | tf_op jit(solution)/shard_map/ppermute | solution.py:431
  269.6 17.8 %collective-permute-start.22 = (bf16[80,8,128]{2,1,0:T(8,128)(2,1)}, bf16[80,8,128]{2,1,0:T(8,128)(2,1)S(1)}, u32[]{:S(2)}, u32[]{:S(2)}) collective-permute-start(bf16[80,8,128]{2,1,0:T(8,128)(2,1)} %bitcast.68), channel_id=1, source_target_pairs={{0,40},{8,48},{16,56},{24,64},{32,72},{40,80},{48,88},{56,96},{64,... | collective-permute-start | bytes 491528 | tf_op jit(solution)/shard_map/ppermute | solution.py:431
  270.6 40.3 %collective-permute-start.28 = (bf16[80,8,128]{2,1,0:T(8,128)(2,1)}, bf16[80,8,128]{2,1,0:T(8,128)(2,1)S(1)}, u32[]{:S(2)}, u32[]{:S(2)}) collective-permute-start(bf16[80,8,128]{2,1,0:T(8,128)(2,1)} %bitcast.77), channel_id=1, source_target_pairs={{0,80},{8,88},{16,96},{24,104},{32,112},{40,120},{48,0},{56,8},{64... | collective-permute-start | bytes 491528 | tf_op jit(solution)/shard_map/ppermute | solution.py:431
  276.9 39.4 %collective-permute-start.29 = (bf16[80,8,128]{2,1,0:T(8,128)(2,1)}, bf16[80,8,128]{2,1,0:T(8,128)(2,1)S(1)}, u32[]{:S(2)}, u32[]{:S(2)}) collective-permute-start(bf16[80,8,128]{2,1,0:T(8,128)(2,1)} %bitcast.76), channel_id=1, source_target_pairs={{0,48},{8,56},{16,64},{24,72},{32,80},{40,88},{48,96},{56,104},{64... | collective-permute-start | bytes 491528 | tf_op jit(solution)/shard_map/ppermute | solution.py:431
  277.8 64.9 %collective-permute-start.30 = (bf16[80,8,128]{2,1,0:T(8,128)(2,1)}, bf16[80,8,128]{2,1,0:T(8,128)(2,1)S(1)}, u32[]{:S(2)}, u32[]{:S(2)}) collective-permute-start(bf16[80,8,128]{2,1,0:T(8,128)(2,1)} %bitcast.75), channel_id=1, source_target_pairs={{0,72},{8,80},{16,88},{24,96},{32,104},{40,112},{48,120},{56,0},{6... | collective-permute-start | bytes 491528 | tf_op jit(solution)/shard_map/ppermute | solution.py:431
  287.4 55.3 %collective-permute-start.31 = (bf16[80,8,128]{2,1,0:T(8,128)(2,1)}, bf16[80,8,128]{2,1,0:T(8,128)(2,1)S(1)}, u32[]{:S(2)}, u32[]{:S(2)}) collective-permute-start(bf16[80,8,128]{2,1,0:T(8,128)(2,1)} %bitcast.74), channel_id=1, source_target_pairs={{0,56},{8,64},{16,72},{24,80},{32,88},{40,96},{48,104},{56,112},{6... | collective-permute-start | bytes 491528 | tf_op jit(solution)/shard_map/ppermute | solution.py:431
  287.4 63.1 %collective-permute-start.32 = (bf16[80,8,128]{2,1,0:T(8,128)(2,1)}, bf16[80,8,128]{2,1,0:T(8,128)(2,1)S(1)}, u32[]{:S(2)}, u32[]{:S(2)}) collective-permute-start(bf16[80,8,128]{2,1,0:T(8,128)(2,1)} %bitcast.73), channel_id=1, source_target_pairs={{0,64},{8,72},{16,80},{24,88},{32,96},{40,104},{48,112},{56,120},{... | collective-permute-start | bytes 491528 | tf_op jit(solution)/shard_map/ppermute | solution.py:431
  307.1 0.9 copy-start.1
